TPU v7x, 512 devices: a whole 4x8x8 slice. The times are simulated.
512 devices in a mesh: sp: 64 (over z, y), tp: 8 (over x, core).
Axes of the slice: x: 4, y: 8, z: 8, core: 2. Of those that a mesh axis runs over, the one named last changes fastest.
Arguments:
- resid: bfloat16 [12288, 2048], P(('sp', 'tp')), may hold values from -6 to 6
- queries: bfloat16 [12288, 2048], P('sp', 'tp'), may hold values from -8 to 8
- keys: bfloat16 [12288, 512], P('sp', 'tp'), may hold values from -8 to 8
- values: bfloat16 [12288, 512], P('sp', 'tp'), may hold values from -6 to 6
- log_gates: float32 [12288, 32], P('sp', 'tp'), may hold values from -6144 to 0, as said below
- out_gate: bfloat16 [12288, 2048], P('sp', 'tp'), may hold values from -8 to 8
- out_weight: bfloat16 [2048, 2048], P('tp'), may hold values from -0.125 to 0.125
- post_gain: float32 [2048], replicated, may hold values from 0.1 to 1.9
- pre_gain: float32 [2048], replicated, may hold values from 0.1 to 1.9
- ffn_gain: float32 [2048], replicated, may hold values from 0.1 to 1.9
- gate_weight: bfloat16 [2048, 5632], P('sp', 'tp'), may hold values from -0.125 to 0.125
- up_weight: bfloat16 [2048, 5632], P('sp', 'tp'), may hold values from -0.125 to 0.125
- down_weight: bfloat16 [5632, 2048], P('tp', 'sp'), may hold values from -0.078125 to 0.078125
Outputs:
- result: bfloat16 [12288, 2048], P(('sp', 'tp'))
Inputs may be any that keep to these rules, and one draw needn't show every extreme that they name: Each head's column of log_gates never rises from one position to the next, and its first entry is at most 0.
All inputs are finite; a program needn't handle non-finite values.
Results may differ from a plain program's by a relative error of at most 0.017.
Values may be sent and summed in bfloat16 or wider, within the bound.
No kernel may reach another device: no remote copies, remote signals or barrier semaphores. Data moves between devices by JAX's collectives and lax.ppermute only.
A program may use at most 64 MiB of HBM per device.

v0:
```python
import jax
import jax.numpy as jnp
from jax import lax
from jax.sharding import Mesh
from jax.sharding import PartitionSpec as P

HD = 64
SP = ("sp_0", "sp_1")
SP_TP = ("sp_0", "sp_1", "tp")


EPS = 1e-06
KEY_BLOCK = 512


def sent_together(arrays, axis, dim, along):
    widths = [a.shape[along] for a in arrays]
    both = jnp.concatenate(arrays, axis=along)
    out = lax.all_gather(both, axis, axis=dim, tiled=True)
    return tuple(jnp.split(out, [sum(widths[:k]) for k in range(1, len(widths))], axis=along))


def in_order(blocks, dim):
    shape = list(blocks.shape[1:])
    shape[dim] *= blocks.shape[0]
    return jnp.moveaxis(blocks, 0, dim).reshape(shape)


def stacked_from(value, axes, order):
    blocks = value
    for k in order:
        blocks = lax.all_gather(blocks, axes[k])
    done = order[::-1]
    back = [done.index(k) for k in range(len(axes))]
    blocks = blocks.transpose(*back, *range(len(axes), blocks.ndim))
    return blocks.reshape(-1, *value.shape)


def gather_axes(value, axes, order, dim):
    return in_order(stacked_from(value, axes, order), dim)


def copy_for_each(value, axis):
    peers = lax.axis_size(axis)
    return lax.all_to_all(
        jnp.broadcast_to(value[None], (peers, *value.shape)), axis, 0, 0, tiled=True
    )


def gathered_copies(value, axis, dim):
    blocks = copy_for_each(value, axis)
    return in_order(blocks, dim)


def split_up(value, dim, peers):
    before, after = (value.shape[:dim], value.shape[dim + 1 :])
    return jnp.moveaxis(value.reshape(*before, peers, -1, *after), dim, 0)


def sum_at_owner(value, axis, dim):
    blocks = split_up(value, dim, lax.axis_size(axis))
    arrived = lax.all_to_all(blocks, axis, split_axis=0, concat_axis=0, tiled=True)
    return arrived.astype(jnp.float32).sum(axis=0)


def rms_scale(rows, gain):
    mean_sq = jnp.mean(rows * rows, axis=-1, keepdims=True)
    return rows * lax.rsqrt(mean_sq + EPS) * gain


def shards(
    resid,
    queries,
    keys,
    values,
    log_gates,
    out_gate,
    out_weight,
    post_gain,
    pre_gain,
    ffn_gain,
    gate_weight,
    up_weight,
    down_weight,
):
    rows = queries.shape[0]
    head_size = HD
    kv_local = keys.shape[1] // head_size
    q_local = queries.shape[1] // head_size
    group = q_local // kv_local
    scale = head_size ** (-0.5)
    offset = lax.axis_index(SP) * rows
    last = offset + rows - 1
    query_pos = offset + jnp.arange(rows, dtype=jnp.int32)
    full_gate, full_up = sent_together((gate_weight, up_weight), SP, 0, 1)
    full_down = gather_axes(down_weight, SP, (0, 1), 1)
    key_gates = gathered_copies(log_gates, SP, 0)
    query_blocks = queries.reshape(rows, kv_local, group, head_size)
    query_gates = log_gates.reshape(rows, kv_local, group).transpose(1, 2, 0)

    def key_block(carry, key_rows, value_rows, start):
        count = key_rows.shape[0]

        def compute(state):
            top, denom, accum = state
            scores = (
                jnp.einsum(
                    "tkgd,skd->kgts",
                    query_blocks,
                    key_rows.reshape(count, kv_local, head_size),
                    preferred_element_type=jnp.float32,
                )
                * scale
            )
            gates_here = (
                lax.dynamic_slice_in_dim(key_gates, start, count, 0)
                .reshape(count, kv_local, group)
                .transpose(1, 2, 0)
            )
            scores = scores + query_gates[:, :, :, None] - gates_here[:, :, None, :]
            causal = (start + jnp.arange(count, dtype=jnp.int32))[None, :] <= query_pos[:, None]
            scores = jnp.where(causal[None, None], scores, -jnp.inf)
            new_top = jnp.maximum(top, jnp.max(scores, axis=-1))
            shrink = jnp.exp(top - new_top)
            weights = jnp.exp(scores - new_top[..., None])
            denom = denom * shrink + jnp.sum(weights, axis=-1)
            accum = accum * shrink[..., None] + jnp.einsum(
                "kgts,skd->kgtd",
                weights.astype(jnp.bfloat16),
                value_rows.reshape(count, kv_local, head_size),
                preferred_element_type=jnp.float32,
            )
            return (new_top, denom, accum)

        def keep(state):
            return state

        return lax.cond(start <= last, compute, keep, carry)

    start_state = (
        jnp.full((kv_local, group, rows), -1e30, jnp.float32),
        jnp.zeros((kv_local, group, rows), jnp.float32),
        jnp.zeros((kv_local, group, rows, head_size), jnp.float32),
    )
    carry = start_state
    key_rows, value_rows = sent_together((keys, values), SP, 0, 1)
    count = key_rows.shape[0]
    blocks = count // KEY_BLOCK
    key_split = key_rows.reshape(blocks, KEY_BLOCK, key_rows.shape[1])
    value_split = value_rows.reshape(blocks, KEY_BLOCK, value_rows.shape[1])

    def advance(state, item):
        index, key_part, value_part = item
        return (key_block(state, key_part, value_part, index * KEY_BLOCK), None)

    carry, _ = lax.scan(
        advance, carry, (jnp.arange(blocks, dtype=jnp.int32), key_split, value_split)
    )
    top, denom, accum = carry
    attended = (accum / denom[..., None]).transpose(2, 0, 1, 3).reshape(rows, q_local * head_size)
    gated = (attended * jax.nn.sigmoid(out_gate.astype(jnp.float32))).astype(jnp.bfloat16)
    projected = sum_at_owner(
        jnp.dot(gated, out_weight, preferred_element_type=jnp.float32).astype(jnp.bfloat16), "tp", 0
    )
    mixed = resid.astype(jnp.float32) + rms_scale(projected, post_gain)
    normed = rms_scale(mixed, pre_gain).astype(jnp.bfloat16)
    normed_all = gathered_copies(normed, "tp", 0)
    gate = jnp.dot(normed_all, full_gate, preferred_element_type=jnp.float32)
    up = jnp.dot(normed_all, full_up, preferred_element_type=jnp.float32)
    hidden = (jax.nn.silu(gate) * up).astype(jnp.bfloat16)
    ffn_partial = jnp.dot(hidden, full_down, preferred_element_type=jnp.float32)
    ffn = sum_at_owner(ffn_partial.astype(jnp.bfloat16), "tp", 0)
    return (mixed + rms_scale(ffn, ffn_gain)).astype(jnp.bfloat16)


def solution(mesh):
    split = Mesh(mesh.devices.reshape(8, 8, mesh.shape["tp"]), ("sp_0", "sp_1", "tp"))
    in_specs = (
        P(SP_TP, None),
        P(SP, "tp"),
        P(SP, "tp"),
        P(SP, "tp"),
        P(SP, "tp"),
        P(SP, "tp"),
        P("tp", None),
        P(),
        P(),
        P(),
        P(SP, "tp"),
        P(SP, "tp"),
        P("tp", SP),
    )
    out_specs = P(SP_TP, None)
    return jax.shard_map(
        shards, mesh=split, in_specs=in_specs, out_specs=out_specs, check_vma=False
    )
```

profile of v0, /device:TPU:1, one launch (start us, length us, event | category | flops | bytes accessed | tf_op | source)
XLA Modules:
  0.0 272.2 jit_solution(14478669596774093260)
XLA Ops:
  6.5 1.0 copy.35
  7.5 0.9 copy.34
  8.4 0.7 pad_maximum_fusion.1
  9.2 28.2 %all-gather.2 = bf16[8,704,32]{1,2,0:T(8,128)(2,1)} all-gather(bf16[1,704,32]{1,2,0:T(8,128)(2,1)} %bitcast.89), channel_id=2, replica_groups=mesh['sp_0'=8,'sp_1'=8,'tp'=8] {'sp_0'}, dimensions={0}, use_global_device_ids=true | all-gather | bytes 405504 | tf_op jit(solution)/shard_map/all_gather | solution.py:32
  37.5 1.5 pad_maximum_fusion
  39.1 1.4 broadcast_in_dim.36
  40.5 10.6 %all-to-all-start = ((f32[64,192,4]{1,2,0:T(4,128)}), f32[64,192,4]{1,2,0:T(4,128)S(1)}, u32[]{:S(2)}, u32[]{:S(2)}) async-start(f32[64,192,4]{1,2,0:T(4,128)} %broadcast_in_dim.36), calls=%async_computation | async-start | bytes 524288 | tf_op jit(solution)/shard_map/all_to_all | solution.py:45
  51.2 12.2 %all-to-all-done = f32[64,192,4]{1,2,0:T(4,128)S(1)} async-done(((f32[64,192,4]{1,2,0:T(4,128)}), f32[64,192,4]{1,2,0:T(4,128)S(1)}, u32[]{:S(2)}, u32[]{:S(2)}) %all-to-all-start) | async-done | bytes 196640 | tf_op jit(solution)/shard_map/all_to_all | solution.py:45
  63.6 34.7 %all-gather.7.cloned.1.call-done = bf16[12288,128]{1,0:T(8,128)(2,1)} async-done(((bf16[192,128]{1,0:T(8,128)(2,1)}), bf16[12288,128]{1,0:T(8,128)(2,1)}) %all-gather.7.cloned.1.call-update) | async-done | bytes 3145744 | tf_op jit(solution)/shard_map/all_gather | solution.py:19
  98.4 6.2 %fusion.40 = (bf16[12288,64]{1,0:T(8,128)(2,1)}, bf16[12288,64]{1,0:T(8,128)(2,1)}) fusion(bf16[12288,128]{1,0:T(8,128)(2,1)} %all-gather.7.cloned.1.call-done), kind=kLoop, calls=%fused_computation.59 | loop fusion | bytes 6291456 | tf_op jit(solution)/shard_map/split | solution.py:20
  104.6 4.3 %copy.40 = bf16[24,512,64]{1,2,0:T(8,128)(2,1)} copy(bf16[24,512,64]{2,1,0:T(8,128)(2,1)} %bitcast.77) | data formatting | bytes 3145728
  108.8 3.1 %copy.41 = bf16[24,512,64]{1,2,0:T(8,128)(2,1)S(1)} copy(bf16[24,512,64]{2,1,0:T(8,128)(2,1)} %bitcast.76) | data formatting | bytes 3145728
  112.0 31.5 %while.15 = (s32[]{:T(128)}, f32[1,4,192]{2,1,0:T(4,128)S(1)}, f32[1,4,192]{2,1,0:T(4,128)S(1)}, f32[1,4,192,64]{2,3,1,0:T(8,128)S(1)}, s32[24]{0:T(128)S(1)}, /...) while((s32[]{:T(128)}, f32[1,4,192]{2,1,0:T(4,128)S(1)}, ...), condition=%wide.region_5.6_spmd.clone, body=%wide.region_0.5_spmd.clone.sunk | while | flops 104401856 | bytes 5690237 | solution.py:156
  113.2 3.0 %conditional.3 = ((f32[1,4,192]{2,1,0:T(4,128)S(1)}, f32[1,4,192]{2,1,0:T(4,128)S(1)}, f32[1,4,192,64]{2,3,1,0:T(8,128)S(1)})) conditional(s32[]{:T(128)} %convert_element_type.74, (f32[1,4,192]{2,1,0:T(4,128)S(1)}, f32[1,4,192]{2,1,0:T(4,128)S(1)}, f32[1,4,192,64]{2,3,1,0:T(8,128)S(1)}) %tuple.43, (s32[]{:T(128)}, s32[]{:T(128)}, ...), branch_computations={%region_1.1_spmd, %region_2.4_spmd} | conditional | flops 104401856 | bytes 5689170 | solution.py:138
  113.4 1.5 fusion.39
  115.0 0.6 fusion.5
  116.2 0.6 dynamic_slice.39
  119.8 0.6 dynamic_slice.39
  123.3 0.6 dynamic_slice.39
  126.9 0.6 dynamic_slice.39
  130.5 0.6 dynamic_slice.39
  134.0 0.6 dynamic_slice.39
  144.2 20.7 %all_to_all.20 = bf16[8,24,2048]{2,1,0:T(8,128)(2,1)S(1)} all-to-all(bf16[8,24,2048]{2,1,0:T(8,128)(2,1)S(1)} %bitcast.80), channel_id=1, replica_groups=mesh['sp_0'=8,'sp_1'=8,'tp'=8] {'tp'}, dimensions={0} | all-to-all | bytes 1572864 | tf_op jit(solution)/shard_map/all_to_all | solution.py:62
  165.4 1.0 broadcast_in_dim.37
  166.4 4.5 %all-to-all-start.2 = ((bf16[8,24,2048]{2,1,0:T(8,128)(2,1)}), bf16[8,24,2048]{2,1,0:T(8,128)(2,1)S(1)}, u32[]{:S(2)}, u32[]{:S(2)}) async-start(bf16[8,24,2048]{2,1,0:T(8,128)(2,1)} %broadcast_in_dim.37), calls=%async_computation.2 | async-start | bytes 1572864 | tf_op jit(solution)/shard_map/all_to_all | solution.py:45
  170.9 3.8 %copy.43 = bf16[8,8,704,32]{2,3,1,0:T(8,128)(2,1)} copy(bf16[8,8,704,32]{2,3,0,1:T(8,128)(2,1)} %bitcast.78) | data formatting | bytes 5767168 | tf_op jit(solution)/shard_map/transpose | solution.py:35
  174.7 8.4 %all-to-all-done.2 = bf16[8,24,2048]{2,1,0:T(8,128)(2,1)S(1)} async-done(((bf16[8,24,2048]{2,1,0:T(8,128)(2,1)}), bf16[8,24,2048]{2,1,0:T(8,128)(2,1)S(1)}, u32[]{:S(2)}, u32[]{:S(2)}) %all-to-all-start.2) | async-done | bytes 786464 | tf_op jit(solution)/shard_map/all_to_all | solution.py:45
  183.1 53.6 %all-gather.9.cloned.1.call-done = bf16[2048,1408]{1,0:T(8,128)(2,1)} async-done(((bf16[32,1408]{1,0:T(8,128)(2,1)}), bf16[2048,1408]{1,0:T(8,128)(2,1)}) %all-gather.9.cloned.1.call-update) | async-done | bytes 5767184 | tf_op jit(solution)/shard_map/all_gather | solution.py:19
  236.7 2.7 fusion.20
  239.3 5.0 %convolution_convert_fusion = bf16[192,2048]{1,0:T(8,128)(2,1)S(1)} fusion(bf16[704,2048]{0,1:T(8,128)(2,1)} %bitcast.79, bf16[192,2048]{1,0:T(8,128)(2,1)S(1)} %bitcast.85, bf16[2048,1408]{1,0:T(8,128)(2,1)} %all-gather.9.cloned.1.call-done, f32[192,704]{1,0:T(8,128)S(1)} %fusion.20), kind=kOutput, calls=%fused_computation.30 | convolution fusion | flops 1108500480 | bytes 8404992 | tf_op jit(solution)/shard_map/dot_general | solution.py:171
  244.4 20.3 %all_to_all.21 = bf16[8,24,2048]{2,1,0:T(8,128)(2,1)S(1)} all-to-all(bf16[8,24,2048]{2,1,0:T(8,128)(2,1)S(1)} %bitcast.86), channel_id=1, replica_groups=mesh['sp_0'=8,'sp_1'=8,'tp'=8] {'tp'}, dimensions={0} | all-to-all | bytes 1572864 | tf_op jit(solution)/shard_map/all_to_all | solution.py:62
  264.9 0.8 add_convert_fusion
  (115 shorter events, 13.2 us)
Async XLA Ops:
  6.5 137.2 %copy-start = (bf16[256,2048]{1,0:T(8,128)(2,1)S(1)}, bf16[256,2048]{1,0:T(8,128)(2,1)}, u32[]{:S(2)}) copy-start(bf16[256,2048]{1,0:T(8,128)(2,1)} %param.23) | copy-start | bytes 3145732
  6.5 44.5 %copy-start.3 = (bf16[192,256]{1,0:T(8,128)(2,1)S(1)}, bf16[192,256]{1,0:T(8,128)(2,1)}, u32[]{:S(2)}) copy-start(bf16[192,256]{1,0:T(8,128)(2,1)} %param.18) | copy-start | bytes 294916
  6.5 91.8 %all-gather.7.cloned.1.call-start = ((), (), s32[]{:S(2)}) async-start(), calls=%async_computation.4 | async-start | bytes 3194880 | tf_op jit(solution)/shard_map/all_gather | solution.py:19
  9.1 161.8 %all-gather.11.cloned.1.call-start = ((), (), s32[]{:S(2)}) async-start(), calls=%async_computation.6 | async-start | bytes 3538944 | tf_op jit(solution)/shard_map/all_gather | solution.py:32
  37.5 199.2 %all-gather.9.cloned.1.call-start = ((), (), s32[]{:S(2)}) async-start(), calls=%async_computation.5 | async-start | bytes 5857280 | tf_op jit(solution)/shard_map/all_gather | solution.py:19
  40.5 22.9 %all-to-all-start = ((f32[64,192,4]{1,2,0:T(4,128)}), f32[64,192,4]{1,2,0:T(4,128)S(1)}, u32[]{:S(2)}, u32[]{:S(2)}) async-start(f32[64,192,4]{1,2,0:T(4,128)} %broadcast_in_dim.36), calls=%async_computation | async-start | bytes 524288 | tf_op jit(solution)/shard_map/all_to_all | solution.py:45
  108.8 3.2 %copy-start.7 = (f32[192,4]{0,1:T(4,128)S(1)}, f32[192,4]{0,1:T(4,128)}, u32[]{:S(2)}) copy-start(f32[192,4]{0,1:T(4,128)} %param.21) | copy-start | bytes 9220
  112.0 31.7 %copy-start.2 = (bf16[192,256]{1,0:T(8,128)(2,1)S(1)}, bf16[192,256]{1,0:T(8,128)(2,1)}, u32[]{:S(2)}) copy-start(bf16[192,256]{1,0:T(8,128)(2,1)} %param.22) | copy-start | bytes 294916
  144.1 20.9 %copy-start.1 = (bf16[24,2048]{1,0:T(8,128)(2,1)S(1)}, bf16[24,2048]{1,0:T(8,128)(2,1)}, u32[]{:S(2)}) copy-start(bf16[24,2048]{1,0:T(8,128)(2,1)} %param.17) | copy-start | bytes 294916
  144.1 20.9 %copy-start.4 = (f32[2048]{0:T(1024)S(1)}, f32[2048]{0:T(1024)}, u32[]{:S(2)}) copy-start(f32[2048]{0:T(1024)} %param.24) | copy-start | bytes 24580
  144.2 21.2 %copy-start.6 = (f32[2048]{0:T(1024)S(1)}, f32[2048]{0:T(1024)}, u32[]{:S(2)}) copy-start(f32[2048]{0:T(1024)} %param.25) | copy-start | bytes 24580
  166.4 16.7 %all-to-all-start.2 = ((bf16[8,24,2048]{2,1,0:T(8,128)(2,1)}), bf16[8,24,2048]{2,1,0:T(8,128)(2,1)S(1)}, u32[]{:S(2)}, u32[]{:S(2)}) async-start(bf16[8,24,2048]{2,1,0:T(8,128)(2,1)} %broadcast_in_dim.37), calls=%async_computation.2 | async-start | bytes 1572864 | tf_op jit(solution)/shard_map/all_to_all | solution.py:45
  244.4 20.5 %copy-start.5 = (f32[2048]{0:T(1024)S(1)}, f32[2048]{0:T(1024)}, u32[]{:S(2)}) copy-start(f32[2048]{0:T(1024)} %param.26) | copy-start | bytes 24580
Sparse Core Ops, SparseCore 0:
  10.3 87.9 all-gather.6
  100.5 46.9 all-gather.10
  150.4 86.1 all-gather.8
where the time goes:
time: 274 us; the launch traced here: 272 us
  waiting for transfers between devices  109 us (40%)
  blocking collectives  69.2 us (25%)
  local copies, waits for them, and re-layouts  35.7 us (13%)
  starting transfers between devices  15.2 us (6%)
  loops' own time  15.1 us (6%)
  between operations  13.3 us (5%)
  matrix products  10.2 us (4%)
  other arithmetic  4.63 us (2%)
    all_gather x2, waiting for transfers between devices, sent_together(): out = lax.all_gather(both, axis, axis=dim, tiled=True)  88.3 us
    all_to_all x2, blocking collectives, sum_at_owner(): lax.all_to_all(blocks, axis, split_axis=0, concat_axis=0, tiled=True)  40.9 us
    all_gather x1, blocking collectives, stacked_from(): blocks = lax.all_gather(blocks, axes[k])  28.2 us
    all_to_all x2, waiting for transfers between devices, copy_for_each(): lax.all_to_all(jnp.broadcast_to(value[None], (peers, *value.shape)), axis...  20.6 us
    all_to_all x2, starting transfers between devices, copy_for_each(): lax.all_to_all(jnp.broadcast_to(value[None], (peers, *value.shape)), axis...  15.1 us
    another operation x1, loops' own time, shards(): lax.scan(advance, carry, (jnp.arange(blocks, dtype=jnp.int32), key_split,...  14.7 us
    dynamic_slice x24, local copies, waits for them, and re-layouts, shards(): lax.scan(advance, carry, (jnp.arange(blocks, dtype=jnp.int32), key_split,...  13.4 us
    unnamed x21, local copies, waits for them, and re-layouts  9.37 us
  transfers between devices with their start and end apart: 5, of which 4 were waited for; matrix products, arithmetic and copies ran while one was open for 14% of the time, Pallas kernels for 0%

commit v1 on v0

v1 whole, which is shorter than its diff:
```python
import jax
import jax.numpy as jnp
from jax import lax
from jax.experimental import pallas as pl
from jax.experimental.pallas import tpu as pltpu
from jax.sharding import Mesh
from jax.sharding import PartitionSpec as P

HD = 64
HL = 4
ROWS = 192
QG = 4
ZH = 8 // QG
YS = 8
NB = ZH * YS
TILE = 384
CH = 256
QR = ROWS * HL
KP = 224
OUTR = 72
FFL = 704
GU = 2 * FFL
WC = 2176
EPS = 1e-06
LOW = -1e30
GAP = 56.0

SP = ("zh", "zl", "y")
TP = ("x", "c")
F32 = jnp.float32
BF16 = jnp.bfloat16
NT = (((1,), (1,)), ((), ()))


def pieces(value):
    one = lax.reduce_precision(value, 8, 7)
    rest = value - one
    two = lax.reduce_precision(rest, 8, 7)
    return one, two, rest - two


def kernel_pieces(value):
    one = value.astype(BF16).astype(F32)
    rest = value - one
    two = rest.astype(BF16).astype(F32)
    return one, two, rest - two


def key_payload(keys, values, log_gates):
    k32 = keys.astype(F32)
    norm = jnp.sqrt(jnp.max(jnp.sum(k32 * k32, axis=1))) * 1.01
    parts = jnp.concatenate(pieces(log_gates), axis=1).T
    ones = jnp.ones((3, ROWS), F32)
    last = jnp.full((1, ROWS), norm, F32)
    side = jnp.concatenate([parts, ones, last], axis=0).astype(BF16)
    left = side[:, :128]
    right = jnp.pad(side[:, 128:], ((0, 0), (0, 64)))
    return jnp.concatenate([jnp.concatenate([keys, values], axis=1), left, right], axis=0)


def attention_kernel(pos, kv, q, own, out, kc, vt, qc, acc, ls, ms):
    zh = pos[0]
    zl = pos[1]
    y = pos[2]
    kc[:, 128:256] = jnp.zeros((NB * ROWS, 128), BF16)
    kmax = jnp.zeros((1, 1), F32)
    for b in range(NB):
        base = b * ROWS
        kc[base : base + ROWS, 0:128] = kv[b, 0:ROWS, :]
        left = kv[b, 192:208, :].astype(F32)
        right = kv[b, 208:224, :].astype(F32)
        kc[base : base + 128, 128:144] = left.T.astype(BF16)
        kc[base + 128 : base + ROWS, 128:144] = right.T[0:64].astype(BF16)
        kmax = jnp.maximum(kmax, left[15:16, 0:1])
    for i in range(NB * ROWS // TILE):
        vt[i] = kc[i * TILE : (i + 1) * TILE, 0:128].T[64:128]
    lane = lax.broadcasted_iota(jnp.int32, (ROWS, 128), 1)
    qmax = jnp.zeros((1, 1), F32)
    for j in range(QG):
        block = jnp.where(j > zl, zh * YS + YS - 1, jnp.maximum(zh * YS - 1, 0))
        ends = kv[block, 208:224, :].astype(F32)[:, 63:64]
        for h in range(HL):
            end = ends[h : h + 1] + ends[4 + h : 5 + h] + ends[8 + h : 9 + h]
            ref = jnp.where(j == zl, own[:, h : h + 1], jnp.broadcast_to(end, (ROWS, 1)))
            qh = q[j, :, h * HD : (h + 1) * HD].astype(F32) * 0.125
            norm = jnp.sqrt(jnp.sum(qh * qh, axis=1, keepdims=True))
            qmax = jnp.maximum(qmax, jnp.max(norm, axis=0, keepdims=True))
            one, two, three = kernel_pieces(ref - norm * kmax)
            side = jnp.where((lane == h) | (lane == 4 + h) | (lane == 8 + h), -1.0, 0.0)
            side = jnp.where(lane == 12, one, side)
            side = jnp.where(lane == 13, two, side)
            side = jnp.where(lane == 14, three, side)
            at = slice(h * ROWS, (h + 1) * ROWS)
            qc[j, at, 0:128] = jnp.concatenate([qh, jnp.zeros((ROWS, HD), F32)], axis=1).astype(BF16)
            qc[j, at, 128:256] = side.astype(BF16)
    acc[...] = jnp.zeros(acc.shape, F32)
    ls[...] = jnp.zeros(ls.shape, F32)
    ms[...] = jnp.full(ms.shape, LOW, F32)
    fast = (2.0 * qmax * kmax)[0, 0] <= GAP

    def unit(j, hz, masked, bounded):
        def step(i, none):
            tile = hz * (YS * ROWS // TILE) + i
            kk = kc[pl.ds(pl.multiple_of(tile * TILE, TILE), TILE), :]
            vv = vt[tile]
            for n in range(QR // CH):
                cols = slice(n * CH, (n + 1) * CH)
                s = lax.dot_general(kk, qc[j, cols, :], NT, preferred_element_type=F32)
                if masked:
                    col = n * CH + lax.broadcasted_iota(jnp.int32, (TILE, CH), 1)
                    for h in range(1, HL):
                        col = jnp.where(col >= ROWS, col - ROWS, col)
                    row = i * TILE + lax.broadcasted_iota(jnp.int32, (TILE, CH), 0)
                    s = jnp.where(row <= col + y * ROWS, s, LOW)
                if bounded:
                    w = jnp.exp(s)
                    ls[j, :, cols] += jnp.sum(w.reshape(TILE // 8, 8, CH), axis=0)
                    acc[j, :, cols] += jnp.dot(vv, w.astype(BF16), preferred_element_type=F32)
                else:
                    old = ms[j, 0:1, cols]
                    new = jnp.maximum(old, jnp.max(s, axis=0, keepdims=True))
                    shrink = jnp.exp(old - new)
                    w = jnp.exp(s - new)
                    ms[j, :, cols] = jnp.broadcast_to(new, (8, CH))
                    part = jnp.sum(w.reshape(TILE // 8, 8, CH), axis=0)
                    ls[j, :, cols] = ls[j, :, cols] * shrink + part
                    got = jnp.dot(vv, w.astype(BF16), preferred_element_type=F32)
                    acc[j, :, cols] = acc[j, :, cols] * shrink + got
            return none

        lax.fori_loop(0, YS * ROWS // TILE, step, 0)

    def units(bounded):
        def one(u, none):
            j = u // ZH
            hz = u % ZH
            edge = (hz == zh) & (j == zl)
            whole = (hz < zh) | ((hz == zh) & (j > zl))

            @pl.when(whole)
            def _():
                unit(j, hz, False, bounded)

            @pl.when(edge)
            def _():
                unit(j, hz, True, bounded)

            return none

        lax.fori_loop(0, QG * ZH, one, 0)

    @pl.when(fast)
    def _():
        units(True)
        ms[...] = jnp.zeros(ms.shape, F32)

    @pl.when(jnp.logical_not(fast))
    def _():
        units(False)

    spot = lax.broadcasted_iota(jnp.int32, (8, 256), 1)
    pick = jnp.where((spot >= 140) & (spot <= 142), 1.0, 0.0).astype(BF16)
    line = lax.broadcasted_iota(jnp.int32, (8, QR), 0)
    for j in range(QG):
        shift = lax.dot_general(pick, qc[j], NT, preferred_element_type=F32)[0:1]
        total = jnp.sum(ls[j], axis=0, keepdims=True)
        top = jnp.where(total > 0.0, ms[j, 0:1, :] - shift, LOW)
        stats = jnp.zeros((8, QR), F32)
        for k, part in enumerate(kernel_pieces(total) + kernel_pieces(top)):
            stats = jnp.where(line == k, part, stats)
        out[j, 0:HD, :] = acc[j].astype(BF16)
        out[j, HD:OUTR, :] = stats.astype(BF16)


def attention(pos, kv, q, own):
    vmem = pl.BlockSpec(memory_space=pltpu.VMEM)
    return pl.pallas_call(
        attention_kernel,
        out_shape=jax.ShapeDtypeStruct((QG, OUTR, QR), BF16),
        in_specs=[pl.BlockSpec(memory_space=pltpu.SMEM), vmem, vmem, vmem],
        out_specs=vmem,
        scratch_shapes=[
            pltpu.VMEM((NB * ROWS, 256), BF16),
            pltpu.VMEM((NB * ROWS // TILE, HD, TILE), BF16),
            pltpu.VMEM((QG, QR, 256), BF16),
            pltpu.VMEM((QG, HD, QR), F32),
            pltpu.VMEM((QG, 8, QR), F32),
            pltpu.VMEM((QG, 8, QR), F32),
        ],
        compiler_params=pltpu.CompilerParams(vmem_limit_bytes=48 * 1024 * 1024),
        cost_estimate=pl.CostEstimate(flops=12_000_000_000, bytes_accessed=4_000_000, transcendentals=9_000_000),
        name="attention",
    )(pos, kv, q, own)


def merge_kernel(parts, gates, weight, out):
    tops = []
    sums = []
    for j in range(QG):
        stats = parts[j, HD:OUTR, :].astype(F32)
        sums.append(stats[0:1] + stats[1:2] + stats[2:3])
        tops.append(stats[3:4] + stats[4:5] + stats[5:6])
    top = tops[0]
    for j in range(1, QG):
        top = jnp.maximum(top, tops[j])
    total = jnp.zeros((1, QR), F32)
    mixed = jnp.zeros((HD, QR), F32)
    for j in range(QG):
        scale = jnp.exp(tops[j] - top)
        total = total + sums[j] * scale
        mixed = mixed + parts[j, 0:HD, :].astype(F32) * scale
    rows = (mixed / total).T
    rows = jnp.concatenate([rows[h * ROWS : (h + 1) * ROWS] for h in range(HL)], axis=1)
    gated = (rows * jax.nn.sigmoid(gates[...].astype(F32))).astype(BF16)
    out[...] = jnp.dot(gated, weight[...], preferred_element_type=F32).astype(BF16)


def merge(parts, gates, weight):
    return pl.pallas_call(
        merge_kernel,
        out_shape=jax.ShapeDtypeStruct((ROWS, weight.shape[1]), BF16),
        compiler_params=pltpu.CompilerParams(vmem_limit_bytes=32 * 1024 * 1024),
        cost_estimate=pl.CostEstimate(flops=400_000_000, bytes_accessed=2_000_000, transcendentals=50_000),
        name="merge",
    )(parts, gates, weight)


FC = 512


def ffn_kernel(rows, weights, out, wv, acc, hid, sems):
    count = weights.shape[0] // FC

    def first(k):
        at = (pl.ds(k * FC, FC), pl.ds(0, GU))
        return pltpu.make_async_copy(weights.at[at], wv.at[at], sems.at[k])

    def second(k):
        at = (pl.ds(k * FC, FC), pl.ds(GU, WC - GU))
        return pltpu.make_async_copy(weights.at[at], wv.at[at], sems.at[count + k])

    for k in range(count):
        first(k).start()
    for k in range(count):
        second(k).start()
    for k in range(count):
        first(k).wait()
        part = jnp.dot(
            rows[:, k * FC : (k + 1) * FC],
            wv[k * FC : (k + 1) * FC, 0:GU],
            preferred_element_type=F32,
        )
        if k == 0:
            acc[...] = part
        else:
            acc[...] += part
    gate = acc[:, 0:FFL]
    up = acc[:, FFL:GU]
    hidden = gate / (1.0 + jnp.exp(-gate)) * up
    hid[:, FFL:] = jnp.zeros((ROWS, WC - GU - FFL), BF16)
    hid[:, 0:FFL] = hidden.astype(BF16)
    for k in range(count):
        second(k).wait()
        out[:, k * FC : (k + 1) * FC] = lax.dot_general(
            hid[...], wv[k * FC : (k + 1) * FC, GU:WC], NT, preferred_element_type=F32
        ).astype(BF16)


def ffn(rows, weights):
    wide = weights.shape[0]
    return pl.pallas_call(
        ffn_kernel,
        out_shape=jax.ShapeDtypeStruct((ROWS, wide), BF16),
        in_specs=[pl.BlockSpec(memory_space=pltpu.VMEM), pl.BlockSpec(memory_space=pl.ANY)],
        out_specs=pl.BlockSpec(memory_space=pltpu.VMEM),
        scratch_shapes=[
            pltpu.VMEM((wide, WC), BF16),
            pltpu.VMEM((ROWS, GU), F32),
            pltpu.VMEM((ROWS, WC - GU), BF16),
            pltpu.SemaphoreType.DMA((2 * (wide // FC),)),
        ],
        compiler_params=pltpu.CompilerParams(vmem_limit_bytes=40 * 1024 * 1024),
        cost_estimate=pl.CostEstimate(flops=1_700_000_000, bytes_accessed=10_000_000, transcendentals=140_000),
        name="ffn",
    )(rows, weights)


def copies(value, axis):
    peers = lax.axis_size(axis)
    return lax.all_to_all(jnp.broadcast_to(value[None], (peers, *value.shape)), axis, 0, 0, tiled=True)


def sum_at_owner(value):
    peers = lax.axis_size(TP)
    blocks = value.reshape(peers, value.shape[0] // peers, value.shape[1])
    arrived = lax.all_to_all(blocks, TP, 0, 0, tiled=True)
    return arrived.astype(F32).sum(axis=0)


def rms_scale(rows, gain):
    mean_sq = jnp.mean(rows * rows, axis=-1, keepdims=True)
    return rows * lax.rsqrt(mean_sq + EPS) * gain


def shards(
    resid,
    queries,
    keys,
    values,
    log_gates,
    out_gate,
    out_weight,
    post_gain,
    pre_gain,
    ffn_gain,
    gate_weight,
    up_weight,
    down_weight,
):
    pad = jnp.zeros((gate_weight.shape[0], WC - GU - FFL), BF16)
    packed = jnp.concatenate([gate_weight, up_weight, down_weight.T, pad], axis=1)
    weights = lax.all_gather(packed, SP, axis=0, tiled=True)
    kv = copies(key_payload(keys, values, log_gates), ("zh", "y"))
    q_all = copies(queries, "zl")
    pos = jnp.stack([lax.axis_index("zh"), lax.axis_index("zl"), lax.axis_index("y")]).astype(jnp.int32)
    parts = attention(pos, kv, q_all, log_gates)
    parts = lax.all_to_all(parts, "zl", 0, 0, tiled=True)
    projected = sum_at_owner(merge(parts, out_gate, out_weight))
    mixed = resid.astype(F32) + rms_scale(projected, post_gain)
    normed = rms_scale(mixed, pre_gain).astype(BF16)
    normed_all = lax.all_gather(normed, TP, axis=0, tiled=True)
    total = sum_at_owner(ffn(normed_all, weights))
    return (mixed + rms_scale(total, ffn_gain)).astype(BF16)


def solution(mesh):
    split = Mesh(mesh.devices.reshape(ZH, QG, YS, 4, 2), ("zh", "zl", "y", "x", "c"))
    in_specs = (
        P((*SP, *TP), None),
        P(SP, TP),
        P(SP, TP),
        P(SP, TP),
        P(SP, TP),
        P(SP, TP),
        P(TP, None),
        P(),
        P(),
        P(),
        P(SP, TP),
        P(SP, TP),
        P(TP, SP),
    )
    return jax.shard_map(
        shards, mesh=split, in_specs=in_specs, out_specs=P((*SP, *TP), None), check_vma=False
    )
```

time: 274 us -> 183 us (0.67)
  the two profiles are of different devices: /device:TPU:1 before, /device:TPU:304 now
where the time goes in v1:
time: 183 us; the launch traced here: 182 us
  blocking collectives  70.8 us (39%)
  Pallas kernels  36.3 us (20%)
  waiting for transfers between devices  33 us (18%)
  starting transfers between devices  16.4 us (9%)
  between operations  14.2 us (8%)
  local copies, waits for them, and re-layouts  8.64 us (5%)
  other arithmetic  2.49 us (1%)
    all_to_all x2, blocking collectives, sum_at_owner(): arrived = lax.all_to_all(blocks, TP, 0, 0, tiled=True)  36.6 us
    all_to_all x2, waiting for transfers between devices, copies(): lax.all_to_all(jnp.broadcast_to(value[None], (peers, *value.shape)), axis...  33 us
    pallas_call x1, Pallas kernels, attention(): pl.pallas_call(attention_kernel, out_shape=jax.ShapeDtypeStruct((QG, OUTR...  31.3 us
    all_to_all x1, blocking collectives, shards(): parts = lax.all_to_all(parts, 'zl', 0, 0, tiled=True)  20.7 us
    all_to_all x2, starting transfers between devices, copies(): lax.all_to_all(jnp.broadcast_to(value[None], (peers, *value.shape)), axis...  16.4 us
    all_gather x1, blocking collectives, shards(): normed_all = lax.all_gather(normed, TP, axis=0, tiled=True)  13.4 us
    pallas_call x1, Pallas kernels, ffn(): pl.pallas_call(ffn_kernel, out_shape=jax.ShapeDtypeStruct((ROWS, wide), B...  4.37 us
    unnamed x22, local copies, waits for them, and re-layouts  3.79 us
  transfers between devices with their start and end apart: 3, of which 2 were waited for; matrix products, arithmetic and copies ran while one was open for 3% of the time, Pallas kernels for 18%

profile of v1, /device:TPU:304, one launch (start us, length us, event | category | flops | bytes accessed | tf_op | source)
XLA Modules:
  0.0 181.8 jit_solution(16254994210090591170)
XLA Ops:
  6.6 1.6 concatenate.21
  8.2 1.7 broadcast_in_dim.13
  9.9 4.6 %all-to-all-start.1 = ((bf16[4,192,256]{2,1,0:T(8,128)(2,1)}), bf16[4,192,256]{2,1,0:T(8,128)(2,1)S(1)}, u32[]{:S(2)}, u32[]{:S(2)}) async-start(bf16[4,192,256]{2,1,0:T(8,128)(2,1)} %broadcast_in_dim.13), calls=%async_computation.1 | async-start | bytes 786432 | tf_op jit(solution)/shard_map/all_to_all | solution.py:290
  14.5 0.6 reduce_max.9
  15.8 0.1 pad.11.clone
  15.9 0.1 pad.10.clone
  16.0 0.1 maximum_maximum_fusion
  16.1 0.1 copy.14
  16.2 0.1 copy.18
  16.3 0.1 fusion.1
  16.4 0.1 copy.16
  16.5 9.6 %all-to-all-done.1.q = bf16[4,192,256]{2,1,0:T(8,128)(2,1)S(1)} async-done(((bf16[4,192,256]{2,1,0:T(8,128)(2,1)}), bf16[4,192,256]{2,1,0:T(8,128)(2,1)S(1)}, u32[]{:S(2)}, u32[]{:S(2)}) %all-to-all-start.1) | async-done | bytes 393248 | tf_op jit(solution)/shard_map/all_to_all | solution.py:290
  26.2 1.1 broadcast_in_dim.12
  27.3 11.8 %all-to-all-start = ((bf16[16,224,128]{2,1,0:T(8,128)(2,1)}), bf16[16,224,128]{2,1,0:T(8,128)(2,1)S(1)}, u32[]{:S(2)}, u32[]{:S(2)}) async-start(bf16[16,224,128]{2,1,0:T(8,128)(2,1)} %broadcast_in_dim.12), calls=%async_computation | async-start | bytes 1835008 | tf_op jit(solution)/shard_map/all_to_all | solution.py:290
  39.1 0.1 copy.17.own
  39.2 0.1 pad_add_fusion.pos
  39.3 23.3 %all-to-all-done.kv = bf16[16,224,128]{2,1,0:T(8,128)(2,1)S(1)} async-done(((bf16[16,224,128]{2,1,0:T(8,128)(2,1)}), bf16[16,224,128]{2,1,0:T(8,128)(2,1)S(1)}, u32[]{:S(2)}, u32[]{:S(2)}) %all-to-all-start) | async-done | bytes 917536 | tf_op jit(solution)/shard_map/all_to_all | solution.py:290
  62.6 31.3 %attention.1 = bf16[4,72,768]{2,1,0:T(8,128)(2,1)S(1)} custom-call(s32[3]{0:T(128)S(1)} %pad_add_fusion.pos, bf16[16,224,128]{2,1,0:T(8,128)(2,1)S(1)} %all-to-all-done.kv, bf16[4,192,256]{2,1,0:T(8,128)(2,1)S(1)} %all-to-all-done.1.q, f32[192,4]{1,0:T(8,128)S(1)} %copy.17.own), custom_call_target="tpu_custom_call" | custom-call | flops 12000000000 | bytes 4000000 | tf_op jit(solution)/shard_map/attention/pallas_call | solution.py:177
  93.9 20.7 %all_to_all.25.parts = bf16[4,72,768]{2,1,0:T(8,128)(2,1)S(1)} all-to-all(bf16[4,72,768]{2,1,0:T(8,128)(2,1)S(1)} %attention.1), channel_id=1, replica_groups=mesh['zh'=2,'zl'=4,'y'=8,'x'=4,'c'=2] {'zl'}, dimensions={0} | all-to-all | bytes 884736 | tf_op jit(solution)/shard_map/all_to_all | solution.py:327
  114.7 0.6 merge.1
  115.3 20.9 %all_to_all.26 = bf16[8,24,2048]{2,1,0:T(8,128)(2,1)S(1)} all-to-all(bf16[8,24,2048]{2,1,0:T(8,128)(2,1)S(1)} %bitcast.10), channel_id=1, replica_groups=mesh['zh'=2,'zl'=4,'y'=8,'x'=4,'c'=2] {'x','c'}, dimensions={0} | all-to-all | bytes 1572864 | tf_op jit(solution)/shard_map/all_to_all | solution.py:296
  136.3 0.1 convert_reduce_fusion.1
  136.4 0.1 multiply_reduce_fusion.2
  136.5 0.2 multiply_reduce_fusion.1
  136.8 0.1 multiply_convert_fusion
  136.9 13.4 %all_gather.6.rows = bf16[192,2048]{1,0:T(8,128)(2,1)S(1)} all-gather(bf16[24,2048]{1,0:T(8,128)(2,1)S(1)} %multiply_convert_fusion), channel_id=1, replica_groups=mesh['zh'=2,'zl'=4,'y'=8,'x'=4,'c'=2] {'x','c'}, dimensions={0}, use_global_device_ids=true | all-gather | bytes 884736 | tf_op jit(solution)/shard_map/all_gather | solution.py:331
  150.3 3.5 %copy-done = bf16[2048,2176]{1,0:T(8,128)(2,1)S(1)} copy-done((bf16[2048,2176]{1,0:T(8,128)(2,1)S(1)}, bf16[2048,2176]{1,0:T(8,128)(2,1)}, u32[]{:S(2)}) %copy-start) | copy-done | bytes 8912920
  153.8 4.4 %ffn.1 = bf16[192,2048]{1,0:T(8,128)(2,1)S(1)} custom-call(bf16[192,2048]{1,0:T(8,128)(2,1)S(1)} %all_gather.6.rows, bf16[2048,2176]{1,0:T(8,128)(2,1)S(1)} %copy-done), custom_call_target="tpu_custom_call" | custom-call | flops 1700000000 | bytes 10000000 | tf_op jit(solution)/shard_map/ffn/pallas_call | solution.py:271
  158.2 15.7 %all_to_all.27 = bf16[8,24,2048]{2,1,0:T(8,128)(2,1)S(1)} all-to-all(bf16[8,24,2048]{2,1,0:T(8,128)(2,1)S(1)} %bitcast.9), channel_id=1, replica_groups=mesh['zh'=2,'zl'=4,'y'=8,'x'=4,'c'=2] {'x','c'}, dimensions={0} | all-to-all | bytes 1572864 | tf_op jit(solution)/shard_map/all_to_all | solution.py:296
  173.9 0.1 convert_reduce_fusion
  174.0 0.1 multiply_reduce_fusion
  174.2 0.8 add_convert_fusion
  (32 shorter events, 0.2 us)
Async XLA Ops:
  6.5 8.0 %copy-start.4 = (bf16[192,64]{0,1:T(8,128)(2,1)S(1)}, bf16[192,64]{0,1:T(8,128)(2,1)}, u32[]{:S(2)}) copy-start(bf16[192,64]{0,1:T(8,128)(2,1)} %param.15) | copy-start | bytes 73732
  6.5 9.4 %copy-start.7 = (f32[192,4]{0,1:T(4,128)S(1)}, f32[192,4]{0,1:T(4,128)}, u32[]{:S(2)}) copy-start(f32[192,4]{0,1:T(4,128)} %param.17) | copy-start | bytes 9220
  6.5 9.8 %copy-start.6 = (bf16[192,64]{0,1:T(8,128)(2,1)S(1)}, bf16[192,64]{0,1:T(8,128)(2,1)}, u32[]{:S(2)}) copy-start(bf16[192,64]{0,1:T(8,128)(2,1)} %param.16) | copy-start | bytes 73732
  6.5 143.7 %all-gather.2.cloned.1.call-start = ((), (), s32[]{:S(2)}) async-start(), calls=%async_computation.5 | async-start | bytes 9052160 | tf_op jit(solution)/shard_map/all_gather | solution.py:322
  9.9 16.2 %all-to-all-start.1 = ((bf16[4,192,256]{2,1,0:T(8,128)(2,1)}), bf16[4,192,256]{2,1,0:T(8,128)(2,1)S(1)}, u32[]{:S(2)}, u32[]{:S(2)}) async-start(bf16[4,192,256]{2,1,0:T(8,128)(2,1)} %broadcast_in_dim.13), calls=%async_computation.1 | async-start | bytes 786432 | tf_op jit(solution)/shard_map/all_to_all | solution.py:290
  27.3 35.3 %all-to-all-start = ((bf16[16,224,128]{2,1,0:T(8,128)(2,1)}), bf16[16,224,128]{2,1,0:T(8,128)(2,1)S(1)}, u32[]{:S(2)}, u32[]{:S(2)}) async-start(bf16[16,224,128]{2,1,0:T(8,128)(2,1)} %broadcast_in_dim.12), calls=%async_computation | async-start | bytes 1835008 | tf_op jit(solution)/shard_map/all_to_all | solution.py:290
  39.3 75.4 %copy-start.2 = (bf16[192,256]{1,0:T(8,128)(2,1)S(1)}, bf16[192,256]{1,0:T(8,128)(2,1)}, u32[]{:S(2)}) copy-start(bf16[192,256]{1,0:T(8,128)(2,1)} %gates.1) | copy-start | bytes 294916
  62.6 52.0 %copy-start.1 = (bf16[256,2048]{1,0:T(8,128)(2,1)S(1)}, bf16[256,2048]{1,0:T(8,128)(2,1)}, u32[]{:S(2)}) copy-start(bf16[256,2048]{1,0:T(8,128)(2,1)} %weight.1) | copy-start | bytes 3145732
  115.3 21.2 %copy-start.3 = (bf16[24,2048]{1,0:T(8,128)(2,1)S(1)}, bf16[24,2048]{1,0:T(8,128)(2,1)}, u32[]{:S(2)}) copy-start(bf16[24,2048]{1,0:T(8,128)(2,1)} %param.13) | copy-start | bytes 294916
  115.3 21.2 %copy-start.5 = (f32[2048]{0:T(1024)S(1)}, f32[2048]{0:T(1024)}, u32[]{:S(2)}) copy-start(f32[2048]{0:T(1024)} %param.20) | copy-start | bytes 24580
  115.3 21.4 %copy-start.9 = (f32[2048]{0:T(1024)S(1)}, f32[2048]{0:T(1024)}, u32[]{:S(2)}) copy-start(f32[2048]{0:T(1024)} %param.21) | copy-start | bytes 24580
  150.3 3.5 %copy-start = (bf16[2048,2176]{1,0:T(8,128)(2,1)S(1)}, bf16[2048,2176]{1,0:T(8,128)(2,1)}, u32[]{:S(2)}) copy-start(bf16[2048,2176]{1,0:T(8,128)(2,1)} %all-gather.2.cloned.1.call-done.weights) | copy-start | bytes 26738692
  158.2 16.0 %copy-start.8 = (f32[2048]{0:T(1024)S(1)}, f32[2048]{0:T(1024)}, u32[]{:S(2)}) copy-start(f32[2048]{0:T(1024)} %param.22) | copy-start | bytes 24580
Sparse Core Ops, SparseCore 0:
  10.3 120.5 all-gather.1

commit v2 on v1

--- a/solution.py
+++ b/solution.py
@@ -11,10 +11,11 @@
 ROWS = 192
 QG = 4
 ZH = 8 // QG
+ZGRID = ((0, 3, 4, 7), (6, 5, 2, 1))
 YS = 8
 NB = ZH * YS
-TILE = 384
-CH = 256
+TILE = 1536
+CH = 768
 QR = ROWS * HL
 KP = 224
 OUTR = 72
@@ -25,7 +26,7 @@
 LOW = -1e30
 GAP = 56.0
 
-SP = ("zh", "zl", "y")
+SP = ("z", "y")
 TP = ("x", "c")
 F32 = jnp.float32
 BF16 = jnp.bfloat16
@@ -58,10 +59,22 @@
     return jnp.concatenate([jnp.concatenate([keys, values], axis=1), left, right], axis=0)
 
 
-def attention_kernel(pos, kv, q, own, out, kc, vt, qc, acc, ls, ms):
+def grid_z(zh, zl):
+    z = jnp.int32(0)
+    for a in range(ZH):
+        for b in range(QG):
+            z = jnp.where((zh == a) & (zl == b), ZGRID[a][b], z)
+    return z
+
+
+def attention_kernel(pos, kv, q, own, out, kc, vt, qt, acc, ls, ms):
     zh = pos[0]
     zl = pos[1]
     y = pos[2]
+    mine = grid_z(zh, zl)
+    lower = jnp.minimum(grid_z(0, zl), grid_z(1, zl))
+    upper = jnp.maximum(grid_z(0, zl), grid_z(1, zl))
+    low_at = jnp.where(grid_z(0, zl) == lower, 0, 1)
     kc[:, 128:256] = jnp.zeros((NB * ROWS, 128), BF16)
     kmax = jnp.zeros((1, 1), F32)
     for b in range(NB):
@@ -74,25 +87,35 @@
         kmax = jnp.maximum(kmax, left[15:16, 0:1])
     for i in range(NB * ROWS // TILE):
         vt[i] = kc[i * TILE : (i + 1) * TILE, 0:128].T[64:128]
-    lane = lax.broadcasted_iota(jnp.int32, (ROWS, 128), 1)
+    head = jnp.zeros((16, QR), jnp.int32)
+    col = lax.broadcasted_iota(jnp.int32, (16, QR), 1)
+    for h in range(1, HL):
+        head = head + jnp.where(col >= h * ROWS, 1, 0)
+    line = lax.broadcasted_iota(jnp.int32, (16, QR), 0)
+    chosen = jnp.where((line < 3 * HL) & (line % HL == head), -1.0, 0.0)
     qmax = jnp.zeros((1, 1), F32)
+    owned = jnp.concatenate([own[h : h + 1, :] for h in range(HL)], axis=1)
     for j in range(QG):
-        block = jnp.where(j > zl, zh * YS + YS - 1, jnp.maximum(zh * YS - 1, 0))
-        ends = kv[block, 208:224, :].astype(F32)[:, 63:64]
+        asked = grid_z(zh, j)
+        last = jnp.where(asked > upper, 1 - low_at, low_at)
+        ends = kv[last * YS + YS - 1, 208:224, :].astype(F32)[:, 63:64]
+        turned = (q[j].astype(F32) * 0.125).T
+        turned = jnp.concatenate([turned[h * HD : (h + 1) * HD] for h in range(HL)], axis=1)
+        norm = jnp.sqrt(jnp.sum(turned * turned, axis=0, keepdims=True))
+        qmax = jnp.maximum(qmax, jnp.max(norm, axis=1, keepdims=True))
+        ref = jnp.zeros((1, QR), F32)
         for h in range(HL):
             end = ends[h : h + 1] + ends[4 + h : 5 + h] + ends[8 + h : 9 + h]
-            ref = jnp.where(j == zl, own[:, h : h + 1], jnp.broadcast_to(end, (ROWS, 1)))
-            qh = q[j, :, h * HD : (h + 1) * HD].astype(F32) * 0.125
-            norm = jnp.sqrt(jnp.sum(qh * qh, axis=1, keepdims=True))
-            qmax = jnp.maximum(qmax, jnp.max(norm, axis=0, keepdims=True))
-            one, two, three = kernel_pieces(ref - norm * kmax)
-            side = jnp.where((lane == h) | (lane == 4 + h) | (lane == 8 + h), -1.0, 0.0)
-            side = jnp.where(lane == 12, one, side)
-            side = jnp.where(lane == 13, two, side)
-            side = jnp.where(lane == 14, three, side)
-            at = slice(h * ROWS, (h + 1) * ROWS)
-            qc[j, at, 0:128] = jnp.concatenate([qh, jnp.zeros((ROWS, HD), F32)], axis=1).astype(BF16)
-            qc[j, at, 128:256] = side.astype(BF16)
+            ref = jnp.where(head[0:1] == h, end, ref)
+        ref = jnp.where(j == zl, owned, ref)
+        one, two, three = kernel_pieces(ref - norm * kmax)
+        side = jnp.where(line == 12, one, chosen)
+        side = jnp.where(line == 13, two, side)
+        side = jnp.where(line == 14, three, side)
+        qt[j, 0:HD, :] = turned.astype(BF16)
+        qt[j, HD:128, :] = jnp.zeros((128 - HD, QR), BF16)
+        qt[j, 128:144, :] = side.astype(BF16)
+        qt[j, 144:256, :] = jnp.zeros((112, QR), BF16)
     acc[...] = jnp.zeros(acc.shape, F32)
     ls[...] = jnp.zeros(ls.shape, F32)
     ms[...] = jnp.full(ms.shape, LOW, F32)
@@ -105,7 +128,7 @@
             vv = vt[tile]
             for n in range(QR // CH):
                 cols = slice(n * CH, (n + 1) * CH)
-                s = lax.dot_general(kk, qc[j, cols, :], NT, preferred_element_type=F32)
+                s = jnp.dot(kk, qt[j, :, cols], preferred_element_type=F32)
                 if masked:
                     col = n * CH + lax.broadcasted_iota(jnp.int32, (TILE, CH), 1)
                     for h in range(1, HL):
@@ -134,8 +157,10 @@
         def one(u, none):
             j = u // ZH
             hz = u % ZH
-            edge = (hz == zh) & (j == zl)
-            whole = (hz < zh) | ((hz == zh) & (j > zl))
+            asked = grid_z(zh, j)
+            held = grid_z(hz, zl)
+            edge = asked == held
+            whole = asked > held
 
             @pl.when(whole)
             def _():
@@ -162,7 +187,7 @@
     pick = jnp.where((spot >= 140) & (spot <= 142), 1.0, 0.0).astype(BF16)
     line = lax.broadcasted_iota(jnp.int32, (8, QR), 0)
     for j in range(QG):
-        shift = lax.dot_general(pick, qc[j], NT, preferred_element_type=F32)[0:1]
+        shift = jnp.dot(pick, qt[j], preferred_element_type=F32)[0:1]
         total = jnp.sum(ls[j], axis=0, keepdims=True)
         top = jnp.where(total > 0.0, ms[j, 0:1, :] - shift, LOW)
         stats = jnp.zeros((8, QR), F32)
@@ -182,7 +207,7 @@
         scratch_shapes=[
             pltpu.VMEM((NB * ROWS, 256), BF16),
             pltpu.VMEM((NB * ROWS // TILE, HD, TILE), BF16),
-            pltpu.VMEM((QG, QR, 256), BF16),
+            pltpu.VMEM((QG, 256, QR), BF16),
             pltpu.VMEM((QG, HD, QR), F32),
             pltpu.VMEM((QG, 8, QR), F32),
             pltpu.VMEM((QG, 8, QR), F32),
@@ -190,7 +215,7 @@
         compiler_params=pltpu.CompilerParams(vmem_limit_bytes=48 * 1024 * 1024),
         cost_estimate=pl.CostEstimate(flops=12_000_000_000, bytes_accessed=4_000_000, transcendentals=9_000_000),
         name="attention",
-    )(pos, kv, q, own)
+    )(pos, kv, q, own.T)
 
 
 def merge_kernel(parts, gates, weight, out):
@@ -271,7 +296,7 @@
     return pl.pallas_call(
         ffn_kernel,
         out_shape=jax.ShapeDtypeStruct((ROWS, wide), BF16),
-        in_specs=[pl.BlockSpec(memory_space=pltpu.VMEM), pl.BlockSpec(memory_space=pl.ANY)],
+        in_specs=[pl.BlockSpec(memory_space=pltpu.VMEM), pl.BlockSpec(memory_space=pltpu.HBM)],
         out_specs=pl.BlockSpec(memory_space=pltpu.VMEM),
         scratch_shapes=[
             pltpu.VMEM((wide, WC), BF16),
@@ -279,15 +304,15 @@
             pltpu.VMEM((ROWS, WC - GU), BF16),
             pltpu.SemaphoreType.DMA((2 * (wide // FC),)),
         ],
-        compiler_params=pltpu.CompilerParams(vmem_limit_bytes=40 * 1024 * 1024),
+        compiler_params=pltpu.CompilerParams(vmem_limit_bytes=60 * 1024 * 1024),
         cost_estimate=pl.CostEstimate(flops=1_700_000_000, bytes_accessed=10_000_000, transcendentals=140_000),
         name="ffn",
     )(rows, weights)
 
 
-def copies(value, axis):
-    peers = lax.axis_size(axis)
-    return lax.all_to_all(jnp.broadcast_to(value[None], (peers, *value.shape)), axis, 0, 0, tiled=True)
+def copies(value, axis, groups):
+    sent = jnp.broadcast_to(value[None], (len(groups[0]), *value.shape))
+    return lax.all_to_all(sent, axis, 0, 0, axis_index_groups=groups, tiled=True)
 
 
 def sum_at_owner(value):
@@ -320,11 +345,16 @@
     pad = jnp.zeros((gate_weight.shape[0], WC - GU - FFL), BF16)
     packed = jnp.concatenate([gate_weight, up_weight, down_weight.T, pad], axis=1)
     weights = lax.all_gather(packed, SP, axis=0, tiled=True)
-    kv = copies(key_payload(keys, values, log_gates), ("zh", "y"))
-    q_all = copies(queries, "zl")
-    pos = jnp.stack([lax.axis_index("zh"), lax.axis_index("zl"), lax.axis_index("y")]).astype(jnp.int32)
+    rows_of = [list(row) for row in ZGRID]
+    columns = [[ZGRID[a][b] * YS + y for a in range(ZH) for y in range(YS)] for b in range(QG)]
+    kv = copies(key_payload(keys, values, log_gates), SP, columns)
+    q_all = copies(queries, "z", rows_of)
+    z = lax.axis_index("z")
+    zh = sum(jnp.where(z == ZGRID[a][b], a, 0) for a in range(ZH) for b in range(QG))
+    zl = sum(jnp.where(z == ZGRID[a][b], b, 0) for a in range(ZH) for b in range(QG))
+    pos = jnp.stack([zh, zl, lax.axis_index("y")]).astype(jnp.int32)
     parts = attention(pos, kv, q_all, log_gates)
-    parts = lax.all_to_all(parts, "zl", 0, 0, tiled=True)
+    parts = lax.all_to_all(parts, "z", 0, 0, axis_index_groups=rows_of, tiled=True)
     projected = sum_at_owner(merge(parts, out_gate, out_weight))
     mixed = resid.astype(F32) + rms_scale(projected, post_gain)
     normed = rms_scale(mixed, pre_gain).astype(BF16)
@@ -334,7 +364,7 @@
 
 
 def solution(mesh):
-    split = Mesh(mesh.devices.reshape(ZH, QG, YS, 4, 2), ("zh", "zl", "y", "x", "c"))
+    split = Mesh(mesh.devices.reshape(8, YS, 4, 2), ("z", "y", "x", "c"))
     in_specs = (
         P((*SP, *TP), None),
         P(SP, TP),

time: 183 us -> 172 us (0.940)
  the two profiles are of different devices: /device:TPU:304 before, /device:TPU:1 now
where the time goes in v2:
time: 172 us
  blocking collectives  76.9 us (45%)
  waiting for transfers between devices  38.4 us (22%)
  starting transfers between devices  19 us (11%)
  Pallas kernels  16.4 us (10%)
  between operations  14.3 us (8%)
  local copies, waits for them, and re-layouts  5 us (3%)
  other arithmetic  2.49 us (1%)
    all_to_all x2, blocking collectives, sum_at_owner(): arrived = lax.all_to_all(blocks, TP, 0, 0, tiled=True)  45.2 us
    all_to_all x2, waiting for transfers between devices, copies(): lax.all_to_all(sent, axis, 0, 0, axis_index_groups=groups, tiled=True)  38.4 us
    all_to_all x2, starting transfers between devices, copies(): lax.all_to_all(sent, axis, 0, 0, axis_index_groups=groups, tiled=True)  19 us
    all_to_all x1, blocking collectives, shards(): lax.all_to_all(parts, 'z', 0, 0, axis_index_groups=rows_of, tiled=True)  16.3 us
    all_gather x1, blocking collectives, shards(): normed_all = lax.all_gather(normed, TP, axis=0, tiled=True)  15.5 us
    pallas_call x1, Pallas kernels, attention(): pl.pallas_call(attention_kernel, out_shape=jax.ShapeDtypeStruct((QG, OUTR...  8.68 us
    pallas_call x1, Pallas kernels, ffn(): pl.pallas_call(ffn_kernel, out_shape=jax.ShapeDtypeStruct((ROWS, wide), B...  7.11 us
  transfers between devices with their start and end apart: 3, of which 2 were waited for; matrix products, arithmetic and copies ran while one was open for 3% of the time, Pallas kernels for 5%

profile of v2, /device:TPU:1, one launch (start us, length us, event | category | flops | bytes accessed | tf_op | source)
XLA Modules:
  0.0 172.4 jit_solution(10189276223562719961)
XLA Ops:
  6.6 1.6 concatenate.21
  8.2 0.0 all-gather.2.cloned.1.call-update
  8.2 1.7 broadcast_in_dim.13
  9.9 10.8 %all-to-all-start.1 = ((bf16[4,192,256]{2,1,0:T(8,128)(2,1)}), bf16[4,192,256]{2,1,0:T(8,128)(2,1)S(1)}, u32[]{:S(2)}, u32[]{:S(2)}) async-start(bf16[4,192,256]{2,1,0:T(8,128)(2,1)} %broadcast_in_dim.13), calls=%async_computation.1 | async-start | bytes 786432 | tf_op jit(solution)/shard_map/all_to_all | solution.py:315
  20.8 0.6 reduce_max.9
  22.1 0.1 pad.11.clone
  22.2 0.1 pad.10.clone
  22.3 0.1 maximum_maximum_fusion
  22.4 0.1 copy.14
  22.5 0.1 copy.17
  22.6 0.1 fusion.1
  22.7 0.1 copy.16
  22.8 10.7 %all-to-all-done.1.q = bf16[4,192,256]{2,1,0:T(8,128)(2,1)S(1)} async-done(((bf16[4,192,256]{2,1,0:T(8,128)(2,1)}), bf16[4,192,256]{2,1,0:T(8,128)(2,1)S(1)}, u32[]{:S(2)}, u32[]{:S(2)}) %all-to-all-start.1) | async-done | bytes 393248 | tf_op jit(solution)/shard_map/all_to_all | solution.py:315
  33.5 1.1 broadcast_in_dim.12
  34.6 8.1 %all-to-all-start = ((bf16[16,224,128]{2,1,0:T(8,128)(2,1)}), bf16[16,224,128]{2,1,0:T(8,128)(2,1)S(1)}, u32[]{:S(2)}, u32[]{:S(2)}) async-start(bf16[16,224,128]{2,1,0:T(8,128)(2,1)} %broadcast_in_dim.12), calls=%async_computation | async-start | bytes 1835008 | tf_op jit(solution)/shard_map/all_to_all | solution.py:315
  42.8 0.1 pad_add_fusion.pos
  42.8 27.7 %all-to-all-done.kv = bf16[16,224,128]{2,1,0:T(8,128)(2,1)S(1)} async-done(((bf16[16,224,128]{2,1,0:T(8,128)(2,1)}), bf16[16,224,128]{2,1,0:T(8,128)(2,1)S(1)}, u32[]{:S(2)}, u32[]{:S(2)}) %all-to-all-start) | async-done | bytes 917536 | tf_op jit(solution)/shard_map/all_to_all | solution.py:315
  70.5 8.7 %attention.1 = bf16[4,72,768]{2,1,0:T(8,128)(2,1)S(1)} custom-call(s32[3]{0:T(128)S(1)} %pad_add_fusion.pos, bf16[16,224,128]{2,1,0:T(8,128)(2,1)S(1)} %all-to-all-done.kv, bf16[4,192,256]{2,1,0:T(8,128)(2,1)S(1)} %all-to-all-done.1.q, f32[4,192]{1,0:T(4,128)S(1)} %bitcast.11), custom_call_target="tpu_custom_call" | custom-call | flops 12000000000 | bytes 4000000 | tf_op jit(solution)/shard_map/attention/pallas_call | solution.py:202
  79.2 16.3 %all_to_all.25.parts = bf16[4,72,768]{2,1,0:T(8,128)(2,1)S(1)} all-to-all(bf16[4,72,768]{2,1,0:T(8,128)(2,1)S(1)} %attention.1), channel_id=1, replica_groups={{0,192,256,448},{384,320,128,64},{1,193,257,449},{385,321,129,65},{2,19..., dimensions={0} | all-to-all | bytes 884736 | tf_op jit(solution)/shard_map/all_to_all | solution.py:357
  95.5 0.6 merge.1
  96.1 0.0 copy-start.8
  96.1 29.4 %all_to_all.26 = bf16[8,24,2048]{2,1,0:T(8,128)(2,1)S(1)} all-to-all(bf16[8,24,2048]{2,1,0:T(8,128)(2,1)S(1)} %bitcast.10), channel_id=1, replica_groups=mesh['z'=8,'y'=8,'x'=4,'c'=2] {'x','c'}, dimensions={0} | all-to-all | bytes 1572864 | tf_op jit(solution)/shard_map/all_to_all | solution.py:321
  125.6 0.1 convert_reduce_fusion.1
  125.7 0.1 multiply_reduce_fusion.2
  125.8 0.2 multiply_reduce_fusion.1
  126.1 0.1 multiply_convert_fusion
  126.2 15.5 %all_gather.6.rows = bf16[192,2048]{1,0:T(8,128)(2,1)} all-gather(bf16[24,2048]{1,0:T(8,128)(2,1)S(1)} %multiply_convert_fusion), channel_id=1, replica_groups=mesh['z'=8,'y'=8,'x'=4,'c'=2] {'x','c'}, dimensions={0}, use_global_device_ids=true | all-gather | bytes 884736 | tf_op jit(solution)/shard_map/all_gather | solution.py:361
  141.6 7.1 %ffn.1 = bf16[192,2048]{1,0:T(8,128)(2,1)} custom-call(bf16[192,2048]{1,0:T(8,128)(2,1)} %all_gather.6.rows, bf16[2048,2176]{1,0:T(8,128)(2,1)} %all-gather.2.cloned.1.call-done.weights), custom_call_target="tpu_custom_call" | custom-call | flops 1700000000 | bytes 10000000 | tf_op jit(solution)/shard_map/ffn/pallas_call | solution.py:296
  148.8 15.7 %all_to_all.27 = bf16[8,24,2048]{2,1,0:T(8,128)(2,1)S(1)} all-to-all(bf16[8,24,2048]{2,1,0:T(8,128)(2,1)} %bitcast.12), channel_id=1, replica_groups=mesh['z'=8,'y'=8,'x'=4,'c'=2] {'x','c'}, dimensions={0} | all-to-all | bytes 1572864 | tf_op jit(solution)/shard_map/all_to_all | solution.py:321
  164.5 0.1 convert_reduce_fusion
  164.6 0.1 multiply_reduce_fusion
  164.8 0.8 add_convert_fusion
  (29 shorter events, 0.1 us)
Async XLA Ops:
  6.5 14.2 %copy-start.4 = (bf16[192,64]{0,1:T(8,128)(2,1)S(1)}, bf16[192,64]{0,1:T(8,128)(2,1)}, u32[]{:S(2)}) copy-start(bf16[192,64]{0,1:T(8,128)(2,1)} %param.15) | copy-start | bytes 73732
  6.5 15.7 %copy-start.2 = (f32[192,4]{0,1:T(4,128)S(1)}, f32[192,4]{0,1:T(4,128)}, u32[]{:S(2)}) copy-start(f32[192,4]{0,1:T(4,128)} %param.17) | copy-start | bytes 9220
  6.5 16.1 %copy-start.6 = (bf16[192,64]{0,1:T(8,128)(2,1)S(1)}, bf16[192,64]{0,1:T(8,128)(2,1)}, u32[]{:S(2)}) copy-start(bf16[192,64]{0,1:T(8,128)(2,1)} %param.16) | copy-start | bytes 73732
  6.5 135.1 %all-gather.2.cloned.1.call-start = ((), (), s32[]{:S(2)}) async-start(), calls=%async_computation.5 | async-start | bytes 9052160 | tf_op jit(solution)/shard_map/all_gather | solution.py:347
  9.9 23.6 %all-to-all-start.1 = ((bf16[4,192,256]{2,1,0:T(8,128)(2,1)}), bf16[4,192,256]{2,1,0:T(8,128)(2,1)S(1)}, u32[]{:S(2)}, u32[]{:S(2)}) async-start(bf16[4,192,256]{2,1,0:T(8,128)(2,1)} %broadcast_in_dim.13), calls=%async_computation.1 | async-start | bytes 786432 | tf_op jit(solution)/shard_map/all_to_all | solution.py:315
  34.6 35.9 %all-to-all-start = ((bf16[16,224,128]{2,1,0:T(8,128)(2,1)}), bf16[16,224,128]{2,1,0:T(8,128)(2,1)S(1)}, u32[]{:S(2)}, u32[]{:S(2)}) async-start(bf16[16,224,128]{2,1,0:T(8,128)(2,1)} %broadcast_in_dim.12), calls=%async_computation | async-start | bytes 1835008 | tf_op jit(solution)/shard_map/all_to_all | solution.py:315
  70.5 25.0 %copy-start = (bf16[256,2048]{1,0:T(8,128)(2,1)S(1)}, bf16[256,2048]{1,0:T(8,128)(2,1)}, u32[]{:S(2)}) copy-start(bf16[256,2048]{1,0:T(8,128)(2,1)} %weight.1) | copy-start | bytes 3145732
  70.5 25.0 %copy-start.1 = (bf16[192,256]{1,0:T(8,128)(2,1)S(1)}, bf16[192,256]{1,0:T(8,128)(2,1)}, u32[]{:S(2)}) copy-start(bf16[192,256]{1,0:T(8,128)(2,1)} %gates.1) | copy-start | bytes 294916
  96.1 29.7 %copy-start.3 = (bf16[24,2048]{1,0:T(8,128)(2,1)S(1)}, bf16[24,2048]{1,0:T(8,128)(2,1)}, u32[]{:S(2)}) copy-start(bf16[24,2048]{1,0:T(8,128)(2,1)} %param.13) | copy-start | bytes 294916
  96.1 29.7 %copy-start.5 = (f32[2048]{0:T(1024)S(1)}, f32[2048]{0:T(1024)}, u32[]{:S(2)}) copy-start(f32[2048]{0:T(1024)} %param.20) | copy-start | bytes 24580
  96.1 29.9 %copy-start.8 = (f32[2048]{0:T(1024)S(1)}, f32[2048]{0:T(1024)}, u32[]{:S(2)}) copy-start(f32[2048]{0:T(1024)} %param.21) | copy-start | bytes 24580
  148.8 16.0 %copy-start.7 = (f32[2048]{0:T(1024)S(1)}, f32[2048]{0:T(1024)}, u32[]{:S(2)}) copy-start(f32[2048]{0:T(1024)} %param.22) | copy-start | bytes 24580
Sparse Core Ops, SparseCore 0:
  10.3 126.2 all-gather.1

commit v3 on v2

--- a/solution.py
+++ b/solution.py
@@ -67,7 +67,9 @@
     return z
 
 
-def attention_kernel(pos, kv, q, own, out, kc, vt, qt, acc, ls, ms):
+def attention_kernel(pos, kv, q0, q1, q2, q3, own, o0, o1, o2, o3, kc, vt, qt, acc, ls, ms):
+    q = (q0, q1, q2, q3)
+    out = (o0, o1, o2, o3)
     zh = pos[0]
     zl = pos[1]
     y = pos[2]
@@ -96,10 +98,10 @@
     qmax = jnp.zeros((1, 1), F32)
     owned = jnp.concatenate([own[h : h + 1, :] for h in range(HL)], axis=1)
     for j in range(QG):
-        asked = grid_z(zh, j)
+        asked = grid_z(zh, (zl + QG - j) % QG)
         last = jnp.where(asked > upper, 1 - low_at, low_at)
         ends = kv[last * YS + YS - 1, 208:224, :].astype(F32)[:, 63:64]
-        turned = (q[j].astype(F32) * 0.125).T
+        turned = (q[j][...].astype(F32) * 0.125).T
         turned = jnp.concatenate([turned[h * HD : (h + 1) * HD] for h in range(HL)], axis=1)
         norm = jnp.sqrt(jnp.sum(turned * turned, axis=0, keepdims=True))
         qmax = jnp.maximum(qmax, jnp.max(norm, axis=1, keepdims=True))
@@ -107,7 +109,7 @@
         for h in range(HL):
             end = ends[h : h + 1] + ends[4 + h : 5 + h] + ends[8 + h : 9 + h]
             ref = jnp.where(head[0:1] == h, end, ref)
-        ref = jnp.where(j == zl, owned, ref)
+        ref = owned if j == 0 else ref
         one, two, three = kernel_pieces(ref - norm * kmax)
         side = jnp.where(line == 12, one, chosen)
         side = jnp.where(line == 13, two, side)
@@ -157,7 +159,7 @@
         def one(u, none):
             j = u // ZH
             hz = u % ZH
-            asked = grid_z(zh, j)
+            asked = grid_z(zh, (zl + QG - j) % QG)
             held = grid_z(hz, zl)
             edge = asked == held
             whole = asked > held
@@ -193,17 +195,17 @@
         stats = jnp.zeros((8, QR), F32)
         for k, part in enumerate(kernel_pieces(total) + kernel_pieces(top)):
             stats = jnp.where(line == k, part, stats)
-        out[j, 0:HD, :] = acc[j].astype(BF16)
-        out[j, HD:OUTR, :] = stats.astype(BF16)
-
-
-def attention(pos, kv, q, own):
+        out[j][0:HD, :] = acc[j].astype(BF16)
+        out[j][HD:OUTR, :] = stats.astype(BF16)
+
+
+def attention(pos, kv, *rest):
     vmem = pl.BlockSpec(memory_space=pltpu.VMEM)
     return pl.pallas_call(
         attention_kernel,
-        out_shape=jax.ShapeDtypeStruct((QG, OUTR, QR), BF16),
-        in_specs=[pl.BlockSpec(memory_space=pltpu.SMEM), vmem, vmem, vmem],
-        out_specs=vmem,
+        out_shape=[jax.ShapeDtypeStruct((OUTR, QR), BF16)] * QG,
+        in_specs=[pl.BlockSpec(memory_space=pltpu.SMEM)] + [vmem] * (QG + 2),
+        out_specs=[vmem] * QG,
         scratch_shapes=[
             pltpu.VMEM((NB * ROWS, 256), BF16),
             pltpu.VMEM((NB * ROWS // TILE, HD, TILE), BF16),
@@ -215,14 +217,15 @@
         compiler_params=pltpu.CompilerParams(vmem_limit_bytes=48 * 1024 * 1024),
         cost_estimate=pl.CostEstimate(flops=12_000_000_000, bytes_accessed=4_000_000, transcendentals=9_000_000),
         name="attention",
-    )(pos, kv, q, own.T)
-
-
-def merge_kernel(parts, gates, weight, out):
+    )(pos, kv, *rest)
+
+
+def merge_kernel(p0, p1, p2, p3, gates, weight, out):
+    parts = (p0, p1, p2, p3)
     tops = []
     sums = []
     for j in range(QG):
-        stats = parts[j, HD:OUTR, :].astype(F32)
+        stats = parts[j][HD:OUTR, :].astype(F32)
         sums.append(stats[0:1] + stats[1:2] + stats[2:3])
         tops.append(stats[3:4] + stats[4:5] + stats[5:6])
     top = tops[0]
@@ -233,7 +236,7 @@
     for j in range(QG):
         scale = jnp.exp(tops[j] - top)
         total = total + sums[j] * scale
-        mixed = mixed + parts[j, 0:HD, :].astype(F32) * scale
+        mixed = mixed + parts[j][0:HD, :].astype(F32) * scale
     rows = (mixed / total).T
     rows = jnp.concatenate([rows[h * ROWS : (h + 1) * ROWS] for h in range(HL)], axis=1)
     gated = (rows * jax.nn.sigmoid(gates[...].astype(F32))).astype(BF16)
@@ -247,10 +250,11 @@
         compiler_params=pltpu.CompilerParams(vmem_limit_bytes=32 * 1024 * 1024),
         cost_estimate=pl.CostEstimate(flops=400_000_000, bytes_accessed=2_000_000, transcendentals=50_000),
         name="merge",
-    )(parts, gates, weight)
-
-
-FC = 512
+    )(*parts, gates, weight)
+
+
+FC = 1024
+DEEP = 4
 
 
 def ffn_kernel(rows, weights, out, wv, acc, hid, sems):
@@ -264,12 +268,17 @@
         at = (pl.ds(k * FC, FC), pl.ds(GU, WC - GU))
         return pltpu.make_async_copy(weights.at[at], wv.at[at], sems.at[count + k])
 
+    moves = [first(k) for k in range(count)] + [second(k) for k in range(count)]
+    for k in range(DEEP):
+        moves[k].start()
+
+    def arrive(k):
+        moves[k].wait()
+        if k + DEEP < len(moves):
+            moves[k + DEEP].start()
+
     for k in range(count):
-        first(k).start()
-    for k in range(count):
-        second(k).start()
-    for k in range(count):
-        first(k).wait()
+        arrive(k)
         part = jnp.dot(
             rows[:, k * FC : (k + 1) * FC],
             wv[k * FC : (k + 1) * FC, 0:GU],
@@ -285,7 +294,7 @@
     hid[:, FFL:] = jnp.zeros((ROWS, WC - GU - FFL), BF16)
     hid[:, 0:FFL] = hidden.astype(BF16)
     for k in range(count):
-        second(k).wait()
+        arrive(count + k)
         out[:, k * FC : (k + 1) * FC] = lax.dot_general(
             hid[...], wv[k * FC : (k + 1) * FC, GU:WC], NT, preferred_element_type=F32
         ).astype(BF16)
@@ -342,19 +351,21 @@
     up_weight,
     down_weight,
 ):
+    def turn(r):
+        return [(row[i], row[(i + r) % QG]) for row in ZGRID for i in range(QG)]
+
     pad = jnp.zeros((gate_weight.shape[0], WC - GU - FFL), BF16)
     packed = jnp.concatenate([gate_weight, up_weight, down_weight.T, pad], axis=1)
     weights = lax.all_gather(packed, SP, axis=0, tiled=True)
-    rows_of = [list(row) for row in ZGRID]
     columns = [[ZGRID[a][b] * YS + y for a in range(ZH) for y in range(YS)] for b in range(QG)]
+    q_all = [queries] + [lax.ppermute(queries, "z", turn(r)) for r in range(1, QG)]
     kv = copies(key_payload(keys, values, log_gates), SP, columns)
-    q_all = copies(queries, "z", rows_of)
     z = lax.axis_index("z")
     zh = sum(jnp.where(z == ZGRID[a][b], a, 0) for a in range(ZH) for b in range(QG))
     zl = sum(jnp.where(z == ZGRID[a][b], b, 0) for a in range(ZH) for b in range(QG))
     pos = jnp.stack([zh, zl, lax.axis_index("y")]).astype(jnp.int32)
-    parts = attention(pos, kv, q_all, log_gates)
-    parts = lax.all_to_all(parts, "z", 0, 0, axis_index_groups=rows_of, tiled=True)
+    parts = attention(pos, kv, *q_all, log_gates.T)
+    parts = [parts[0]] + [lax.ppermute(parts[r], "z", turn(QG - r)) for r in range(1, QG)]
     projected = sum_at_owner(merge(parts, out_gate, out_weight))
     mixed = resid.astype(F32) + rms_scale(projected, post_gain)
     normed = rms_scale(mixed, pre_gain).astype(BF16)

time: 172 us -> 174 us (1.012)
  blocking collectives: 76.9 us -> 51.5 us
  starting transfers between devices: 19 us -> 34.5 us
  waiting for transfers between devices: 38.4 us -> 44 us
  Pallas kernels: 16.4 us -> 21.4 us
  other arithmetic: 2.49 us -> 4.72 us
    all_to_all x2 -> x1, waiting for transfers between devices: 38.4 us -> 0.01 us  [copies(): lax.all_to_all(sent, axis, 0, 0, axis_index_groups=groups, tiled=True)]
    ppermute x0 -> x6, waiting for transfers between devices: none -> 27.9 us  [the longest x3 22.1 us: shards(): lax.ppermute(queries, 'z', turn(r))]
    ppermute x0 -> x6, starting transfers between devices: none -> 18.3 us  [the longest x3 9.3 us: shards(): lax.ppermute(queries, 'z', turn(r))]
    all_to_all x1 -> x0, blocking collectives: 16.3 us -> none  [shards(): lax.all_to_all(parts, 'z', 0, 0, axis_index_groups=rows_of, tiled=True)]
    all_gather x1, waiting for transfers between devices: 0.01 us -> 16.1 us  [shards(): weights = lax.all_gather(packed, SP, axis=0, tiled=True)]
    all_to_all x2, blocking collectives: 45.2 us -> 36 us  [sum_at_owner(): arrived = lax.all_to_all(blocks, TP, 0, 0, tiled=True)]
    pallas_call x1, Pallas kernels: 8.68 us -> 13.8 us  [attention(): pl.pallas_call(attention_kernel, out_shape=[jax.ShapeDtypeStruct((OUTR, Q...]
    all_to_all x2 -> x1, starting transfers between devices: 19 us -> 16.2 us  [copies(): lax.all_to_all(sent, axis, 0, 0, axis_index_groups=groups, tiled=True)]
  transfers between devices with their start and end apart: 3 -> 8, of which waited for: 2 -> 4; matrix products, arithmetic and copies ran while one was open for 3% -> 3% of each run, Pallas kernels for 5% -> 8%
where the time goes in v3:
time: 174 us
  blocking collectives  51.5 us (30%)
  waiting for transfers between devices  44 us (25%)
  starting transfers between devices  34.5 us (20%)
  Pallas kernels  21.4 us (12%)
  between operations  14.3 us (8%)
  other arithmetic  4.72 us (3%)
  local copies, waits for them, and re-layouts  3.28 us (2%)
    all_to_all x2, blocking collectives, sum_at_owner(): arrived = lax.all_to_all(blocks, TP, 0, 0, tiled=True)  36 us
    ppermute x3, waiting for transfers between devices, shards(): lax.ppermute(queries, 'z', turn(r))  22.1 us
    all_to_all x1, starting transfers between devices, copies(): lax.all_to_all(sent, axis, 0, 0, axis_index_groups=groups, tiled=True)  16.2 us
    all_gather x1, waiting for transfers between devices, shards(): weights = lax.all_gather(packed, SP, axis=0, tiled=True)  16.1 us
    all_gather x1, blocking collectives, shards(): normed_all = lax.all_gather(normed, TP, axis=0, tiled=True)  15.5 us
    pallas_call x1, Pallas kernels, attention(): pl.pallas_call(attention_kernel, out_shape=[jax.ShapeDtypeStruct((OUTR, Q...  13.8 us
    ppermute x3, starting transfers between devices, shards(): lax.ppermute(queries, 'z', turn(r))  9.3 us
    ppermute x3, starting transfers between devices, shards(): lax.ppermute(parts[r], 'z', turn(QG - r))  9 us
  transfers between devices with their start and end apart: 8, of which 4 were waited for; matrix products, arithmetic and copies ran while one was open for 3% of the time, Pallas kernels for 8%

profile of v3, /device:TPU:1, one launch (start us, length us, event | category | flops | bytes accessed | tf_op | source)
XLA Modules:
  0.0 173.7 jit_solution(9925587854802604330)
XLA Ops:
  6.5 1.6 concatenate.21
  8.2 0.8 multiply_reduce_fusion.3
  9.0 0.6 reduce_max.9
  10.4 0.7 reduce-precision_convert_fusion.1
  11.2 0.1 copy.14
  11.5 0.9 fusion.1
  12.3 0.1 copy.16
  12.4 1.1 broadcast_in_dim.10
  13.6 16.2 %all-to-all-start = ((bf16[16,224,128]{2,1,0:T(8,128)(2,1)}), bf16[16,224,128]{2,1,0:T(8,128)(2,1)S(1)}, u32[]{:S(2)}, u32[]{:S(2)}) async-start(bf16[16,224,128]{2,1,0:T(8,128)(2,1)} %broadcast_in_dim.10), calls=%async_computation | async-start | bytes 1835008 | tf_op jit(solution)/shard_map/all_to_all | solution.py:324
  29.8 3.1 %collective-permute-start = (bf16[192,256]{1,0:T(8,128)(2,1)S(1)}, bf16[192,256]{1,0:T(8,128)(2,1)S(1)}, u32[]{:S(2)}, u32[]{:S(2)}) collective-permute-start(bf16[192,256]{1,0:T(8,128)(2,1)S(1)} %copy-done.3), channel_id=1, source_target_pairs={{0,192},{192,256},{256,448},{448,0},{384,320},{320,128},{128,64},{... | collective-permute-start | bytes 294920 | tf_op jit(solution)/shard_map/ppermute | solution.py:361
  32.9 4.0 %collective-permute-start.1 = (bf16[192,256]{1,0:T(8,128)(2,1)S(1)}, bf16[192,256]{1,0:T(8,128)(2,1)S(1)}, u32[]{:S(2)}, u32[]{:S(2)}) collective-permute-start(bf16[192,256]{1,0:T(8,128)(2,1)S(1)} %copy-done.3), channel_id=1, source_target_pairs={{0,256},{192,448},{256,0},{448,192},{384,128},{320,64},{128,384},{... | collective-permute-start | bytes 294920 | tf_op jit(solution)/shard_map/ppermute | solution.py:361
  36.9 2.2 %collective-permute-start.2 = (bf16[192,256]{1,0:T(8,128)(2,1)S(1)}, bf16[192,256]{1,0:T(8,128)(2,1)S(1)}, u32[]{:S(2)}, u32[]{:S(2)}) collective-permute-start(bf16[192,256]{1,0:T(8,128)(2,1)S(1)} %copy-done.3), channel_id=1, source_target_pairs={{0,448},{192,0},{256,192},{448,256},{384,64},{320,384},{128,320},{... | collective-permute-start | bytes 294920 | tf_op jit(solution)/shard_map/ppermute | solution.py:361
  39.2 22.1 %collective-permute-done.q1 = bf16[192,256]{1,0:T(8,128)(2,1)S(1)} collective-permute-done((bf16[192,256]{1,0:T(8,128)(2,1)S(1)}, bf16[192,256]{1,0:T(8,128)(2,1)S(1)}, u32[]{:S(2)}, u32[]{:S(2)}) %collective-permute-start) | collective-permute-done | bytes 98336 | tf_op jit(solution)/shard_map/ppermute | solution.py:361
  61.4 13.8 %attention.1 = (bf16[72,768]{1,0:T(8,128)(2,1)S(1)}, bf16[72,768]{1,0:T(8,128)(2,1)S(1)}, bf16[72,768]{1,0:T(8,128)(2,1)S(1)}, bf16[72,768]{1,0:T(8,128)(2,1)S(1)}) custom-call(s32[3]{0:T(128)S(1)} %pad_add_fusion.pos, bf16[16,224,128]{2,1,0:T(8,128)(2,1)S(1)} %all-to-all-done.kv, bf16[192,256]{1,0:T(8,128)(2,1)S(1)} %copy-done.3, ...), custom_call_target="tpu_custom_call" | custom-call | flops 12000000000 | bytes 4000000 | tf_op jit(solution)/shard_map/attention/pallas_call | solution.py:204
  75.2 1.9 %collective-permute-start.3 = (bf16[72,768]{1,0:T(8,128)(2,1)S(1)}, bf16[72,768]{1,0:T(8,128)(2,1)S(1)}, u32[]{:S(2)}, u32[]{:S(2)}) collective-permute-start(bf16[72,768]{1,0:T(8,128)(2,1)S(1)} %get-tuple-element.10), channel_id=1, source_target_pairs={{0,448},{192,0},{256,192},{448,256},{384,64},{320,384},{128,320},{... | collective-permute-start | bytes 331784 | tf_op jit(solution)/shard_map/ppermute | solution.py:368
  77.1 1.9 %collective-permute-start.4 = (bf16[72,768]{1,0:T(8,128)(2,1)S(1)}, bf16[72,768]{1,0:T(8,128)(2,1)S(1)}, u32[]{:S(2)}, u32[]{:S(2)}) collective-permute-start(bf16[72,768]{1,0:T(8,128)(2,1)S(1)} %get-tuple-element.11), channel_id=1, source_target_pairs={{0,256},{192,448},{256,0},{448,192},{384,128},{320,64},{128,384},{... | collective-permute-start | bytes 331784 | tf_op jit(solution)/shard_map/ppermute | solution.py:368
  79.0 5.2 %collective-permute-start.5 = (bf16[72,768]{1,0:T(8,128)(2,1)S(1)}, bf16[72,768]{1,0:T(8,128)(2,1)S(1)}, u32[]{:S(2)}, u32[]{:S(2)}) collective-permute-start(bf16[72,768]{1,0:T(8,128)(2,1)S(1)} %get-tuple-element.12), channel_id=1, source_target_pairs={{0,192},{192,256},{256,448},{448,0},{384,320},{320,128},{128,64},{... | collective-permute-start | bytes 331784 | tf_op jit(solution)/shard_map/ppermute | solution.py:368
  84.2 3.9 %collective-permute-done.4.p2 = bf16[72,768]{1,0:T(8,128)(2,1)S(1)} collective-permute-done((bf16[72,768]{1,0:T(8,128)(2,1)S(1)}, bf16[72,768]{1,0:T(8,128)(2,1)S(1)}, u32[]{:S(2)}, u32[]{:S(2)}) %collective-permute-start.4) | collective-permute-done | bytes 110624 | tf_op jit(solution)/shard_map/ppermute | solution.py:368
  88.1 1.9 %collective-permute-done.5.p3 = bf16[72,768]{1,0:T(8,128)(2,1)S(1)} collective-permute-done((bf16[72,768]{1,0:T(8,128)(2,1)S(1)}, bf16[72,768]{1,0:T(8,128)(2,1)S(1)}, u32[]{:S(2)}, u32[]{:S(2)}) %collective-permute-start.5) | collective-permute-done | bytes 110624 | tf_op jit(solution)/shard_map/ppermute | solution.py:368
  90.0 0.6 merge.1
  90.7 18.8 %all_to_all.15 = bf16[8,24,2048]{2,1,0:T(8,128)(2,1)S(1)} all-to-all(bf16[8,24,2048]{2,1,0:T(8,128)(2,1)S(1)} %bitcast.10), channel_id=1, replica_groups=mesh['z'=8,'y'=8,'x'=4,'c'=2] {'x','c'}, dimensions={0} | all-to-all | bytes 1572864 | tf_op jit(solution)/shard_map/all_to_all | solution.py:330
  109.5 0.1 convert_reduce_fusion.1
  109.6 0.1 multiply_reduce_fusion.2
  109.8 0.2 multiply_reduce_fusion.1
  110.0 0.1 multiply_convert_fusion
  110.1 15.5 %all_gather.6.rows = bf16[192,2048]{1,0:T(8,128)(2,1)} all-gather(bf16[24,2048]{1,0:T(8,128)(2,1)S(1)} %multiply_convert_fusion), channel_id=1, replica_groups=mesh['z'=8,'y'=8,'x'=4,'c'=2] {'x','c'}, dimensions={0}, use_global_device_ids=true | all-gather | bytes 884736 | tf_op jit(solution)/shard_map/all_gather | solution.py:372
  125.6 16.1 %all-gather.2.cloned.1.call-done.weights = bf16[2048,2176]{1,0:T(8,128)(2,1)} async-done(((bf16[32,2176]{1,0:T(8,128)(2,1)}), bf16[2048,2176]{1,0:T(8,128)(2,1)}) %all-gather.2.cloned.1.call-update) | async-done | bytes 8912912 | tf_op jit(solution)/shard_map/all_gather | solution.py:359
  141.6 7.0 %ffn.1 = bf16[192,2048]{1,0:T(8,128)(2,1)} custom-call(bf16[192,2048]{1,0:T(8,128)(2,1)} %all_gather.6.rows, bf16[2048,2176]{1,0:T(8,128)(2,1)} %all-gather.2.cloned.1.call-done.weights), custom_call_target="tpu_custom_call" | custom-call | flops 1700000000 | bytes 10000000 | tf_op jit(solution)/shard_map/ffn/pallas_call | solution.py:305
  148.7 17.2 %all_to_all.16 = bf16[8,24,2048]{2,1,0:T(8,128)(2,1)S(1)} all-to-all(bf16[8,24,2048]{2,1,0:T(8,128)(2,1)} %bitcast.12), channel_id=1, replica_groups=mesh['z'=8,'y'=8,'x'=4,'c'=2] {'x','c'}, dimensions={0} | all-to-all | bytes 1572864 | tf_op jit(solution)/shard_map/all_to_all | solution.py:330
  165.9 0.1 convert_reduce_fusion
  166.0 0.1 multiply_reduce_fusion
  166.1 0.8 add_convert_fusion
  (35 shorter events, 0.5 us)
Async XLA Ops:
  6.5 135.1 %all-gather.2.cloned.1.call-start = ((), (), s32[]{:S(2)}) async-start(), calls=%async_computation.3 | async-start | bytes 9052160 | tf_op jit(solution)/shard_map/all_gather | solution.py:359
  11.3 18.4 %copy-start.3 = (bf16[192,256]{1,0:T(8,128)(2,1)S(1)}, bf16[192,256]{1,0:T(8,128)(2,1)}, u32[]{:S(2)}) copy-start(bf16[192,256]{1,0:T(8,128)(2,1)} %q0.1) | copy-start | bytes 294916
  11.5 49.9 %copy-start.2 = (f32[192,4]{0,1:T(4,128)S(1)}, f32[192,4]{0,1:T(4,128)}, u32[]{:S(2)}) copy-start(f32[192,4]{0,1:T(4,128)} %param.17) | copy-start | bytes 9220
  13.6 47.8 %all-to-all-start = ((bf16[16,224,128]{2,1,0:T(8,128)(2,1)}), bf16[16,224,128]{2,1,0:T(8,128)(2,1)S(1)}, u32[]{:S(2)}, u32[]{:S(2)}) async-start(bf16[16,224,128]{2,1,0:T(8,128)(2,1)} %broadcast_in_dim.10), calls=%async_computation | async-start | bytes 1835008 | tf_op jit(solution)/shard_map/all_to_all | solution.py:324
  29.8 31.6 %collective-permute-start = (bf16[192,256]{1,0:T(8,128)(2,1)S(1)}, bf16[192,256]{1,0:T(8,128)(2,1)S(1)}, u32[]{:S(2)}, u32[]{:S(2)}) collective-permute-start(bf16[192,256]{1,0:T(8,128)(2,1)S(1)} %copy-done.3), channel_id=1, source_target_pairs={{0,192},{192,256},{256,448},{448,0},{384,320},{320,128},{128,64},{... | collective-permute-start | bytes 294920 | tf_op jit(solution)/shard_map/ppermute | solution.py:361
  32.9 28.5 %collective-permute-start.1 = (bf16[192,256]{1,0:T(8,128)(2,1)S(1)}, bf16[192,256]{1,0:T(8,128)(2,1)S(1)}, u32[]{:S(2)}, u32[]{:S(2)}) collective-permute-start(bf16[192,256]{1,0:T(8,128)(2,1)S(1)} %copy-done.3), channel_id=1, source_target_pairs={{0,256},{192,448},{256,0},{448,192},{384,128},{320,64},{128,384},{... | collective-permute-start | bytes 294920 | tf_op jit(solution)/shard_map/ppermute | solution.py:361
  36.9 24.4 %collective-permute-start.2 = (bf16[192,256]{1,0:T(8,128)(2,1)S(1)}, bf16[192,256]{1,0:T(8,128)(2,1)S(1)}, u32[]{:S(2)}, u32[]{:S(2)}) collective-permute-start(bf16[192,256]{1,0:T(8,128)(2,1)S(1)} %copy-done.3), channel_id=1, source_target_pairs={{0,448},{192,0},{256,192},{448,256},{384,64},{320,384},{128,320},{... | collective-permute-start | bytes 294920 | tf_op jit(solution)/shard_map/ppermute | solution.py:361
  61.4 28.7 %copy-start = (bf16[256,2048]{1,0:T(8,128)(2,1)S(1)}, bf16[256,2048]{1,0:T(8,128)(2,1)}, u32[]{:S(2)}) copy-start(bf16[256,2048]{1,0:T(8,128)(2,1)} %weight.1) | copy-start | bytes 3145732
  61.4 28.7 %copy-start.1 = (bf16[192,256]{1,0:T(8,128)(2,1)S(1)}, bf16[192,256]{1,0:T(8,128)(2,1)}, u32[]{:S(2)}) copy-start(bf16[192,256]{1,0:T(8,128)(2,1)} %gates.1) | copy-start | bytes 294916
  75.2 9.0 %collective-permute-start.3 = (bf16[72,768]{1,0:T(8,128)(2,1)S(1)}, bf16[72,768]{1,0:T(8,128)(2,1)S(1)}, u32[]{:S(2)}, u32[]{:S(2)}) collective-permute-start(bf16[72,768]{1,0:T(8,128)(2,1)S(1)} %get-tuple-element.10), channel_id=1, source_target_pairs={{0,448},{192,0},{256,192},{448,256},{384,64},{320,384},{128,320},{... | collective-permute-start | bytes 331784 | tf_op jit(solution)/shard_map/ppermute | solution.py:368
  77.1 11.0 %collective-permute-start.4 = (bf16[72,768]{1,0:T(8,128)(2,1)S(1)}, bf16[72,768]{1,0:T(8,128)(2,1)S(1)}, u32[]{:S(2)}, u32[]{:S(2)}) collective-permute-start(bf16[72,768]{1,0:T(8,128)(2,1)S(1)} %get-tuple-element.11), channel_id=1, source_target_pairs={{0,256},{192,448},{256,0},{448,192},{384,128},{320,64},{128,384},{... | collective-permute-start | bytes 331784 | tf_op jit(solution)/shard_map/ppermute | solution.py:368
  79.0 11.0 %collective-permute-start.5 = (bf16[72,768]{1,0:T(8,128)(2,1)S(1)}, bf16[72,768]{1,0:T(8,128)(2,1)S(1)}, u32[]{:S(2)}, u32[]{:S(2)}) collective-permute-start(bf16[72,768]{1,0:T(8,128)(2,1)S(1)} %get-tuple-element.12), channel_id=1, source_target_pairs={{0,192},{192,256},{256,448},{448,0},{384,320},{320,128},{128,64},{... | collective-permute-start | bytes 331784 | tf_op jit(solution)/shard_map/ppermute | solution.py:368
  90.7 19.1 %copy-start.4 = (bf16[24,2048]{1,0:T(8,128)(2,1)S(1)}, bf16[24,2048]{1,0:T(8,128)(2,1)}, u32[]{:S(2)}) copy-start(bf16[24,2048]{1,0:T(8,128)(2,1)} %param.13) | copy-start | bytes 294916
  90.7 19.1 %copy-start.5 = (f32[2048]{0:T(1024)S(1)}, f32[2048]{0:T(1024)}, u32[]{:S(2)}) copy-start(f32[2048]{0:T(1024)} %param.20) | copy-start | bytes 24580
  90.7 19.3 %copy-start.7 = (f32[2048]{0:T(1024)S(1)}, f32[2048]{0:T(1024)}, u32[]{:S(2)}) copy-start(f32[2048]{0:T(1024)} %param.21) | copy-start | bytes 24580
  148.6 17.5 %copy-start.6 = (f32[2048]{0:T(1024)S(1)}, f32[2048]{0:T(1024)}, u32[]{:S(2)}) copy-start(f32[2048]{0:T(1024)} %param.22) | copy-start | bytes 24580
Sparse Core Ops, SparseCore 0:
  10.3 131.2 all-gather.1

commit v4 on v3

--- a/solution.py
+++ b/solution.py
@@ -11,7 +11,7 @@
 ROWS = 192
 QG = 4
 ZH = 8 // QG
-ZGRID = ((0, 3, 4, 7), (6, 5, 2, 1))
+ZGRID = ((0, 2, 4, 6), (7, 1, 3, 5))
 YS = 8
 NB = ZH * YS
 TILE = 1536
@@ -67,23 +67,25 @@
     return z
 
 
-def attention_kernel(pos, kv, q0, q1, q2, q3, own, o0, o1, o2, o3, kc, vt, qt, acc, ls, ms):
+def attention_kernel(pos, kv0, kv1, q0, q1, q2, q3, own, o0, o1, o2, o3, kc, vt, qt, acc, ls, ms):
+    kv = (kv0, kv1)
     q = (q0, q1, q2, q3)
     out = (o0, o1, o2, o3)
     zh = pos[0]
     zl = pos[1]
     y = pos[2]
     mine = grid_z(zh, zl)
-    lower = jnp.minimum(grid_z(0, zl), grid_z(1, zl))
-    upper = jnp.maximum(grid_z(0, zl), grid_z(1, zl))
-    low_at = jnp.where(grid_z(0, zl) == lower, 0, 1)
+    theirs = grid_z(1 - zh, zl)
+    upper = jnp.maximum(mine, theirs)
+    low_at = jnp.where(mine < theirs, 0, 1)
     kc[:, 128:256] = jnp.zeros((NB * ROWS, 128), BF16)
     kmax = jnp.zeros((1, 1), F32)
     for b in range(NB):
         base = b * ROWS
-        kc[base : base + ROWS, 0:128] = kv[b, 0:ROWS, :]
-        left = kv[b, 192:208, :].astype(F32)
-        right = kv[b, 208:224, :].astype(F32)
+        block = kv[b // YS].at[b % YS]
+        kc[base : base + ROWS, 0:128] = block[0:ROWS, :]
+        left = block[192:208, :].astype(F32)
+        right = block[208:224, :].astype(F32)
         kc[base : base + 128, 128:144] = left.T.astype(BF16)
         kc[base + 128 : base + ROWS, 128:144] = right.T[0:64].astype(BF16)
         kmax = jnp.maximum(kmax, left[15:16, 0:1])
@@ -100,7 +102,8 @@
     for j in range(QG):
         asked = grid_z(zh, (zl + QG - j) % QG)
         last = jnp.where(asked > upper, 1 - low_at, low_at)
-        ends = kv[last * YS + YS - 1, 208:224, :].astype(F32)[:, 63:64]
+        ends = [rows[YS - 1, 208:224, :].astype(F32)[:, 63:64] for rows in kv]
+        ends = jnp.where(last == 0, ends[0], ends[1])
         turned = (q[j][...].astype(F32) * 0.125).T
         turned = jnp.concatenate([turned[h * HD : (h + 1) * HD] for h in range(HL)], axis=1)
         norm = jnp.sqrt(jnp.sum(turned * turned, axis=0, keepdims=True))
@@ -160,9 +163,8 @@
             j = u // ZH
             hz = u % ZH
             asked = grid_z(zh, (zl + QG - j) % QG)
-            held = grid_z(hz, zl)
-            edge = asked == held
-            whole = asked > held
+            edge = u == 0
+            whole = asked > jnp.where(hz == 0, mine, theirs)
 
             @pl.when(whole)
             def _():
@@ -199,12 +201,12 @@
         out[j][HD:OUTR, :] = stats.astype(BF16)
 
 
-def attention(pos, kv, *rest):
+def attention(pos, *rest):
     vmem = pl.BlockSpec(memory_space=pltpu.VMEM)
     return pl.pallas_call(
         attention_kernel,
         out_shape=[jax.ShapeDtypeStruct((OUTR, QR), BF16)] * QG,
-        in_specs=[pl.BlockSpec(memory_space=pltpu.SMEM)] + [vmem] * (QG + 2),
+        in_specs=[pl.BlockSpec(memory_space=pltpu.SMEM)] + [vmem] * (QG + 3),
         out_specs=[vmem] * QG,
         scratch_shapes=[
             pltpu.VMEM((NB * ROWS, 256), BF16),
@@ -217,7 +219,7 @@
         compiler_params=pltpu.CompilerParams(vmem_limit_bytes=48 * 1024 * 1024),
         cost_estimate=pl.CostEstimate(flops=12_000_000_000, bytes_accessed=4_000_000, transcendentals=9_000_000),
         name="attention",
-    )(pos, kv, *rest)
+    )(pos, *rest)
 
 
 def merge_kernel(p0, p1, p2, p3, gates, weight, out):
@@ -319,9 +321,9 @@
     )(rows, weights)
 
 
-def copies(value, axis, groups):
-    sent = jnp.broadcast_to(value[None], (len(groups[0]), *value.shape))
-    return lax.all_to_all(sent, axis, 0, 0, axis_index_groups=groups, tiled=True)
+def copies(value, axis):
+    sent = jnp.broadcast_to(value[None], (lax.axis_size(axis), *value.shape))
+    return lax.all_to_all(sent, axis, 0, 0, tiled=True)
 
 
 def sum_at_owner(value):
@@ -357,14 +359,15 @@
     pad = jnp.zeros((gate_weight.shape[0], WC - GU - FFL), BF16)
     packed = jnp.concatenate([gate_weight, up_weight, down_weight.T, pad], axis=1)
     weights = lax.all_gather(packed, SP, axis=0, tiled=True)
-    columns = [[ZGRID[a][b] * YS + y for a in range(ZH) for y in range(YS)] for b in range(QG)]
     q_all = [queries] + [lax.ppermute(queries, "z", turn(r)) for r in range(1, QG)]
-    kv = copies(key_payload(keys, values, log_gates), SP, columns)
+    held = copies(key_payload(keys, values, log_gates), "y")
+    swap = [pair for column in zip(*ZGRID) for pair in (column, column[::-1])]
+    lent = lax.ppermute(held, "z", swap)
     z = lax.axis_index("z")
     zh = sum(jnp.where(z == ZGRID[a][b], a, 0) for a in range(ZH) for b in range(QG))
     zl = sum(jnp.where(z == ZGRID[a][b], b, 0) for a in range(ZH) for b in range(QG))
     pos = jnp.stack([zh, zl, lax.axis_index("y")]).astype(jnp.int32)
-    parts = attention(pos, kv, *q_all, log_gates.T)
+    parts = attention(pos, held, lent, *q_all, log_gates.T)
     parts = [parts[0]] + [lax.ppermute(parts[r], "z", turn(QG - r)) for r in range(1, QG)]
     projected = sum_at_owner(merge(parts, out_gate, out_weight))
     mixed = resid.astype(F32) + rms_scale(projected, post_gain)

time: 174 us -> 168 us (0.966)
  blocking collectives: 51.5 us -> 75.9 us
  waiting for transfers between devices: 44 us -> 20.3 us
  Pallas kernels: 21.4 us -> 15.2 us
    all_to_all x0 -> x1, blocking collectives: none -> 21.5 us  [copies(): return lax.all_to_all(sent, axis, 0, 0, tiled=True)]
    all_to_all x1 -> x0, starting transfers between devices: 16.2 us -> none  [copies(): lax.all_to_all(sent, axis, 0, 0, axis_index_groups=groups, tiled=True)]
    all_gather x1, waiting for transfers between devices: 16.1 us -> 0.01 us  [shards(): weights = lax.all_gather(packed, SP, axis=0, tiled=True)]
    ppermute x3, waiting for transfers between devices: 22.1 us -> 8.9 us  [shards(): lax.ppermute(queries, 'z', turn(r))]
    ppermute x0 -> x1, starting transfers between devices: none -> 12.2 us  [shards(): lent = lax.ppermute(held, 'z', swap)]
    pallas_call x1, Pallas kernels: 13.8 us -> 7.57 us  [attention(): pl.pallas_call(attention_kernel, out_shape=[jax.ShapeDtypeStruct((OUTR, Q...]
    ppermute x3, waiting for transfers between devices: 5.82 us -> 11 us  [shards(): lax.ppermute(parts[r], 'z', turn(QG - r))]
    ppermute x3, starting transfers between devices: 9 us -> 12.3 us  [shards(): lax.ppermute(parts[r], 'z', turn(QG - r))]
  transfers between devices with their start and end apart: 8 -> 8, of which waited for: 4 -> 6; matrix products, arithmetic and copies ran while one was open for 3% -> 3% of each run, Pallas kernels for 8% -> 5%
where the time goes in v4:
time: 168 us; the launch traced here: 167 us
  blocking collectives  75.9 us (45%)
  starting transfers between devices  33.9 us (20%)
  waiting for transfers between devices  20.3 us (12%)
  Pallas kernels  15.2 us (9%)
  between operations  14.3 us (9%)
  other arithmetic  4.71 us (3%)
  local copies, waits for them, and re-layouts  2.25 us (1%)
    all_to_all x2, blocking collectives, sum_at_owner(): arrived = lax.all_to_all(blocks, TP, 0, 0, tiled=True)  38.9 us
    all_to_all x1, blocking collectives, copies(): return lax.all_to_all(sent, axis, 0, 0, tiled=True)  21.5 us
    all_gather x1, blocking collectives, shards(): normed_all = lax.all_gather(normed, TP, axis=0, tiled=True)  15.5 us
    ppermute x3, starting transfers between devices, shards(): lax.ppermute(parts[r], 'z', turn(QG - r))  12.3 us
    ppermute x1, starting transfers between devices, shards(): lent = lax.ppermute(held, 'z', swap)  12.2 us
    ppermute x3, waiting for transfers between devices, shards(): lax.ppermute(parts[r], 'z', turn(QG - r))  11 us
    ppermute x3, starting transfers between devices, shards(): lax.ppermute(queries, 'z', turn(r))  9.31 us
    ppermute x3, waiting for transfers between devices, shards(): lax.ppermute(queries, 'z', turn(r))  8.9 us
  transfers between devices with their start and end apart: 8, of which 6 were waited for; matrix products, arithmetic and copies ran while one was open for 3% of the time, Pallas kernels for 5%

profile of v4, /device:TPU:1, one launch (start us, length us, event | category | flops | bytes accessed | tf_op | source)
XLA Modules:
  0.0 166.6 jit_solution(17488111648438640368)
XLA Ops:
  6.5 1.7 concatenate.21
  8.2 0.8 multiply_reduce_fusion.3
  9.0 0.6 reduce_max.9
  10.5 0.7 reduce-precision_convert_fusion.1
  11.4 0.1 copy.14
  11.5 0.9 fusion.1
  12.5 21.5 %all_to_all.15.kv0 = bf16[8,224,128]{2,1,0:T(8,128)(2,1)S(1)} all-to-all(bf16[8,224,128]{2,1,0:T(8,128)(2,1)S(1)} %broadcast_in_dim.10), channel_id=1, replica_groups=mesh['z'=8,'y'=8,'x'=4,'c'=2] {'y'}, dimensions={0} | all-to-all | bytes 917504 | tf_op jit(solution)/shard_map/all_to_all | solution.py:326
  34.1 12.2 %collective-permute-start = (bf16[8,224,128]{2,1,0:T(8,128)(2,1)S(1)}, bf16[8,224,128]{2,1,0:T(8,128)(2,1)S(1)}, u32[]{:S(2)}, u32[]{:S(2)}) collective-permute-start(bf16[8,224,128]{2,1,0:T(8,128)(2,1)S(1)} %all_to_all.15.kv0), channel_id=1, source_target_pairs={{0,448},{448,0},{128,64},{64,128},{256,192},{192,256},{384,320},{3... | collective-permute-start | bytes 1376264 | tf_op jit(solution)/shard_map/ppermute | solution.py:365
  46.3 1.9 %collective-permute-start.2 = (bf16[192,256]{1,0:T(8,128)(2,1)S(1)}, bf16[192,256]{1,0:T(8,128)(2,1)S(1)}, u32[]{:S(2)}, u32[]{:S(2)}) collective-permute-start(bf16[192,256]{1,0:T(8,128)(2,1)S(1)} %copy-done.3), channel_id=1, source_target_pairs={{0,256},{128,384},{256,0},{384,128},{448,192},{64,320},{192,448},{... | collective-permute-start | bytes 294920 | tf_op jit(solution)/shard_map/ppermute | solution.py:362
  48.3 4.0 %collective-permute-start.1 = (bf16[192,256]{1,0:T(8,128)(2,1)S(1)}, bf16[192,256]{1,0:T(8,128)(2,1)S(1)}, u32[]{:S(2)}, u32[]{:S(2)}) collective-permute-start(bf16[192,256]{1,0:T(8,128)(2,1)S(1)} %copy-done.3), channel_id=1, source_target_pairs={{0,128},{128,256},{256,384},{384,0},{448,64},{64,192},{192,320},{3... | collective-permute-start | bytes 294920 | tf_op jit(solution)/shard_map/ppermute | solution.py:362
  52.2 3.4 %collective-permute-start.3 = (bf16[192,256]{1,0:T(8,128)(2,1)S(1)}, bf16[192,256]{1,0:T(8,128)(2,1)S(1)}, u32[]{:S(2)}, u32[]{:S(2)}) collective-permute-start(bf16[192,256]{1,0:T(8,128)(2,1)S(1)} %copy-done.3), channel_id=1, source_target_pairs={{0,384},{128,0},{256,128},{384,256},{448,320},{64,448},{192,64},{3... | collective-permute-start | bytes 294920 | tf_op jit(solution)/shard_map/ppermute | solution.py:362
  55.8 1.0 collective-permute-done.2.q2
  56.8 0.3 collective-permute-done.1.q1
  57.1 7.6 %collective-permute-done.3.q3 = bf16[192,256]{1,0:T(8,128)(2,1)S(1)} collective-permute-done((bf16[192,256]{1,0:T(8,128)(2,1)S(1)}, bf16[192,256]{1,0:T(8,128)(2,1)S(1)}, u32[]{:S(2)}, u32[]{:S(2)}) %collective-permute-start.3) | collective-permute-done | bytes 98336 | tf_op jit(solution)/shard_map/ppermute | solution.py:362
  64.7 0.4 collective-permute-done.kv1
  65.1 7.6 %attention.1 = (bf16[72,768]{1,0:T(8,128)(2,1)S(1)}, bf16[72,768]{1,0:T(8,128)(2,1)S(1)}, bf16[72,768]{1,0:T(8,128)(2,1)S(1)}, bf16[72,768]{1,0:T(8,128)(2,1)S(1)}) custom-call(s32[3]{0:T(128)S(1)} %pad_add_fusion.pos, bf16[8,224,128]{2,1,0:T(8,128)(2,1)S(1)} %all_to_all.15.kv0, bf16[8,224,128]{2,1,0:T(8,128)(2,1)S(1)} %collective-permute-done.kv1, ...), custom_call_target="tpu_custom_call" | custom-call | flops 12000000000 | bytes 4000000 | tf_op jit(solution)/shard_map/attention/pallas_call | solution.py:206
  72.6 3.4 %collective-permute-start.4 = (bf16[72,768]{1,0:T(8,128)(2,1)S(1)}, bf16[72,768]{1,0:T(8,128)(2,1)S(1)}, u32[]{:S(2)}, u32[]{:S(2)}) collective-permute-start(bf16[72,768]{1,0:T(8,128)(2,1)S(1)} %get-tuple-element.10), channel_id=1, source_target_pairs={{0,384},{128,0},{256,128},{384,256},{448,320},{64,448},{192,64},{3... | collective-permute-start | bytes 331784 | tf_op jit(solution)/shard_map/ppermute | solution.py:371
  76.1 7.0 %collective-permute-start.5 = (bf16[72,768]{1,0:T(8,128)(2,1)S(1)}, bf16[72,768]{1,0:T(8,128)(2,1)S(1)}, u32[]{:S(2)}, u32[]{:S(2)}) collective-permute-start(bf16[72,768]{1,0:T(8,128)(2,1)S(1)} %get-tuple-element.11), channel_id=1, source_target_pairs={{0,256},{128,384},{256,0},{384,128},{448,192},{64,320},{192,448},{... | collective-permute-start | bytes 331784 | tf_op jit(solution)/shard_map/ppermute | solution.py:371
  83.0 1.9 %collective-permute-start.6 = (bf16[72,768]{1,0:T(8,128)(2,1)S(1)}, bf16[72,768]{1,0:T(8,128)(2,1)S(1)}, u32[]{:S(2)}, u32[]{:S(2)}) collective-permute-start(bf16[72,768]{1,0:T(8,128)(2,1)S(1)} %get-tuple-element.12), channel_id=1, source_target_pairs={{0,128},{128,256},{256,384},{384,0},{448,64},{64,192},{192,320},{3... | collective-permute-start | bytes 331784 | tf_op jit(solution)/shard_map/ppermute | solution.py:371
  85.0 4.3 %collective-permute-done.5.p2 = bf16[72,768]{1,0:T(8,128)(2,1)S(1)} collective-permute-done((bf16[72,768]{1,0:T(8,128)(2,1)S(1)}, bf16[72,768]{1,0:T(8,128)(2,1)S(1)}, u32[]{:S(2)}, u32[]{:S(2)}) %collective-permute-start.5) | collective-permute-done | bytes 110624 | tf_op jit(solution)/shard_map/ppermute | solution.py:371
  89.3 6.8 %collective-permute-done.6.p3 = bf16[72,768]{1,0:T(8,128)(2,1)S(1)} collective-permute-done((bf16[72,768]{1,0:T(8,128)(2,1)S(1)}, bf16[72,768]{1,0:T(8,128)(2,1)S(1)}, u32[]{:S(2)}, u32[]{:S(2)}) %collective-permute-start.6) | collective-permute-done | bytes 110624 | tf_op jit(solution)/shard_map/ppermute | solution.py:371
  96.0 0.6 merge.1
  96.7 23.2 %all_to_all.16 = bf16[8,24,2048]{2,1,0:T(8,128)(2,1)S(1)} all-to-all(bf16[8,24,2048]{2,1,0:T(8,128)(2,1)S(1)} %bitcast.10), channel_id=1, replica_groups=mesh['z'=8,'y'=8,'x'=4,'c'=2] {'x','c'}, dimensions={0} | all-to-all | bytes 1572864 | tf_op jit(solution)/shard_map/all_to_all | solution.py:332
  119.8 0.1 convert_reduce_fusion.1
  120.0 0.1 multiply_reduce_fusion.2
  120.1 0.2 multiply_reduce_fusion.1
  120.3 0.1 multiply_convert_fusion
  120.5 15.5 %all_gather.6.rows = bf16[192,2048]{1,0:T(8,128)(2,1)} all-gather(bf16[24,2048]{1,0:T(8,128)(2,1)S(1)} %multiply_convert_fusion), channel_id=1, replica_groups=mesh['z'=8,'y'=8,'x'=4,'c'=2] {'x','c'}, dimensions={0}, use_global_device_ids=true | all-gather | bytes 884736 | tf_op jit(solution)/shard_map/all_gather | solution.py:375
  135.9 7.0 %ffn.1 = bf16[192,2048]{1,0:T(8,128)(2,1)} custom-call(bf16[192,2048]{1,0:T(8,128)(2,1)} %all_gather.6.rows, bf16[2048,2176]{1,0:T(8,128)(2,1)} %all-gather.2.cloned.1.call-done.weights), custom_call_target="tpu_custom_call" | custom-call | flops 1700000000 | bytes 10000000 | tf_op jit(solution)/shard_map/ffn/pallas_call | solution.py:307
  142.9 15.7 %all_to_all.17 = bf16[8,24,2048]{2,1,0:T(8,128)(2,1)S(1)} all-to-all(bf16[8,24,2048]{2,1,0:T(8,128)(2,1)} %bitcast.12), channel_id=1, replica_groups=mesh['z'=8,'y'=8,'x'=4,'c'=2] {'x','c'}, dimensions={0} | all-to-all | bytes 1572864 | tf_op jit(solution)/shard_map/all_to_all | solution.py:332
  158.8 0.1 multiply_reduce_fusion
  158.9 0.8 add_convert_fusion
  (36 shorter events, 0.8 us)
Async XLA Ops:
  6.5 58.5 %copy-start.2 = (f32[192,4]{0,1:T(4,128)S(1)}, f32[192,4]{0,1:T(4,128)}, u32[]{:S(2)}) copy-start(f32[192,4]{0,1:T(4,128)} %param.17) | copy-start | bytes 9220
  6.5 39.8 %copy-start.3 = (bf16[192,256]{1,0:T(8,128)(2,1)S(1)}, bf16[192,256]{1,0:T(8,128)(2,1)}, u32[]{:S(2)}) copy-start(bf16[192,256]{1,0:T(8,128)(2,1)} %q0.1) | copy-start | bytes 294916
  6.5 129.4 %all-gather.2.cloned.1.call-start = ((), (), s32[]{:S(2)}) async-start(), calls=%async_computation.3 | async-start | bytes 9052160 | tf_op jit(solution)/shard_map/all_gather | solution.py:361
  34.1 31.0 %collective-permute-start = (bf16[8,224,128]{2,1,0:T(8,128)(2,1)S(1)}, bf16[8,224,128]{2,1,0:T(8,128)(2,1)S(1)}, u32[]{:S(2)}, u32[]{:S(2)}) collective-permute-start(bf16[8,224,128]{2,1,0:T(8,128)(2,1)S(1)} %all_to_all.15.kv0), channel_id=1, source_target_pairs={{0,448},{448,0},{128,64},{64,128},{256,192},{192,256},{384,320},{3... | collective-permute-start | bytes 1376264 | tf_op jit(solution)/shard_map/ppermute | solution.py:365
  46.3 10.4 %collective-permute-start.2 = (bf16[192,256]{1,0:T(8,128)(2,1)S(1)}, bf16[192,256]{1,0:T(8,128)(2,1)S(1)}, u32[]{:S(2)}, u32[]{:S(2)}) collective-permute-start(bf16[192,256]{1,0:T(8,128)(2,1)S(1)} %copy-done.3), channel_id=1, source_target_pairs={{0,256},{128,384},{256,0},{384,128},{448,192},{64,320},{192,448},{... | collective-permute-start | bytes 294920 | tf_op jit(solution)/shard_map/ppermute | solution.py:362
  48.3 8.8 %collective-permute-start.1 = (bf16[192,256]{1,0:T(8,128)(2,1)S(1)}, bf16[192,256]{1,0:T(8,128)(2,1)S(1)}, u32[]{:S(2)}, u32[]{:S(2)}) collective-permute-start(bf16[192,256]{1,0:T(8,128)(2,1)S(1)} %copy-done.3), channel_id=1, source_target_pairs={{0,128},{128,256},{256,384},{384,0},{448,64},{64,192},{192,320},{3... | collective-permute-start | bytes 294920 | tf_op jit(solution)/shard_map/ppermute | solution.py:362
  52.2 12.4 %collective-permute-start.3 = (bf16[192,256]{1,0:T(8,128)(2,1)S(1)}, bf16[192,256]{1,0:T(8,128)(2,1)S(1)}, u32[]{:S(2)}, u32[]{:S(2)}) collective-permute-start(bf16[192,256]{1,0:T(8,128)(2,1)S(1)} %copy-done.3), channel_id=1, source_target_pairs={{0,384},{128,0},{256,128},{384,256},{448,320},{64,448},{192,64},{3... | collective-permute-start | bytes 294920 | tf_op jit(solution)/shard_map/ppermute | solution.py:362
  65.1 30.9 %copy-start = (bf16[256,2048]{1,0:T(8,128)(2,1)S(1)}, bf16[256,2048]{1,0:T(8,128)(2,1)}, u32[]{:S(2)}) copy-start(bf16[256,2048]{1,0:T(8,128)(2,1)} %weight.1) | copy-start | bytes 3145732
  65.1 30.9 %copy-start.1 = (bf16[192,256]{1,0:T(8,128)(2,1)S(1)}, bf16[192,256]{1,0:T(8,128)(2,1)}, u32[]{:S(2)}) copy-start(bf16[192,256]{1,0:T(8,128)(2,1)} %gates.1) | copy-start | bytes 294916
  72.6 12.3 %collective-permute-start.4 = (bf16[72,768]{1,0:T(8,128)(2,1)S(1)}, bf16[72,768]{1,0:T(8,128)(2,1)S(1)}, u32[]{:S(2)}, u32[]{:S(2)}) collective-permute-start(bf16[72,768]{1,0:T(8,128)(2,1)S(1)} %get-tuple-element.10), channel_id=1, source_target_pairs={{0,384},{128,0},{256,128},{384,256},{448,320},{64,448},{192,64},{3... | collective-permute-start | bytes 331784 | tf_op jit(solution)/shard_map/ppermute | solution.py:371
  76.1 13.2 %collective-permute-start.5 = (bf16[72,768]{1,0:T(8,128)(2,1)S(1)}, bf16[72,768]{1,0:T(8,128)(2,1)S(1)}, u32[]{:S(2)}, u32[]{:S(2)}) collective-permute-start(bf16[72,768]{1,0:T(8,128)(2,1)S(1)} %get-tuple-element.11), channel_id=1, source_target_pairs={{0,256},{128,384},{256,0},{384,128},{448,192},{64,320},{192,448},{... | collective-permute-start | bytes 331784 | tf_op jit(solution)/shard_map/ppermute | solution.py:371
  83.0 13.0 %collective-permute-start.6 = (bf16[72,768]{1,0:T(8,128)(2,1)S(1)}, bf16[72,768]{1,0:T(8,128)(2,1)S(1)}, u32[]{:S(2)}, u32[]{:S(2)}) collective-permute-start(bf16[72,768]{1,0:T(8,128)(2,1)S(1)} %get-tuple-element.12), channel_id=1, source_target_pairs={{0,128},{128,256},{256,384},{384,0},{448,64},{64,192},{192,320},{3... | collective-permute-start | bytes 331784 | tf_op jit(solution)/shard_map/ppermute | solution.py:371
  96.6 23.4 %copy-start.4 = (bf16[24,2048]{1,0:T(8,128)(2,1)S(1)}, bf16[24,2048]{1,0:T(8,128)(2,1)}, u32[]{:S(2)}) copy-start(bf16[24,2048]{1,0:T(8,128)(2,1)} %param.13) | copy-start | bytes 294916
  96.7 23.4 %copy-start.5 = (f32[2048]{0:T(1024)S(1)}, f32[2048]{0:T(1024)}, u32[]{:S(2)}) copy-start(f32[2048]{0:T(1024)} %param.20) | copy-start | bytes 24580
  96.7 23.7 %copy-start.7 = (f32[2048]{0:T(1024)S(1)}, f32[2048]{0:T(1024)}, u32[]{:S(2)}) copy-start(f32[2048]{0:T(1024)} %param.21) | copy-start | bytes 24580
  142.9 16.0 %copy-start.6 = (f32[2048]{0:T(1024)S(1)}, f32[2048]{0:T(1024)}, u32[]{:S(2)}) copy-start(f32[2048]{0:T(1024)} %param.22) | copy-start | bytes 24580
Sparse Core Ops, SparseCore 0:
  10.3 121.5 all-gather.1

commit v5 on v4

--- a/solution.py
+++ b/solution.py
@@ -23,6 +23,8 @@
 GU = 2 * FFL
 WC = 2176
 EPS = 1e-06
+TPS = 8
+OWN = ROWS // TPS
 LOW = -1e30
 GAP = 56.0
 
@@ -222,7 +224,14 @@
     )(pos, *rest)
 
 
-def merge_kernel(p0, p1, p2, p3, gates, weight, out):
+def by_core(core, rows, mine, theirs, cols):
+    low = rows[0 : ROWS // 2].astype(BF16)
+    high = rows[ROWS // 2 :].astype(BF16)
+    mine[:, cols] = jnp.where(core == 0, low, high)
+    theirs[:, cols] = jnp.where(core == 0, high, low)
+
+
+def merge_kernel(core, p0, p1, p2, p3, gates, weight, mine, theirs):
     parts = (p0, p1, p2, p3)
     tops = []
     sums = []
@@ -241,25 +250,35 @@
         mixed = mixed + parts[j][0:HD, :].astype(F32) * scale
     rows = (mixed / total).T
     rows = jnp.concatenate([rows[h * ROWS : (h + 1) * ROWS] for h in range(HL)], axis=1)
-    gated = (rows * jax.nn.sigmoid(gates[...].astype(F32))).astype(BF16)
-    out[...] = jnp.dot(gated, weight[...], preferred_element_type=F32).astype(BF16)
-
-
-def merge(parts, gates, weight):
+    rows = rows * jax.nn.sigmoid(gates[...].astype(F32))
+    order = [x * 2 + c for c in range(2) for x in range(TPS // 2)]
+    gated = jnp.concatenate([rows[k * OWN : (k + 1) * OWN] for k in order], axis=0).astype(BF16)
+    projected = jnp.dot(gated, weight[...], preferred_element_type=F32)
+    by_core(core[0], projected, mine, theirs, slice(None))
+
+
+def halves(wide):
+    return [jax.ShapeDtypeStruct((ROWS // 2, wide), BF16)] * 2
+
+
+def merge(core, parts, gates, weight):
+    vmem = pl.BlockSpec(memory_space=pltpu.VMEM)
     return pl.pallas_call(
         merge_kernel,
-        out_shape=jax.ShapeDtypeStruct((ROWS, weight.shape[1]), BF16),
+        out_shape=halves(weight.shape[1]),
+        in_specs=[pl.BlockSpec(memory_space=pltpu.SMEM)] + [vmem] * (QG + 2),
+        out_specs=[vmem] * 2,
         compiler_params=pltpu.CompilerParams(vmem_limit_bytes=32 * 1024 * 1024),
         cost_estimate=pl.CostEstimate(flops=400_000_000, bytes_accessed=2_000_000, transcendentals=50_000),
         name="merge",
-    )(*parts, gates, weight)
+    )(core, *parts, gates, weight)
 
 
 FC = 1024
 DEEP = 4
 
 
-def ffn_kernel(rows, weights, out, wv, acc, hid, sems):
+def ffn_kernel(core, rows, weights, mine, theirs, wv, acc, hid, sems):
     count = weights.shape[0] // FC
 
     def first(k):
@@ -297,28 +316,30 @@
     hid[:, 0:FFL] = hidden.astype(BF16)
     for k in range(count):
         arrive(count + k)
-        out[:, k * FC : (k + 1) * FC] = lax.dot_general(
+        part = lax.dot_general(
             hid[...], wv[k * FC : (k + 1) * FC, GU:WC], NT, preferred_element_type=F32
-        ).astype(BF16)
-
-
-def ffn(rows, weights):
+        )
+        by_core(core[0], part, mine, theirs, slice(k * FC, (k + 1) * FC))
+
+
+def ffn(core, rows, weights):
     wide = weights.shape[0]
+    vmem = pl.BlockSpec(memory_space=pltpu.VMEM)
     return pl.pallas_call(
         ffn_kernel,
-        out_shape=jax.ShapeDtypeStruct((ROWS, wide), BF16),
-        in_specs=[pl.BlockSpec(memory_space=pltpu.VMEM), pl.BlockSpec(memory_space=pltpu.HBM)],
-        out_specs=pl.BlockSpec(memory_space=pltpu.VMEM),
+        out_shape=halves(wide),
+        in_specs=[pl.BlockSpec(memory_space=pltpu.SMEM), vmem, pl.BlockSpec(memory_space=pltpu.HBM)],
+        out_specs=[vmem] * 2,
         scratch_shapes=[
             pltpu.VMEM((wide, WC), BF16),
             pltpu.VMEM((ROWS, GU), F32),
             pltpu.VMEM((ROWS, WC - GU), BF16),
             pltpu.SemaphoreType.DMA((2 * (wide // FC),)),
         ],
-        compiler_params=pltpu.CompilerParams(vmem_limit_bytes=60 * 1024 * 1024),
+        compiler_params=pltpu.CompilerParams(vmem_limit_bytes=55 * 1024 * 1024),
         cost_estimate=pl.CostEstimate(flops=1_700_000_000, bytes_accessed=10_000_000, transcendentals=140_000),
         name="ffn",
-    )(rows, weights)
+    )(core, rows, weights)
 
 
 def copies(value, axis):
@@ -326,10 +347,11 @@
     return lax.all_to_all(sent, axis, 0, 0, tiled=True)
 
 
-def sum_at_owner(value):
-    peers = lax.axis_size(TP)
-    blocks = value.reshape(peers, value.shape[0] // peers, value.shape[1])
-    arrived = lax.all_to_all(blocks, TP, 0, 0, tiled=True)
+def sum_at_owner(mine, theirs):
+    given = lax.ppermute(theirs, "c", [(0, 1), (1, 0)])
+    both = (mine.astype(F32) + given.astype(F32)).astype(BF16)
+    blocks = both.reshape(TPS // 2, OWN, both.shape[1])
+    arrived = lax.all_to_all(blocks, "x", 0, 0, tiled=True)
     return arrived.astype(F32).sum(axis=0)
 
 
@@ -369,11 +391,13 @@
     pos = jnp.stack([zh, zl, lax.axis_index("y")]).astype(jnp.int32)
     parts = attention(pos, held, lent, *q_all, log_gates.T)
     parts = [parts[0]] + [lax.ppermute(parts[r], "z", turn(QG - r)) for r in range(1, QG)]
-    projected = sum_at_owner(merge(parts, out_gate, out_weight))
+    core = lax.axis_index("c").astype(jnp.int32)[None]
+    projected = sum_at_owner(*merge(core, parts, out_gate, out_weight))
     mixed = resid.astype(F32) + rms_scale(projected, post_gain)
     normed = rms_scale(mixed, pre_gain).astype(BF16)
-    normed_all = lax.all_gather(normed, TP, axis=0, tiled=True)
-    total = sum_at_owner(ffn(normed_all, weights))
+    along = copies(normed, "x").reshape(ROWS // 2, -1)
+    normed_all = lax.all_gather(along, "c", axis=0, tiled=True)
+    total = sum_at_owner(*ffn(core, normed_all, weights))
     return (mixed + rms_scale(total, ffn_gain)).astype(BF16)
 
 

time: 168 us -> 167 us (level)
  blocking collectives: 75.9 us -> 58.9 us
  starting transfers between devices: 33.9 us -> 44.3 us
  waiting for transfers between devices: 20.3 us -> 24.3 us
    all_to_all x2, blocking collectives: 38.9 us -> 23.6 us  [sum_at_owner(): arrived = lax.all_to_all(blocks, 'x', 0, 0, tiled=True)]
    all_gather x1, blocking collectives: 15.5 us -> 5.2 us  [shards(): normed_all = lax.all_gather(along, 'c', axis=0, tiled=True)]
    all_to_all x1 -> x2, blocking collectives: 21.5 us -> 30.1 us  [copies(): return lax.all_to_all(sent, axis, 0, 0, tiled=True)]
    ppermute x3, starting transfers between devices: 12.3 us -> 18.5 us  [shards(): lax.ppermute(parts[r], 'z', turn(QG - r))]
    ppermute x0 -> x2, starting transfers between devices: none -> 4.21 us  [sum_at_owner(): given = lax.ppermute(theirs, 'c', [(0, 1), (1, 0)])]
    ppermute x0 -> x2, waiting for transfers between devices: none -> 3.23 us  [sum_at_owner(): given = lax.ppermute(theirs, 'c', [(0, 1), (1, 0)])]
  transfers between devices with their start and end apart: 8 -> 10, of which waited for: 6 -> 7; matrix products, arithmetic and copies ran while one was open for 3% -> 3% of each run, Pallas kernels for 5% -> 5%
where the time goes in v5:
time: 167 us
  blocking collectives  58.9 us (35%)
  starting transfers between devices  44.3 us (27%)
  waiting for transfers between devices  24.3 us (15%)
  Pallas kernels  15.2 us (9%)
  between operations  14.3 us (9%)
  other arithmetic  5.79 us (3%)
  local copies, waits for them, and re-layouts  3.79 us (2%)
    all_to_all x2, blocking collectives, copies(): return lax.all_to_all(sent, axis, 0, 0, tiled=True)  30.1 us
    all_to_all x2, blocking collectives, sum_at_owner(): arrived = lax.all_to_all(blocks, 'x', 0, 0, tiled=True)  23.6 us
    ppermute x3, starting transfers between devices, shards(): lax.ppermute(parts[r], 'z', turn(QG - r))  18.5 us
    ppermute x1, starting transfers between devices, shards(): lent = lax.ppermute(held, 'z', swap)  12.2 us
    ppermute x3, waiting for transfers between devices, shards(): lax.ppermute(parts[r], 'z', turn(QG - r))  11.9 us
    ppermute x3, starting transfers between devices, shards(): lax.ppermute(queries, 'z', turn(r))  9.32 us
    ppermute x3, waiting for transfers between devices, shards(): lax.ppermute(queries, 'z', turn(r))  9.13 us
    pallas_call x1, Pallas kernels, attention(): pl.pallas_call(attention_kernel, out_shape=[jax.ShapeDtypeStruct((OUTR, Q...  7.58 us
  transfers between devices with their start and end apart: 10, of which 7 were waited for; matrix products, arithmetic and copies ran while one was open for 3% of the time, Pallas kernels for 5%

profile of v5, /device:TPU:1, one launch (start us, length us, event | category | flops | bytes accessed | tf_op | source)
XLA Modules:
  0.0 166.5 jit_solution(15406656517330459514)
XLA Ops:
  6.5 1.6 concatenate.21
  8.2 0.8 multiply_reduce_fusion.3
  8.9 0.6 reduce_max.9
  10.4 0.7 reduce-precision_convert_fusion.1
  11.4 0.9 fusion.1
  12.5 21.5 %all_to_all.20.kv0 = bf16[8,224,128]{2,1,0:T(8,128)(2,1)S(1)} all-to-all(bf16[8,224,128]{2,1,0:T(8,128)(2,1)S(1)} %broadcast_in_dim.15), channel_id=1, replica_groups=mesh['z'=8,'y'=8,'x'=4,'c'=2] {'y'}, dimensions={0} | all-to-all | bytes 917504 | tf_op jit(solution)/shard_map/all_to_all | solution.py:347
  34.0 12.2 %collective-permute-start = (bf16[8,224,128]{2,1,0:T(8,128)(2,1)S(1)}, bf16[8,224,128]{2,1,0:T(8,128)(2,1)S(1)}, u32[]{:S(2)}, u32[]{:S(2)}) collective-permute-start(bf16[8,224,128]{2,1,0:T(8,128)(2,1)S(1)} %all_to_all.20.kv0), channel_id=1, source_target_pairs={{0,448},{448,0},{128,64},{64,128},{256,192},{192,256},{384,320},{3... | collective-permute-start | bytes 1376264 | tf_op jit(solution)/shard_map/ppermute | solution.py:387
  46.3 1.9 %collective-permute-start.2 = (bf16[192,256]{1,0:T(8,128)(2,1)}, bf16[192,256]{1,0:T(8,128)(2,1)S(1)}, u32[]{:S(2)}, u32[]{:S(2)}) collective-permute-start(bf16[192,256]{1,0:T(8,128)(2,1)} %q0.1), channel_id=1, source_target_pairs={{0,256},{128,384},{256,0},{384,128},{448,192},{64,320},{192,448},{... | collective-permute-start | bytes 294920 | tf_op jit(solution)/shard_map/ppermute | solution.py:384
  48.2 4.0 %collective-permute-start.1 = (bf16[192,256]{1,0:T(8,128)(2,1)}, bf16[192,256]{1,0:T(8,128)(2,1)S(1)}, u32[]{:S(2)}, u32[]{:S(2)}) collective-permute-start(bf16[192,256]{1,0:T(8,128)(2,1)} %q0.1), channel_id=1, source_target_pairs={{0,128},{128,256},{256,384},{384,0},{448,64},{64,192},{192,320},{3... | collective-permute-start | bytes 294920 | tf_op jit(solution)/shard_map/ppermute | solution.py:384
  52.2 3.4 %collective-permute-start.3 = (bf16[192,256]{1,0:T(8,128)(2,1)}, bf16[192,256]{1,0:T(8,128)(2,1)S(1)}, u32[]{:S(2)}, u32[]{:S(2)}) collective-permute-start(bf16[192,256]{1,0:T(8,128)(2,1)} %q0.1), channel_id=1, source_target_pairs={{0,384},{128,0},{256,128},{384,256},{448,320},{64,448},{192,64},{3... | collective-permute-start | bytes 294920 | tf_op jit(solution)/shard_map/ppermute | solution.py:384
  55.7 1.2 collective-permute-done.2.q2
  57.3 7.6 %collective-permute-done.3.q3 = bf16[192,256]{1,0:T(8,128)(2,1)S(1)} collective-permute-done((bf16[192,256]{1,0:T(8,128)(2,1)}, bf16[192,256]{1,0:T(8,128)(2,1)S(1)}, u32[]{:S(2)}, u32[]{:S(2)}) %collective-permute-start.3) | collective-permute-done | bytes 98336 | tf_op jit(solution)/shard_map/ppermute | solution.py:384
  64.9 0.7 copy-done.2
  65.6 0.9 copy-done.3
  66.5 7.6 %attention.1 = (bf16[72,768]{1,0:T(8,128)(2,1)S(1)}, bf16[72,768]{1,0:T(8,128)(2,1)S(1)}, bf16[72,768]{1,0:T(8,128)(2,1)S(1)}, bf16[72,768]{1,0:T(8,128)(2,1)S(1)}) custom-call(s32[3]{0:T(128)S(1)} %pad_add_fusion.pos, bf16[8,224,128]{2,1,0:T(8,128)(2,1)S(1)} %all_to_all.20.kv0, bf16[8,224,128]{2,1,0:T(8,128)(2,1)S(1)} %collective-permute-done.kv1, ...), custom_call_target="tpu_custom_call" | custom-call | flops 12000000000 | bytes 4000000 | tf_op jit(solution)/shard_map/attention/pallas_call | solution.py:208
  74.1 3.6 %collective-permute-start.4 = (bf16[72,768]{1,0:T(8,128)(2,1)S(1)}, bf16[72,768]{1,0:T(8,128)(2,1)S(1)}, u32[]{:S(2)}, u32[]{:S(2)}) collective-permute-start(bf16[72,768]{1,0:T(8,128)(2,1)S(1)} %get-tuple-element.14), channel_id=1, source_target_pairs={{0,384},{128,0},{256,128},{384,256},{448,320},{64,448},{192,64},{3... | collective-permute-start | bytes 331784 | tf_op jit(solution)/shard_map/ppermute | solution.py:393
  77.7 13.0 %collective-permute-start.5 = (bf16[72,768]{1,0:T(8,128)(2,1)S(1)}, bf16[72,768]{1,0:T(8,128)(2,1)S(1)}, u32[]{:S(2)}, u32[]{:S(2)}) collective-permute-start(bf16[72,768]{1,0:T(8,128)(2,1)S(1)} %get-tuple-element.15), channel_id=1, source_target_pairs={{0,256},{128,384},{256,0},{384,128},{448,192},{64,320},{192,448},{... | collective-permute-start | bytes 331784 | tf_op jit(solution)/shard_map/ppermute | solution.py:393
  90.7 1.9 %collective-permute-start.6 = (bf16[72,768]{1,0:T(8,128)(2,1)S(1)}, bf16[72,768]{1,0:T(8,128)(2,1)S(1)}, u32[]{:S(2)}, u32[]{:S(2)}) collective-permute-start(bf16[72,768]{1,0:T(8,128)(2,1)S(1)} %get-tuple-element.16), channel_id=1, source_target_pairs={{0,128},{128,256},{256,384},{384,0},{448,64},{64,192},{192,320},{3... | collective-permute-start | bytes 331784 | tf_op jit(solution)/shard_map/ppermute | solution.py:393
  92.6 6.6 %collective-permute-done.5.p2 = bf16[72,768]{1,0:T(8,128)(2,1)S(1)} collective-permute-done((bf16[72,768]{1,0:T(8,128)(2,1)S(1)}, bf16[72,768]{1,0:T(8,128)(2,1)S(1)}, u32[]{:S(2)}, u32[]{:S(2)}) %collective-permute-start.5) | collective-permute-done | bytes 110624 | tf_op jit(solution)/shard_map/ppermute | solution.py:393
  99.2 5.3 %collective-permute-done.6.p3 = bf16[72,768]{1,0:T(8,128)(2,1)S(1)} collective-permute-done((bf16[72,768]{1,0:T(8,128)(2,1)S(1)}, bf16[72,768]{1,0:T(8,128)(2,1)S(1)}, u32[]{:S(2)}, u32[]{:S(2)}) %collective-permute-start.6) | collective-permute-done | bytes 110624 | tf_op jit(solution)/shard_map/ppermute | solution.py:393
  104.5 0.6 merge.1
  105.1 1.9 %collective-permute-start.7 = (bf16[96,2048]{1,0:T(8,128)(2,1)S(1)}, bf16[96,2048]{1,0:T(8,128)(2,1)S(1)}, u32[]{:S(2)}, u32[]{:S(2)}) collective-permute-start(bf16[96,2048]{1,0:T(8,128)(2,1)S(1)} %get-tuple-element.18), channel_id=1, source_target_pairs={{0,1},{1,0},{2,3},{3,2},{4,5},{5,4},{6,7},{7,6},{8,9},{9,8},{10,11... | collective-permute-start | bytes 1179656 | tf_op jit(solution)/shard_map/ppermute | solution.py:351
  107.0 1.7 %collective-permute-done.7 = bf16[96,2048]{1,0:T(8,128)(2,1)S(1)} collective-permute-done((bf16[96,2048]{1,0:T(8,128)(2,1)S(1)}, bf16[96,2048]{1,0:T(8,128)(2,1)S(1)}, u32[]{:S(2)}, u32[]{:S(2)}) %collective-permute-start.7) | collective-permute-done | bytes 393248 | tf_op jit(solution)/shard_map/ppermute | solution.py:351
  108.8 13.4 %all_to_all.21 = bf16[4,24,2048]{2,1,0:T(8,128)(2,1)S(1)} all-to-all(bf16[4,24,2048]{2,1,0:T(8,128)(2,1)S(1)} %bitcast.13), channel_id=1, replica_groups=mesh['z'=8,'y'=8,'x'=4,'c'=2] {'x'}, dimensions={0} | all-to-all | bytes 786432 | tf_op jit(solution)/shard_map/all_to_all | solution.py:354
  122.8 8.6 %all_to_all.22 = bf16[4,24,2048]{2,1,0:T(8,128)(2,1)S(1)} all-to-all(bf16[4,24,2048]{2,1,0:T(8,128)(2,1)S(1)} %broadcast_in_dim.16), channel_id=1, replica_groups=mesh['z'=8,'y'=8,'x'=4,'c'=2] {'x'}, dimensions={0} | all-to-all | bytes 786432 | tf_op jit(solution)/shard_map/all_to_all | solution.py:347
  131.4 5.2 %all_gather.6.rows = bf16[192,2048]{1,0:T(8,128)(2,1)} all-gather(bf16[96,2048]{1,0:T(8,128)(2,1)S(1)} %bitcast.15), channel_id=1, replica_groups=mesh['z'=8,'y'=8,'x'=4,'c'=2] {'c'}, dimensions={0}, use_global_device_ids=true | all-gather | bytes 1179648 | tf_op jit(solution)/shard_map/all_gather | solution.py:399
  136.6 7.0 %ffn.1 = (bf16[96,2048]{1,0:T(8,128)(2,1)}, bf16[96,2048]{1,0:T(8,128)(2,1)}) custom-call(s32[1]{0:T(128)} %bitcast.core, bf16[192,2048]{1,0:T(8,128)(2,1)} %all_gather.6.rows, bf16[2048,2176]{1,0:T(8,128)(2,1)} %all-gather.2.cloned.1.call-done.weights), custom_call_target="tpu_custom_call" | custom-call | flops 1700000000 | bytes 10000000 | tf_op jit(solution)/shard_map/ffn/pallas_call | solution.py:328
  143.6 2.3 %collective-permute-start.8 = (bf16[96,2048]{1,0:T(8,128)(2,1)}, bf16[96,2048]{1,0:T(8,128)(2,1)S(1)}, u32[]{:S(2)}, u32[]{:S(2)}) collective-permute-start(bf16[96,2048]{1,0:T(8,128)(2,1)} %get-tuple-element.20), channel_id=1, source_target_pairs={{0,1},{1,0},{2,3},{3,2},{4,5},{5,4},{6,7},{7,6},{8,9},{9,8},{10,11... | collective-permute-start | bytes 1179656 | tf_op jit(solution)/shard_map/ppermute | solution.py:351
  145.9 1.5 collective-permute-done.8
  147.4 1.1 add_convert_fusion
  148.5 10.2 %all_to_all.23 = bf16[4,24,2048]{2,1,0:T(8,128)(2,1)S(1)} all-to-all(bf16[4,24,2048]{2,1,0:T(8,128)(2,1)S(1)} %bitcast.14), channel_id=1, replica_groups=mesh['z'=8,'y'=8,'x'=4,'c'=2] {'x'}, dimensions={0} | all-to-all | bytes 786432 | tf_op jit(solution)/shard_map/all_to_all | solution.py:354
  158.9 0.8 add_convert_fusion.2
  (44 shorter events, 1.9 us)
Async XLA Ops:
  6.5 130.1 %all-gather.2.cloned.1.call-start = ((), (), s32[]{:S(2)}) async-start(), calls=%async_computation.4 | async-start | bytes 9052160 | tf_op jit(solution)/shard_map/all_gather | solution.py:383
  34.0 30.9 %collective-permute-start = (bf16[8,224,128]{2,1,0:T(8,128)(2,1)S(1)}, bf16[8,224,128]{2,1,0:T(8,128)(2,1)S(1)}, u32[]{:S(2)}, u32[]{:S(2)}) collective-permute-start(bf16[8,224,128]{2,1,0:T(8,128)(2,1)S(1)} %all_to_all.20.kv0), channel_id=1, source_target_pairs={{0,448},{448,0},{128,64},{64,128},{256,192},{192,256},{384,320},{3... | collective-permute-start | bytes 1376264 | tf_op jit(solution)/shard_map/ppermute | solution.py:387
  46.3 10.7 %collective-permute-start.2 = (bf16[192,256]{1,0:T(8,128)(2,1)}, bf16[192,256]{1,0:T(8,128)(2,1)S(1)}, u32[]{:S(2)}, u32[]{:S(2)}) collective-permute-start(bf16[192,256]{1,0:T(8,128)(2,1)} %q0.1), channel_id=1, source_target_pairs={{0,256},{128,384},{256,0},{384,128},{448,192},{64,320},{192,448},{... | collective-permute-start | bytes 294920 | tf_op jit(solution)/shard_map/ppermute | solution.py:384
  48.2 9.1 %collective-permute-start.1 = (bf16[192,256]{1,0:T(8,128)(2,1)}, bf16[192,256]{1,0:T(8,128)(2,1)S(1)}, u32[]{:S(2)}, u32[]{:S(2)}) collective-permute-start(bf16[192,256]{1,0:T(8,128)(2,1)} %q0.1), channel_id=1, source_target_pairs={{0,128},{128,256},{256,384},{384,0},{448,64},{64,192},{192,320},{3... | collective-permute-start | bytes 294920 | tf_op jit(solution)/shard_map/ppermute | solution.py:384
  52.2 12.7 %collective-permute-start.3 = (bf16[192,256]{1,0:T(8,128)(2,1)}, bf16[192,256]{1,0:T(8,128)(2,1)S(1)}, u32[]{:S(2)}, u32[]{:S(2)}) collective-permute-start(bf16[192,256]{1,0:T(8,128)(2,1)} %q0.1), channel_id=1, source_target_pairs={{0,384},{128,0},{256,128},{384,256},{448,320},{64,448},{192,64},{3... | collective-permute-start | bytes 294920 | tf_op jit(solution)/shard_map/ppermute | solution.py:384
  64.9 0.7 copy-start.2
  65.6 0.9 copy-start.3
  66.5 38.0 %copy-start = (bf16[256,2048]{1,0:T(8,128)(2,1)S(1)}, bf16[256,2048]{1,0:T(8,128)(2,1)}, u32[]{:S(2)}) copy-start(bf16[256,2048]{1,0:T(8,128)(2,1)} %weight.1) | copy-start | bytes 3145732
  66.5 38.0 %copy-start.1 = (bf16[192,256]{1,0:T(8,128)(2,1)S(1)}, bf16[192,256]{1,0:T(8,128)(2,1)}, u32[]{:S(2)}) copy-start(bf16[192,256]{1,0:T(8,128)(2,1)} %gates.1) | copy-start | bytes 294916
  66.5 55.9 %copy-start.4 = (bf16[24,2048]{1,0:T(8,128)(2,1)S(1)}, bf16[24,2048]{1,0:T(8,128)(2,1)}, u32[]{:S(2)}) copy-start(bf16[24,2048]{1,0:T(8,128)(2,1)} %param.13) | copy-start | bytes 294916
  66.5 55.9 %copy-start.5 = (f32[2048]{0:T(1024)S(1)}, f32[2048]{0:T(1024)}, u32[]{:S(2)}) copy-start(f32[2048]{0:T(1024)} %param.20) | copy-start | bytes 24580
  66.5 56.2 %copy-start.7 = (f32[2048]{0:T(1024)S(1)}, f32[2048]{0:T(1024)}, u32[]{:S(2)}) copy-start(f32[2048]{0:T(1024)} %param.21) | copy-start | bytes 24580
  74.1 18.5 %collective-permute-start.4 = (bf16[72,768]{1,0:T(8,128)(2,1)S(1)}, bf16[72,768]{1,0:T(8,128)(2,1)S(1)}, u32[]{:S(2)}, u32[]{:S(2)}) collective-permute-start(bf16[72,768]{1,0:T(8,128)(2,1)S(1)} %get-tuple-element.14), channel_id=1, source_target_pairs={{0,384},{128,0},{256,128},{384,256},{448,320},{64,448},{192,64},{3... | collective-permute-start | bytes 331784 | tf_op jit(solution)/shard_map/ppermute | solution.py:393
  77.7 21.5 %collective-permute-start.5 = (bf16[72,768]{1,0:T(8,128)(2,1)S(1)}, bf16[72,768]{1,0:T(8,128)(2,1)S(1)}, u32[]{:S(2)}, u32[]{:S(2)}) collective-permute-start(bf16[72,768]{1,0:T(8,128)(2,1)S(1)} %get-tuple-element.15), channel_id=1, source_target_pairs={{0,256},{128,384},{256,0},{384,128},{448,192},{64,320},{192,448},{... | collective-permute-start | bytes 331784 | tf_op jit(solution)/shard_map/ppermute | solution.py:393
  90.7 13.8 %collective-permute-start.6 = (bf16[72,768]{1,0:T(8,128)(2,1)S(1)}, bf16[72,768]{1,0:T(8,128)(2,1)S(1)}, u32[]{:S(2)}, u32[]{:S(2)}) collective-permute-start(bf16[72,768]{1,0:T(8,128)(2,1)S(1)} %get-tuple-element.16), channel_id=1, source_target_pairs={{0,128},{128,256},{256,384},{384,0},{448,64},{64,192},{192,320},{3... | collective-permute-start | bytes 331784 | tf_op jit(solution)/shard_map/ppermute | solution.py:393
  105.1 3.6 %collective-permute-start.7 = (bf16[96,2048]{1,0:T(8,128)(2,1)S(1)}, bf16[96,2048]{1,0:T(8,128)(2,1)S(1)}, u32[]{:S(2)}, u32[]{:S(2)}) collective-permute-start(bf16[96,2048]{1,0:T(8,128)(2,1)S(1)} %get-tuple-element.18), channel_id=1, source_target_pairs={{0,1},{1,0},{2,3},{3,2},{4,5},{5,4},{6,7},{7,6},{8,9},{9,8},{10,11... | collective-permute-start | bytes 1179656 | tf_op jit(solution)/shard_map/ppermute | solution.py:351
  108.7 50.2 %copy-start.6 = (f32[2048]{0:T(1024)S(1)}, f32[2048]{0:T(1024)}, u32[]{:S(2)}) copy-start(f32[2048]{0:T(1024)} %param.22) | copy-start | bytes 24580
  143.6 3.8 %collective-permute-start.8 = (bf16[96,2048]{1,0:T(8,128)(2,1)}, bf16[96,2048]{1,0:T(8,128)(2,1)S(1)}, u32[]{:S(2)}, u32[]{:S(2)}) collective-permute-start(bf16[96,2048]{1,0:T(8,128)(2,1)} %get-tuple-element.20), channel_id=1, source_target_pairs={{0,1},{1,0},{2,3},{3,2},{4,5},{5,4},{6,7},{7,6},{8,9},{9,8},{10,11... | collective-permute-start | bytes 1179656 | tf_op jit(solution)/shard_map/ppermute | solution.py:351
Sparse Core Ops, SparseCore 0:
  10.3 121.0 all-gather.1

commit v6 on v5

--- a/solution.py
+++ b/solution.py
@@ -35,13 +35,6 @@
 NT = (((1,), (1,)), ((), ()))
 
 
-def pieces(value):
-    one = lax.reduce_precision(value, 8, 7)
-    rest = value - one
-    two = lax.reduce_precision(rest, 8, 7)
-    return one, two, rest - two
-
-
 def kernel_pieces(value):
     one = value.astype(BF16).astype(F32)
     rest = value - one
@@ -49,16 +42,29 @@
     return one, two, rest - two
 
 
-def key_payload(keys, values, log_gates):
-    k32 = keys.astype(F32)
-    norm = jnp.sqrt(jnp.max(jnp.sum(k32 * k32, axis=1))) * 1.01
-    parts = jnp.concatenate(pieces(log_gates), axis=1).T
-    ones = jnp.ones((3, ROWS), F32)
-    last = jnp.full((1, ROWS), norm, F32)
-    side = jnp.concatenate([parts, ones, last], axis=0).astype(BF16)
-    left = side[:, :128]
-    right = jnp.pad(side[:, 128:], ((0, 0), (0, 64)))
-    return jnp.concatenate([jnp.concatenate([keys, values], axis=1), left, right], axis=0)
+def payload_kernel(keys, values, gates, out):
+    k32 = keys[...].astype(F32)
+    norm = jnp.max(jnp.sum(k32 * k32, axis=0, keepdims=True), axis=1, keepdims=True)
+    norm = jnp.sqrt(norm) * 1.01
+    rows = jnp.concatenate([k32, values[...].astype(F32)], axis=0).T.astype(BF16)
+    line = lax.broadcasted_iota(jnp.int32, (16, ROWS), 0)
+    side = jnp.concatenate([*kernel_pieces(gates[...]), jnp.ones((HL, ROWS), F32)], axis=0)
+    side = jnp.where(line == 15, norm, side)
+    left = side[:, 0:128].astype(BF16)
+    right = jnp.concatenate([side[:, 128:], jnp.zeros((16, 64), F32)], axis=1).astype(BF16)
+    for n in range(YS):
+        out[n, 0:ROWS, :] = rows
+        out[n, ROWS : ROWS + 16, :] = left
+        out[n, ROWS + 16 : KP, :] = right
+
+
+def payload(keys, values, gates):
+    return pl.pallas_call(
+        payload_kernel,
+        out_shape=jax.ShapeDtypeStruct((YS, KP, 128), BF16),
+        cost_estimate=pl.CostEstimate(flops=100_000, bytes_accessed=500_000, transcendentals=0),
+        name="payload",
+    )(keys, values, gates)
 
 
 def grid_z(zh, zl):
@@ -69,7 +75,7 @@
     return z
 
 
-def attention_kernel(pos, kv0, kv1, q0, q1, q2, q3, own, o0, o1, o2, o3, kc, vt, qt, acc, ls, ms):
+def attention_kernel(pos, kv0, kv1, q0, q1, q2, q3, o0, o1, o2, o3, kc, vt, qt, acc, ls, ms):
     kv = (kv0, kv1)
     q = (q0, q1, q2, q3)
     out = (o0, o1, o2, o3)
@@ -100,13 +106,17 @@
     line = lax.broadcasted_iota(jnp.int32, (16, QR), 0)
     chosen = jnp.where((line < 3 * HL) & (line % HL == head), -1.0, 0.0)
     qmax = jnp.zeros((1, 1), F32)
-    owned = jnp.concatenate([own[h : h + 1, :] for h in range(HL)], axis=1)
+    left = kv0[y, ROWS : ROWS + 16, :].astype(F32)
+    right = kv0[y, ROWS + 16 : KP, :].astype(F32)[:, 0:64]
+    owned = jnp.concatenate([left, right], axis=1)
+    owned = owned[0:4] + owned[4:8] + owned[8:12]
+    owned = jnp.concatenate([owned[h : h + 1] for h in range(HL)], axis=1)
     for j in range(QG):
         asked = grid_z(zh, (zl + QG - j) % QG)
         last = jnp.where(asked > upper, 1 - low_at, low_at)
         ends = [rows[YS - 1, 208:224, :].astype(F32)[:, 63:64] for rows in kv]
         ends = jnp.where(last == 0, ends[0], ends[1])
-        turned = (q[j][...].astype(F32) * 0.125).T
+        turned = q[j][...].astype(F32).T
         turned = jnp.concatenate([turned[h * HD : (h + 1) * HD] for h in range(HL)], axis=1)
         norm = jnp.sqrt(jnp.sum(turned * turned, axis=0, keepdims=True))
         qmax = jnp.maximum(qmax, jnp.max(norm, axis=1, keepdims=True))
@@ -208,7 +218,7 @@
     return pl.pallas_call(
         attention_kernel,
         out_shape=[jax.ShapeDtypeStruct((OUTR, QR), BF16)] * QG,
-        in_specs=[pl.BlockSpec(memory_space=pltpu.SMEM)] + [vmem] * (QG + 3),
+        in_specs=[pl.BlockSpec(memory_space=pltpu.SMEM)] + [vmem] * (QG + 2),
         out_specs=[vmem] * QG,
         scratch_shapes=[
             pltpu.VMEM((NB * ROWS, 256), BF16),
@@ -238,7 +248,7 @@
     for j in range(QG):
         stats = parts[j][HD:OUTR, :].astype(F32)
         sums.append(stats[0:1] + stats[1:2] + stats[2:3])
-        tops.append(stats[3:4] + stats[4:5] + stats[5:6])
+        tops.append(jnp.where(sums[j] > 0.0, stats[3:4] + stats[4:5] + stats[5:6], LOW))
     top = tops[0]
     for j in range(1, QG):
         top = jnp.maximum(top, tops[j])
@@ -375,22 +385,30 @@
     up_weight,
     down_weight,
 ):
-    def turn(r):
-        return [(row[i], row[(i + r) % QG]) for row in ZGRID for i in range(QG)]
-
+    pairs = [(row, i, (i + r) % QG, r) for row in ZGRID for i in range(QG) for r in range(1, QG)]
+    partner = {a: b for column in zip(*ZGRID) for a, b in (column, column[::-1])}
+    asks = [(row[i], row[k], r) for row, i, k, r in pairs if row[i] > min(row[k], partner[row[k]])]
+
+    def ask(r):
+        return [(q, k) for q, k, turn in asks if turn == r]
+
+    def answer(r):
+        return [(k, q) for q, k, turn in asks if turn == r]
+
+    swap = [(partner[d], d) for row in ZGRID for d in row if max(row) > partner[d]]
     pad = jnp.zeros((gate_weight.shape[0], WC - GU - FFL), BF16)
     packed = jnp.concatenate([gate_weight, up_weight, down_weight.T, pad], axis=1)
     weights = lax.all_gather(packed, SP, axis=0, tiled=True)
-    q_all = [queries] + [lax.ppermute(queries, "z", turn(r)) for r in range(1, QG)]
-    held = copies(key_payload(keys, values, log_gates), "y")
-    swap = [pair for column in zip(*ZGRID) for pair in (column, column[::-1])]
+    scaled = queries * jnp.asarray(HD**-0.5, BF16)
+    q_all = [scaled] + [lax.ppermute(scaled, "z", ask(r)) for r in range(1, QG)]
+    held = lax.all_to_all(payload(keys.T, values.T, log_gates.T), "y", 0, 0, tiled=True)
     lent = lax.ppermute(held, "z", swap)
     z = lax.axis_index("z")
     zh = sum(jnp.where(z == ZGRID[a][b], a, 0) for a in range(ZH) for b in range(QG))
     zl = sum(jnp.where(z == ZGRID[a][b], b, 0) for a in range(ZH) for b in range(QG))
     pos = jnp.stack([zh, zl, lax.axis_index("y")]).astype(jnp.int32)
-    parts = attention(pos, held, lent, *q_all, log_gates.T)
-    parts = [parts[0]] + [lax.ppermute(parts[r], "z", turn(QG - r)) for r in range(1, QG)]
+    parts = attention(pos, held, lent, *q_all)
+    parts = [parts[0]] + [lax.ppermute(parts[r], "z", answer(r)) for r in range(1, QG)]
     core = lax.axis_index("c").astype(jnp.int32)[None]
     projected = sum_at_owner(*merge(core, parts, out_gate, out_weight))
     mixed = resid.astype(F32) + rms_scale(projected, post_gain)

time: 167 us -> 158 us (0.946)
  starting transfers between devices: 44.3 us -> 40.4 us
  blocking collectives: 58.9 us -> 56.6 us
  other arithmetic: 5.79 us -> 3.65 us
  local copies, waits for them, and re-layouts: 3.79 us -> 1.67 us
    all_to_all x2 -> x1, blocking collectives: 30.1 us -> 9.29 us  [copies(): return lax.all_to_all(sent, axis, 0, 0, tiled=True)]
    all_to_all x0 -> x1, blocking collectives: none -> 20.5 us  [shards(): lax.all_to_all(payload(keys.T, values.T, log_gates.T), 'y', 0, 0, tiled=T...]
    ppermute x6, starting transfers between devices: 27.8 us -> 13.8 us  [the longest x3 9.88 us: shards(): lax.ppermute(parts[r], 'z', answer(r))]
    ppermute x2, starting transfers between devices: 4.21 us -> 14 us  [sum_at_owner(): given = lax.ppermute(theirs, 'c', [(0, 1), (1, 0)])]
    all_gather x1, waiting for transfers between devices: 0.01 us -> 5.53 us  [shards(): weights = lax.all_gather(packed, SP, axis=0, tiled=True)]
    ppermute x6, waiting for transfers between devices: 21 us -> 16.4 us  [the longest x3 12.3 us: shards(): q_all = [scaled] + [lax.ppermute(scaled, 'z', ask(r)) for r in range(1, QG)]]
    pallas_call x0 -> x1, Pallas kernels: none -> 1.74 us  [payload(): pl.pallas_call(payload_kernel, out_shape=jax.ShapeDtypeStruct((YS, KP, 12...]
    unnamed x17 -> x12, local copies, waits for them, and re-layouts: 1.7 us -> 0.02 us
  transfers between devices with their start and end apart: 10 -> 10, of which waited for: 7 -> 6; matrix products, arithmetic and copies ran while one was open for 3% -> 1% of each run, Pallas kernels for 5% -> 6%
where the time goes in v6:
time: 158 us; the launch traced here: 157 us
  blocking collectives  56.6 us (36%)
  starting transfers between devices  40.4 us (26%)
  waiting for transfers between devices  24.8 us (16%)
  Pallas kernels  16.6 us (11%)
  between operations  13.6 us (9%)
  other arithmetic  3.65 us (2%)
  local copies, waits for them, and re-layouts  1.67 us (1%)
    all_to_all x2, blocking collectives, sum_at_owner(): arrived = lax.all_to_all(blocks, 'x', 0, 0, tiled=True)  22.4 us
    all_to_all x1, blocking collectives, shards(): lax.all_to_all(payload(keys.T, values.T, log_gates.T), 'y', 0, 0, tiled=T...  20.5 us
    ppermute x2, starting transfers between devices, sum_at_owner(): given = lax.ppermute(theirs, 'c', [(0, 1), (1, 0)])  14 us
    ppermute x1, starting transfers between devices, shards(): lent = lax.ppermute(held, 'z', swap)  12.7 us
    ppermute x3, waiting for transfers between devices, shards(): q_all = [scaled] + [lax.ppermute(scaled, 'z', ask(r)) for r in range(1, QG)]  12.3 us
    ppermute x3, starting transfers between devices, shards(): lax.ppermute(parts[r], 'z', answer(r))  9.88 us
    all_to_all x1, blocking collectives, copies(): return lax.all_to_all(sent, axis, 0, 0, tiled=True)  9.29 us
    pallas_call x1, Pallas kernels, attention(): pl.pallas_call(attention_kernel, out_shape=[jax.ShapeDtypeStruct((OUTR, Q...  7.28 us
  transfers between devices with their start and end apart: 10, of which 6 were waited for; matrix products, arithmetic and copies ran while one was open for 1% of the time, Pallas kernels for 6%

profile of v6, /device:TPU:1, one launch (start us, length us, event | category | flops | bytes accessed | tf_op | source)
XLA Modules:
  0.0 157.3 jit_solution(4504057698957220257)
XLA Ops:
  6.5 1.6 %concatenate.3 = bf16[32,2176]{1,0:T(8,128)(2,1)} concatenate(bf16[32,704]{1,0:T(8,128)(2,1)} %param.23, bf16[32,704]{1,0:T(8,128)(2,1)} %param.24, bf16[32,704]{1,0:T(8,128)(2,1)} %bitcast.14, bf16[32,64]{1,0:T(8,128)(2,1)S(1)} %broadcast_in_dim.8), dimensions={1} | concatenate | bytes 278528 | tf_op jit(solution)/shard_map/concatenate | solution.py:400
  8.2 1.7 %payload.1 = bf16[8,224,128]{2,1,0:T(8,128)(2,1)} custom-call(bf16[64,192]{1,0:T(8,128)(2,1)} %bitcast.15, bf16[64,192]{1,0:T(8,128)(2,1)} %bitcast.16, f32[4,192]{1,0:T(4,128)} %bitcast.17), custom_call_target="tpu_custom_call" | custom-call | flops 100000 | bytes 500000 | tf_op jit(solution)/shard_map/payload/pallas_call | solution.py:62
  9.9 20.5 %all_to_all.20.kv0 = bf16[8,224,128]{2,1,0:T(8,128)(2,1)S(1)} all-to-all(bf16[8,224,128]{2,1,0:T(8,128)(2,1)} %payload.1), channel_id=1, replica_groups=mesh['z'=8,'y'=8,'x'=4,'c'=2] {'y'}, dimensions={0} | all-to-all | bytes 917504 | tf_op jit(solution)/shard_map/all_to_all | solution.py:404
  30.4 12.7 %collective-permute-start = (bf16[8,224,128]{2,1,0:T(8,128)(2,1)S(1)}, bf16[8,224,128]{2,1,0:T(8,128)(2,1)S(1)}, u32[]{:S(2)}, u32[]{:S(2)}) collective-permute-start(bf16[8,224,128]{2,1,0:T(8,128)(2,1)S(1)} %all_to_all.20.kv0), channel_id=1, source_target_pairs={{64,128},{192,256},{320,384},{0,448},{128,64},{256,192},{384,320},... | collective-permute-start | bytes 1376264 | tf_op jit(solution)/shard_map/ppermute | solution.py:405
  43.1 0.9 broadcast_multiply_fusion.q0
  44.0 1.3 collective-permute-start.3
  45.3 1.3 collective-permute-start.2
  46.6 1.3 collective-permute-start.1
  48.0 8.4 %collective-permute-done.3.q3 = bf16[192,256]{1,0:T(8,128)(2,1)S(1)} collective-permute-done((bf16[192,256]{1,0:T(8,128)(2,1)S(1)}, bf16[192,256]{1,0:T(8,128)(2,1)S(1)}, u32[]{:S(2)}, u32[]{:S(2)}) %collective-permute-start.3) | collective-permute-done | bytes 98336 | tf_op jit(solution)/shard_map/ppermute | solution.py:403
  56.5 3.8 %collective-permute-done.1.q1 = bf16[192,256]{1,0:T(8,128)(2,1)S(1)} collective-permute-done((bf16[192,256]{1,0:T(8,128)(2,1)S(1)}, bf16[192,256]{1,0:T(8,128)(2,1)S(1)}, u32[]{:S(2)}, u32[]{:S(2)}) %collective-permute-start.1) | collective-permute-done | bytes 98336 | tf_op jit(solution)/shard_map/ppermute | solution.py:403
  60.3 7.3 %attention.1 = (bf16[72,768]{1,0:T(8,128)(2,1)S(1)}, bf16[72,768]{1,0:T(8,128)(2,1)S(1)}, bf16[72,768]{1,0:T(8,128)(2,1)S(1)}, bf16[72,768]{1,0:T(8,128)(2,1)S(1)}) custom-call(s32[3]{0:T(128)S(1)} %pad_add_fusion.pos, bf16[8,224,128]{2,1,0:T(8,128)(2,1)S(1)} %all_to_all.20.kv0, bf16[8,224,128]{2,1,0:T(8,128)(2,1)S(1)} %collective-permute-done.kv1, ...), custom_call_target="tpu_custom_call" | custom-call | flops 12000000000 | bytes 4000000 | tf_op jit(solution)/shard_map/attention/pallas_call | solution.py:218
  67.6 1.3 collective-permute-start.4
  68.9 5.4 %collective-permute-start.5 = (bf16[72,768]{1,0:T(8,128)(2,1)S(1)}, bf16[72,768]{1,0:T(8,128)(2,1)S(1)}, u32[]{:S(2)}, u32[]{:S(2)}) collective-permute-start(bf16[72,768]{1,0:T(8,128)(2,1)S(1)} %get-tuple-element.15), channel_id=1, source_target_pairs={{0,256},{128,384},{192,448},{448,192},{64,320},{1,257},{129,385},{... | collective-permute-start | bytes 331784 | tf_op jit(solution)/shard_map/ppermute | solution.py:411
  74.3 3.2 %collective-permute-start.6 = (bf16[72,768]{1,0:T(8,128)(2,1)S(1)}, bf16[72,768]{1,0:T(8,128)(2,1)S(1)}, u32[]{:S(2)}, u32[]{:S(2)}) collective-permute-start(bf16[72,768]{1,0:T(8,128)(2,1)S(1)} %get-tuple-element.16), channel_id=1, source_target_pairs={{0,128},{128,256},{256,384},{320,448},{448,64},{64,192},{192,320},... | collective-permute-start | bytes 331784 | tf_op jit(solution)/shard_map/ppermute | solution.py:411
  77.5 4.1 %collective-permute-done.6.p3 = bf16[72,768]{1,0:T(8,128)(2,1)S(1)} collective-permute-done((bf16[72,768]{1,0:T(8,128)(2,1)S(1)}, bf16[72,768]{1,0:T(8,128)(2,1)S(1)}, u32[]{:S(2)}, u32[]{:S(2)}) %collective-permute-start.6) | collective-permute-done | bytes 110624 | tf_op jit(solution)/shard_map/ppermute | solution.py:411
  81.6 0.6 merge.1
  82.2 11.4 %collective-permute-start.7 = (bf16[96,2048]{1,0:T(8,128)(2,1)S(1)}, bf16[96,2048]{1,0:T(8,128)(2,1)S(1)}, u32[]{:S(2)}, u32[]{:S(2)}) collective-permute-start(bf16[96,2048]{1,0:T(8,128)(2,1)S(1)} %get-tuple-element.18), channel_id=1, source_target_pairs={{0,1},{1,0},{2,3},{3,2},{4,5},{5,4},{6,7},{7,6},{8,9},{9,8},{10,11... | collective-permute-start | bytes 1179656 | tf_op jit(solution)/shard_map/ppermute | solution.py:361
  93.7 1.3 collective-permute-done.7
  95.1 11.1 %all_to_all.21 = bf16[4,24,2048]{2,1,0:T(8,128)(2,1)S(1)} all-to-all(bf16[4,24,2048]{2,1,0:T(8,128)(2,1)S(1)} %bitcast.11), channel_id=1, replica_groups=mesh['z'=8,'y'=8,'x'=4,'c'=2] {'x'}, dimensions={0} | all-to-all | bytes 786432 | tf_op jit(solution)/shard_map/all_to_all | solution.py:364
  106.3 0.1 multiply_reduce_fusion.2
  106.4 0.2 multiply_reduce_fusion.1
  106.7 0.1 multiply_convert_fusion
  106.8 9.3 %all_to_all.22 = bf16[4,24,2048]{2,1,0:T(8,128)(2,1)S(1)} all-to-all(bf16[4,24,2048]{2,1,0:T(8,128)(2,1)S(1)} %broadcast_in_dim.7), channel_id=1, replica_groups=mesh['z'=8,'y'=8,'x'=4,'c'=2] {'x'}, dimensions={0} | all-to-all | bytes 786432 | tf_op jit(solution)/shard_map/all_to_all | solution.py:357
  116.1 4.4 %all_gather.6.rows = bf16[192,2048]{1,0:T(8,128)(2,1)} all-gather(bf16[96,2048]{1,0:T(8,128)(2,1)S(1)} %bitcast.13), channel_id=1, replica_groups=mesh['z'=8,'y'=8,'x'=4,'c'=2] {'c'}, dimensions={0}, use_global_device_ids=true | all-gather | bytes 1179648 | tf_op jit(solution)/shard_map/all_gather | solution.py:417
  120.5 5.5 %all-gather.2.cloned.1.call-done.weights = bf16[2048,2176]{1,0:T(8,128)(2,1)} async-done(((bf16[32,2176]{1,0:T(8,128)(2,1)}), bf16[2048,2176]{1,0:T(8,128)(2,1)}) %all-gather.2.cloned.1.call-update) | async-done | bytes 8912912 | tf_op jit(solution)/shard_map/all_gather | solution.py:401
  126.1 7.0 %ffn.1 = (bf16[96,2048]{1,0:T(8,128)(2,1)}, bf16[96,2048]{1,0:T(8,128)(2,1)}) custom-call(s32[1]{0:T(128)} %bitcast.core, bf16[192,2048]{1,0:T(8,128)(2,1)} %all_gather.6.rows, bf16[2048,2176]{1,0:T(8,128)(2,1)} %all-gather.2.cloned.1.call-done.weights), custom_call_target="tpu_custom_call" | custom-call | flops 1700000000 | bytes 10000000 | tf_op jit(solution)/shard_map/ffn/pallas_call | solution.py:338
  133.0 2.5 %collective-permute-start.8 = (bf16[96,2048]{1,0:T(8,128)(2,1)}, bf16[96,2048]{1,0:T(8,128)(2,1)S(1)}, u32[]{:S(2)}, u32[]{:S(2)}) collective-permute-start(bf16[96,2048]{1,0:T(8,128)(2,1)} %get-tuple-element.20), channel_id=1, source_target_pairs={{0,1},{1,0},{2,3},{3,2},{4,5},{5,4},{6,7},{7,6},{8,9},{9,8},{10,11... | collective-permute-start | bytes 1179656 | tf_op jit(solution)/shard_map/ppermute | solution.py:361
  135.6 1.5 collective-permute-done.8
  137.1 1.1 add_convert_fusion
  138.2 11.3 %all_to_all.23 = bf16[4,24,2048]{2,1,0:T(8,128)(2,1)S(1)} all-to-all(bf16[4,24,2048]{2,1,0:T(8,128)(2,1)S(1)} %bitcast.12), channel_id=1, replica_groups=mesh['z'=8,'y'=8,'x'=4,'c'=2] {'x'}, dimensions={0} | all-to-all | bytes 786432 | tf_op jit(solution)/shard_map/all_to_all | solution.py:364
  149.6 0.1 multiply_reduce_fusion
  149.7 0.8 add_convert_fusion.2
  (27 shorter events, 0.4 us)
Async XLA Ops:
  6.5 119.5 %all-gather.2.cloned.1.call-start = ((), (), s32[]{:S(2)}) async-start(), calls=%async_computation.4 | async-start | bytes 9052160 | tf_op jit(solution)/shard_map/all_gather | solution.py:401
  30.4 29.9 %collective-permute-start = (bf16[8,224,128]{2,1,0:T(8,128)(2,1)S(1)}, bf16[8,224,128]{2,1,0:T(8,128)(2,1)S(1)}, u32[]{:S(2)}, u32[]{:S(2)}) collective-permute-start(bf16[8,224,128]{2,1,0:T(8,128)(2,1)S(1)} %all_to_all.20.kv0), channel_id=1, source_target_pairs={{64,128},{192,256},{320,384},{0,448},{128,64},{256,192},{384,320},... | collective-permute-start | bytes 1376264 | tf_op jit(solution)/shard_map/ppermute | solution.py:405
  44.0 12.5 %collective-permute-start.3 = (bf16[192,256]{1,0:T(8,128)(2,1)S(1)}, bf16[192,256]{1,0:T(8,128)(2,1)S(1)}, u32[]{:S(2)}, u32[]{:S(2)}) collective-permute-start(bf16[192,256]{1,0:T(8,128)(2,1)S(1)} %broadcast_multiply_fusion.q0), channel_id=1, source_target_pairs={{128,0},{256,128},{384,256},{448,320},{64,448},{192,64},{320,192},... | collective-permute-start | bytes 294920 | tf_op jit(solution)/shard_map/ppermute | solution.py:403
  45.3 11.2 %collective-permute-start.2 = (bf16[192,256]{1,0:T(8,128)(2,1)S(1)}, bf16[192,256]{1,0:T(8,128)(2,1)S(1)}, u32[]{:S(2)}, u32[]{:S(2)}) collective-permute-start(bf16[192,256]{1,0:T(8,128)(2,1)S(1)} %broadcast_multiply_fusion.q0), channel_id=1, source_target_pairs={{256,0},{384,128},{448,192},{192,448},{320,64},{257,1},{385,129},{... | collective-permute-start | bytes 294920 | tf_op jit(solution)/shard_map/ppermute | solution.py:403
  46.6 13.7 %collective-permute-start.1 = (bf16[192,256]{1,0:T(8,128)(2,1)S(1)}, bf16[192,256]{1,0:T(8,128)(2,1)S(1)}, u32[]{:S(2)}, u32[]{:S(2)}) collective-permute-start(bf16[192,256]{1,0:T(8,128)(2,1)S(1)} %broadcast_multiply_fusion.q0), channel_id=1, source_target_pairs={{384,0},{448,64},{320,448},{385,1},{449,65},{321,449},{386,2},{450... | collective-permute-start | bytes 294920 | tf_op jit(solution)/shard_map/ppermute | solution.py:403
  48.0 33.6 %copy-start = (bf16[256,2048]{1,0:T(8,128)(2,1)S(1)}, bf16[256,2048]{1,0:T(8,128)(2,1)}, u32[]{:S(2)}) copy-start(bf16[256,2048]{1,0:T(8,128)(2,1)} %weight.1) | copy-start | bytes 3145732
  48.0 33.6 %copy-start.1 = (bf16[192,256]{1,0:T(8,128)(2,1)S(1)}, bf16[192,256]{1,0:T(8,128)(2,1)}, u32[]{:S(2)}) copy-start(bf16[192,256]{1,0:T(8,128)(2,1)} %gates.1) | copy-start | bytes 294916
  48.0 58.4 %copy-start.2 = (bf16[24,2048]{1,0:T(8,128)(2,1)S(1)}, bf16[24,2048]{1,0:T(8,128)(2,1)}, u32[]{:S(2)}) copy-start(bf16[24,2048]{1,0:T(8,128)(2,1)} %param.13) | copy-start | bytes 294916
  48.0 58.4 %copy-start.3 = (f32[2048]{0:T(1024)S(1)}, f32[2048]{0:T(1024)}, u32[]{:S(2)}) copy-start(f32[2048]{0:T(1024)} %param.20) | copy-start | bytes 24580
  48.0 58.7 %copy-start.5 = (f32[2048]{0:T(1024)S(1)}, f32[2048]{0:T(1024)}, u32[]{:S(2)}) copy-start(f32[2048]{0:T(1024)} %param.21) | copy-start | bytes 24580
  67.6 9.9 %collective-permute-start.4 = (bf16[72,768]{1,0:T(8,128)(2,1)S(1)}, bf16[72,768]{1,0:T(8,128)(2,1)S(1)}, u32[]{:S(2)}, u32[]{:S(2)}) collective-permute-start(bf16[72,768]{1,0:T(8,128)(2,1)S(1)} %get-tuple-element.14), channel_id=1, source_target_pairs={{0,384},{64,448},{448,320},{1,385},{65,449},{449,321},{2,386},{66,... | collective-permute-start | bytes 331784 | tf_op jit(solution)/shard_map/ppermute | solution.py:411
  68.9 8.6 %collective-permute-start.5 = (bf16[72,768]{1,0:T(8,128)(2,1)S(1)}, bf16[72,768]{1,0:T(8,128)(2,1)S(1)}, u32[]{:S(2)}, u32[]{:S(2)}) collective-permute-start(bf16[72,768]{1,0:T(8,128)(2,1)S(1)} %get-tuple-element.15), channel_id=1, source_target_pairs={{0,256},{128,384},{192,448},{448,192},{64,320},{1,257},{129,385},{... | collective-permute-start | bytes 331784 | tf_op jit(solution)/shard_map/ppermute | solution.py:411
  74.3 7.3 %collective-permute-start.6 = (bf16[72,768]{1,0:T(8,128)(2,1)S(1)}, bf16[72,768]{1,0:T(8,128)(2,1)S(1)}, u32[]{:S(2)}, u32[]{:S(2)}) collective-permute-start(bf16[72,768]{1,0:T(8,128)(2,1)S(1)} %get-tuple-element.16), channel_id=1, source_target_pairs={{0,128},{128,256},{256,384},{320,448},{448,64},{64,192},{192,320},... | collective-permute-start | bytes 331784 | tf_op jit(solution)/shard_map/ppermute | solution.py:411
  82.2 12.8 %collective-permute-start.7 = (bf16[96,2048]{1,0:T(8,128)(2,1)S(1)}, bf16[96,2048]{1,0:T(8,128)(2,1)S(1)}, u32[]{:S(2)}, u32[]{:S(2)}) collective-permute-start(bf16[96,2048]{1,0:T(8,128)(2,1)S(1)} %get-tuple-element.18), channel_id=1, source_target_pairs={{0,1},{1,0},{2,3},{3,2},{4,5},{5,4},{6,7},{7,6},{8,9},{9,8},{10,11... | collective-permute-start | bytes 1179656 | tf_op jit(solution)/shard_map/ppermute | solution.py:361
  95.0 54.7 %copy-start.4 = (f32[2048]{0:T(1024)S(1)}, f32[2048]{0:T(1024)}, u32[]{:S(2)}) copy-start(f32[2048]{0:T(1024)} %param.22) | copy-start | bytes 24580
  133.0 4.1 %collective-permute-start.8 = (bf16[96,2048]{1,0:T(8,128)(2,1)}, bf16[96,2048]{1,0:T(8,128)(2,1)S(1)}, u32[]{:S(2)}, u32[]{:S(2)}) collective-permute-start(bf16[96,2048]{1,0:T(8,128)(2,1)} %get-tuple-element.20), channel_id=1, source_target_pairs={{0,1},{1,0},{2,3},{3,2},{4,5},{5,4},{6,7},{7,6},{8,9},{9,8},{10,11... | collective-permute-start | bytes 1179656 | tf_op jit(solution)/shard_map/ppermute | solution.py:361
Sparse Core Ops, SparseCore 0:
  10.3 115.6 all-gather.1

commit v7 on v6

--- a/solution.py
+++ b/solution.py
@@ -346,7 +346,7 @@
             pltpu.VMEM((ROWS, WC - GU), BF16),
             pltpu.SemaphoreType.DMA((2 * (wide // FC),)),
         ],
-        compiler_params=pltpu.CompilerParams(vmem_limit_bytes=55 * 1024 * 1024),
+        compiler_params=pltpu.CompilerParams(vmem_limit_bytes=48 * 1024 * 1024),
         cost_estimate=pl.CostEstimate(flops=1_700_000_000, bytes_accessed=10_000_000, transcendentals=140_000),
         name="ffn",
     )(core, rows, weights)

time: 158 us -> 155 us (0.981)
  starting transfers between devices: 40.4 us -> 33.2 us
  waiting for transfers between devices: 24.8 us -> 31.2 us
  Pallas kernels: 16.6 us -> 14.6 us
    ppermute x2, starting transfers between devices: 14 us -> 4.67 us  [sum_at_owner(): given = lax.ppermute(theirs, 'c', [(0, 1), (1, 0)])]
    ppermute x3, waiting for transfers between devices: 4.08 us -> 9.02 us  [shards(): lax.ppermute(parts[r], 'z', answer(r))]
    ppermute x3, starting transfers between devices: 9.88 us -> 12 us  [shards(): lax.ppermute(parts[r], 'z', answer(r))]
    pallas_call x1, Pallas kernels: 6.97 us -> 4.96 us  [ffn(): pl.pallas_call(ffn_kernel, out_shape=halves(wide), in_specs=[pl.BlockSpec...]
  transfers between devices with their start and end apart: 10 -> 10, of which waited for: 6 -> 7; matrix products, arithmetic and copies ran while one was open for 1% -> 1% of each run, Pallas kernels for 6% -> 6%
where the time goes in v7:
time: 155 us; the launch traced here: 154 us
  blocking collectives  57.1 us (37%)
  starting transfers between devices  33.2 us (21%)
  waiting for transfers between devices  31.2 us (20%)
  Pallas kernels  14.6 us (9%)
  between operations  13.6 us (9%)
  other arithmetic  2.65 us (2%)
  local copies, waits for them, and re-layouts  1.67 us (1%)
    all_to_all x2, blocking collectives, sum_at_owner(): arrived = lax.all_to_all(blocks, 'x', 0, 0, tiled=True)  23 us
    all_to_all x1, blocking collectives, shards(): lax.all_to_all(payload(keys.T, values.T, log_gates.T), 'y', 0, 0, tiled=T...  20.5 us
    ppermute x1, starting transfers between devices, shards(): lent = lax.ppermute(held, 'z', swap)  12.7 us
    ppermute x3, waiting for transfers between devices, shards(): q_all = [scaled] + [lax.ppermute(scaled, 'z', ask(r)) for r in range(1, QG)]  12.3 us
    ppermute x3, starting transfers between devices, shards(): lax.ppermute(parts[r], 'z', answer(r))  12 us
    ppermute x3, waiting for transfers between devices, shards(): lax.ppermute(parts[r], 'z', answer(r))  9.02 us
    all_to_all x1, blocking collectives, copies(): return lax.all_to_all(sent, axis, 0, 0, tiled=True)  8.68 us
    pallas_call x1, Pallas kernels, attention(): pl.pallas_call(attention_kernel, out_shape=[jax.ShapeDtypeStruct((OUTR, Q...  7.28 us
  transfers between devices with their start and end apart: 10, of which 7 were waited for; matrix products, arithmetic and copies ran while one was open for 1% of the time, Pallas kernels for 6%

profile of v7, /device:TPU:1, one launch (start us, length us, event | category | flops | bytes accessed | tf_op | source)
XLA Modules:
  0.0 154.1 jit_solution(14416812784552539404)
XLA Ops:
  6.5 1.6 %concatenate.3 = bf16[32,2176]{1,0:T(8,128)(2,1)} concatenate(bf16[32,704]{1,0:T(8,128)(2,1)} %param.23, bf16[32,704]{1,0:T(8,128)(2,1)} %param.24, bf16[32,704]{1,0:T(8,128)(2,1)} %bitcast.14, bf16[32,64]{1,0:T(8,128)(2,1)S(1)} %broadcast_in_dim.8), dimensions={1} | concatenate | bytes 278528 | tf_op jit(solution)/shard_map/concatenate | solution.py:400
  8.2 1.7 %payload.1 = bf16[8,224,128]{2,1,0:T(8,128)(2,1)} custom-call(bf16[64,192]{1,0:T(8,128)(2,1)} %bitcast.15, bf16[64,192]{1,0:T(8,128)(2,1)} %bitcast.16, f32[4,192]{1,0:T(4,128)} %bitcast.17), custom_call_target="tpu_custom_call" | custom-call | flops 100000 | bytes 500000 | tf_op jit(solution)/shard_map/payload/pallas_call | solution.py:62
  9.9 20.5 %all_to_all.20.kv0 = bf16[8,224,128]{2,1,0:T(8,128)(2,1)S(1)} all-to-all(bf16[8,224,128]{2,1,0:T(8,128)(2,1)} %payload.1), channel_id=1, replica_groups=mesh['z'=8,'y'=8,'x'=4,'c'=2] {'y'}, dimensions={0} | all-to-all | bytes 917504 | tf_op jit(solution)/shard_map/all_to_all | solution.py:404
  30.4 12.7 %collective-permute-start = (bf16[8,224,128]{2,1,0:T(8,128)(2,1)S(1)}, bf16[8,224,128]{2,1,0:T(8,128)(2,1)S(1)}, u32[]{:S(2)}, u32[]{:S(2)}) collective-permute-start(bf16[8,224,128]{2,1,0:T(8,128)(2,1)S(1)} %all_to_all.20.kv0), channel_id=1, source_target_pairs={{64,128},{192,256},{320,384},{0,448},{128,64},{256,192},{384,320},... | collective-permute-start | bytes 1376264 | tf_op jit(solution)/shard_map/ppermute | solution.py:405
  43.1 0.9 broadcast_multiply_fusion.q0
  44.0 1.3 collective-permute-start.3
  45.3 1.3 collective-permute-start.2
  46.6 1.3 collective-permute-start.1
  48.0 8.4 %collective-permute-done.3.q3 = bf16[192,256]{1,0:T(8,128)(2,1)S(1)} collective-permute-done((bf16[192,256]{1,0:T(8,128)(2,1)S(1)}, bf16[192,256]{1,0:T(8,128)(2,1)S(1)}, u32[]{:S(2)}, u32[]{:S(2)}) %collective-permute-start.3) | collective-permute-done | bytes 98336 | tf_op jit(solution)/shard_map/ppermute | solution.py:403
  56.5 3.8 %collective-permute-done.1.q1 = bf16[192,256]{1,0:T(8,128)(2,1)S(1)} collective-permute-done((bf16[192,256]{1,0:T(8,128)(2,1)S(1)}, bf16[192,256]{1,0:T(8,128)(2,1)S(1)}, u32[]{:S(2)}, u32[]{:S(2)}) %collective-permute-start.1) | collective-permute-done | bytes 98336 | tf_op jit(solution)/shard_map/ppermute | solution.py:403
  60.3 7.3 %attention.1 = (bf16[72,768]{1,0:T(8,128)(2,1)S(1)}, bf16[72,768]{1,0:T(8,128)(2,1)S(1)}, bf16[72,768]{1,0:T(8,128)(2,1)S(1)}, bf16[72,768]{1,0:T(8,128)(2,1)S(1)}) custom-call(s32[3]{0:T(128)S(1)} %pad_add_fusion.pos, bf16[8,224,128]{2,1,0:T(8,128)(2,1)S(1)} %all_to_all.20.kv0, bf16[8,224,128]{2,1,0:T(8,128)(2,1)S(1)} %collective-permute-done.kv1, ...), custom_call_target="tpu_custom_call" | custom-call | flops 12000000000 | bytes 4000000 | tf_op jit(solution)/shard_map/attention/pallas_call | solution.py:218
  67.6 1.3 collective-permute-start.4
  68.9 9.4 %collective-permute-start.5 = (bf16[72,768]{1,0:T(8,128)(2,1)S(1)}, bf16[72,768]{1,0:T(8,128)(2,1)S(1)}, u32[]{:S(2)}, u32[]{:S(2)}) collective-permute-start(bf16[72,768]{1,0:T(8,128)(2,1)S(1)} %get-tuple-element.15), channel_id=1, source_target_pairs={{0,256},{128,384},{192,448},{448,192},{64,320},{1,257},{129,385},{... | collective-permute-start | bytes 331784 | tf_op jit(solution)/shard_map/ppermute | solution.py:411
  78.3 1.3 collective-permute-start.6
  79.6 3.5 %collective-permute-done.5.p2 = bf16[72,768]{1,0:T(8,128)(2,1)S(1)} collective-permute-done((bf16[72,768]{1,0:T(8,128)(2,1)S(1)}, bf16[72,768]{1,0:T(8,128)(2,1)S(1)}, u32[]{:S(2)}, u32[]{:S(2)}) %collective-permute-start.5) | collective-permute-done | bytes 110624 | tf_op jit(solution)/shard_map/ppermute | solution.py:411
  83.1 5.5 %collective-permute-done.6.p3 = bf16[72,768]{1,0:T(8,128)(2,1)S(1)} collective-permute-done((bf16[72,768]{1,0:T(8,128)(2,1)S(1)}, bf16[72,768]{1,0:T(8,128)(2,1)S(1)}, u32[]{:S(2)}, u32[]{:S(2)}) %collective-permute-start.6) | collective-permute-done | bytes 110624 | tf_op jit(solution)/shard_map/ppermute | solution.py:411
  88.6 0.6 merge.1
  89.3 1.9 %collective-permute-start.7 = (bf16[96,2048]{1,0:T(8,128)(2,1)S(1)}, bf16[96,2048]{1,0:T(8,128)(2,1)S(1)}, u32[]{:S(2)}, u32[]{:S(2)}) collective-permute-start(bf16[96,2048]{1,0:T(8,128)(2,1)S(1)} %get-tuple-element.18), channel_id=1, source_target_pairs={{0,1},{1,0},{2,3},{3,2},{4,5},{5,4},{6,7},{7,6},{8,9},{9,8},{10,11... | collective-permute-start | bytes 1179656 | tf_op jit(solution)/shard_map/ppermute | solution.py:361
  91.2 1.7 %collective-permute-done.7 = bf16[96,2048]{1,0:T(8,128)(2,1)S(1)} collective-permute-done((bf16[96,2048]{1,0:T(8,128)(2,1)S(1)}, bf16[96,2048]{1,0:T(8,128)(2,1)S(1)}, u32[]{:S(2)}, u32[]{:S(2)}) %collective-permute-start.7) | collective-permute-done | bytes 393248 | tf_op jit(solution)/shard_map/ppermute | solution.py:361
  93.0 12.3 %all_to_all.21 = bf16[4,24,2048]{2,1,0:T(8,128)(2,1)S(1)} all-to-all(bf16[4,24,2048]{2,1,0:T(8,128)(2,1)S(1)} %bitcast.11), channel_id=1, replica_groups=mesh['z'=8,'y'=8,'x'=4,'c'=2] {'x'}, dimensions={0} | all-to-all | bytes 786432 | tf_op jit(solution)/shard_map/all_to_all | solution.py:364
  105.3 0.1 multiply_reduce_fusion.2
  105.5 0.2 multiply_reduce_fusion.1
  105.7 0.1 multiply_convert_fusion
  105.9 8.7 %all_to_all.22 = bf16[4,24,2048]{2,1,0:T(8,128)(2,1)S(1)} all-to-all(bf16[4,24,2048]{2,1,0:T(8,128)(2,1)S(1)} %broadcast_in_dim.7), channel_id=1, replica_groups=mesh['z'=8,'y'=8,'x'=4,'c'=2] {'x'}, dimensions={0} | all-to-all | bytes 786432 | tf_op jit(solution)/shard_map/all_to_all | solution.py:357
  114.5 5.0 %all_gather.6.rows = bf16[192,2048]{1,0:T(8,128)(2,1)S(1)} all-gather(bf16[96,2048]{1,0:T(8,128)(2,1)S(1)} %bitcast.13), channel_id=1, replica_groups=mesh['z'=8,'y'=8,'x'=4,'c'=2] {'c'}, dimensions={0}, use_global_device_ids=true | all-gather | bytes 1179648 | tf_op jit(solution)/shard_map/all_gather | solution.py:417
  119.6 6.8 %all-gather.2.cloned.1.call-done.weights = bf16[2048,2176]{1,0:T(8,128)(2,1)} async-done(((bf16[32,2176]{1,0:T(8,128)(2,1)}), bf16[2048,2176]{1,0:T(8,128)(2,1)}) %all-gather.2.cloned.1.call-update) | async-done | bytes 8912912 | tf_op jit(solution)/shard_map/all_gather | solution.py:401
  126.4 5.0 %ffn.1 = (bf16[96,2048]{1,0:T(8,128)(2,1)S(1)}, bf16[96,2048]{1,0:T(8,128)(2,1)S(1)}) custom-call(s32[1]{0:T(128)} %bitcast.core, bf16[192,2048]{1,0:T(8,128)(2,1)S(1)} %all_gather.6.rows, bf16[2048,2176]{1,0:T(8,128)(2,1)} %all-gather.2.cloned.1.call-done.weights), custom_call_target="tpu_custom_call" | custom-call | flops 1700000000 | bytes 10000000 | tf_op jit(solution)/shard_map/ffn/pallas_call | solution.py:338
  131.4 2.8 %collective-permute-start.8 = (bf16[96,2048]{1,0:T(8,128)(2,1)S(1)}, bf16[96,2048]{1,0:T(8,128)(2,1)S(1)}, u32[]{:S(2)}, u32[]{:S(2)}) collective-permute-start(bf16[96,2048]{1,0:T(8,128)(2,1)S(1)} %get-tuple-element.20), channel_id=1, source_target_pairs={{0,1},{1,0},{2,3},{3,2},{4,5},{5,4},{6,7},{7,6},{8,9},{9,8},{10,11... | collective-permute-start | bytes 1179656 | tf_op jit(solution)/shard_map/ppermute | solution.py:361
  134.1 1.3 collective-permute-done.8
  135.6 10.7 %all_to_all.23 = bf16[4,24,2048]{2,1,0:T(8,128)(2,1)S(1)} all-to-all(bf16[4,24,2048]{2,1,0:T(8,128)(2,1)S(1)} %bitcast.12), channel_id=1, replica_groups=mesh['z'=8,'y'=8,'x'=4,'c'=2] {'x'}, dimensions={0} | all-to-all | bytes 786432 | tf_op jit(solution)/shard_map/all_to_all | solution.py:364
  146.3 0.1 multiply_reduce_fusion
  146.5 0.8 add_convert_fusion.2
  (27 shorter events, 0.5 us)
Async XLA Ops:
  6.5 119.9 %all-gather.2.cloned.1.call-start = ((), (), s32[]{:S(2)}) async-start(), calls=%async_computation.4 | async-start | bytes 9052160 | tf_op jit(solution)/shard_map/all_gather | solution.py:401
  30.4 29.9 %collective-permute-start = (bf16[8,224,128]{2,1,0:T(8,128)(2,1)S(1)}, bf16[8,224,128]{2,1,0:T(8,128)(2,1)S(1)}, u32[]{:S(2)}, u32[]{:S(2)}) collective-permute-start(bf16[8,224,128]{2,1,0:T(8,128)(2,1)S(1)} %all_to_all.20.kv0), channel_id=1, source_target_pairs={{64,128},{192,256},{320,384},{0,448},{128,64},{256,192},{384,320},... | collective-permute-start | bytes 1376264 | tf_op jit(solution)/shard_map/ppermute | solution.py:405
  44.0 12.5 %collective-permute-start.3 = (bf16[192,256]{1,0:T(8,128)(2,1)S(1)}, bf16[192,256]{1,0:T(8,128)(2,1)S(1)}, u32[]{:S(2)}, u32[]{:S(2)}) collective-permute-start(bf16[192,256]{1,0:T(8,128)(2,1)S(1)} %broadcast_multiply_fusion.q0), channel_id=1, source_target_pairs={{128,0},{256,128},{384,256},{448,320},{64,448},{192,64},{320,192},... | collective-permute-start | bytes 294920 | tf_op jit(solution)/shard_map/ppermute | solution.py:403
  45.3 11.2 %collective-permute-start.2 = (bf16[192,256]{1,0:T(8,128)(2,1)S(1)}, bf16[192,256]{1,0:T(8,128)(2,1)S(1)}, u32[]{:S(2)}, u32[]{:S(2)}) collective-permute-start(bf16[192,256]{1,0:T(8,128)(2,1)S(1)} %broadcast_multiply_fusion.q0), channel_id=1, source_target_pairs={{256,0},{384,128},{448,192},{192,448},{320,64},{257,1},{385,129},{... | collective-permute-start | bytes 294920 | tf_op jit(solution)/shard_map/ppermute | solution.py:403
  46.6 13.7 %collective-permute-start.1 = (bf16[192,256]{1,0:T(8,128)(2,1)S(1)}, bf16[192,256]{1,0:T(8,128)(2,1)S(1)}, u32[]{:S(2)}, u32[]{:S(2)}) collective-permute-start(bf16[192,256]{1,0:T(8,128)(2,1)S(1)} %broadcast_multiply_fusion.q0), channel_id=1, source_target_pairs={{384,0},{448,64},{320,448},{385,1},{449,65},{321,449},{386,2},{450... | collective-permute-start | bytes 294920 | tf_op jit(solution)/shard_map/ppermute | solution.py:403
  48.0 40.6 %copy-start = (bf16[256,2048]{1,0:T(8,128)(2,1)S(1)}, bf16[256,2048]{1,0:T(8,128)(2,1)}, u32[]{:S(2)}) copy-start(bf16[256,2048]{1,0:T(8,128)(2,1)} %weight.1) | copy-start | bytes 3145732
  48.0 40.6 %copy-start.1 = (bf16[192,256]{1,0:T(8,128)(2,1)S(1)}, bf16[192,256]{1,0:T(8,128)(2,1)}, u32[]{:S(2)}) copy-start(bf16[192,256]{1,0:T(8,128)(2,1)} %gates.1) | copy-start | bytes 294916
  48.0 57.5 %copy-start.2 = (bf16[24,2048]{1,0:T(8,128)(2,1)S(1)}, bf16[24,2048]{1,0:T(8,128)(2,1)}, u32[]{:S(2)}) copy-start(bf16[24,2048]{1,0:T(8,128)(2,1)} %param.13) | copy-start | bytes 294916
  48.0 57.5 %copy-start.3 = (f32[2048]{0:T(1024)S(1)}, f32[2048]{0:T(1024)}, u32[]{:S(2)}) copy-start(f32[2048]{0:T(1024)} %param.20) | copy-start | bytes 24580
  48.0 57.7 %copy-start.5 = (f32[2048]{0:T(1024)S(1)}, f32[2048]{0:T(1024)}, u32[]{:S(2)}) copy-start(f32[2048]{0:T(1024)} %param.21) | copy-start | bytes 24580
  67.6 12.0 %collective-permute-start.4 = (bf16[72,768]{1,0:T(8,128)(2,1)S(1)}, bf16[72,768]{1,0:T(8,128)(2,1)S(1)}, u32[]{:S(2)}, u32[]{:S(2)}) collective-permute-start(bf16[72,768]{1,0:T(8,128)(2,1)S(1)} %get-tuple-element.14), channel_id=1, source_target_pairs={{0,384},{64,448},{448,320},{1,385},{65,449},{449,321},{2,386},{66,... | collective-permute-start | bytes 331784 | tf_op jit(solution)/shard_map/ppermute | solution.py:411
  68.9 14.2 %collective-permute-start.5 = (bf16[72,768]{1,0:T(8,128)(2,1)S(1)}, bf16[72,768]{1,0:T(8,128)(2,1)S(1)}, u32[]{:S(2)}, u32[]{:S(2)}) collective-permute-start(bf16[72,768]{1,0:T(8,128)(2,1)S(1)} %get-tuple-element.15), channel_id=1, source_target_pairs={{0,256},{128,384},{192,448},{448,192},{64,320},{1,257},{129,385},{... | collective-permute-start | bytes 331784 | tf_op jit(solution)/shard_map/ppermute | solution.py:411
  78.3 10.3 %collective-permute-start.6 = (bf16[72,768]{1,0:T(8,128)(2,1)S(1)}, bf16[72,768]{1,0:T(8,128)(2,1)S(1)}, u32[]{:S(2)}, u32[]{:S(2)}) collective-permute-start(bf16[72,768]{1,0:T(8,128)(2,1)S(1)} %get-tuple-element.16), channel_id=1, source_target_pairs={{0,128},{128,256},{256,384},{320,448},{448,64},{64,192},{192,320},... | collective-permute-start | bytes 331784 | tf_op jit(solution)/shard_map/ppermute | solution.py:411
  89.3 3.6 %collective-permute-start.7 = (bf16[96,2048]{1,0:T(8,128)(2,1)S(1)}, bf16[96,2048]{1,0:T(8,128)(2,1)S(1)}, u32[]{:S(2)}, u32[]{:S(2)}) collective-permute-start(bf16[96,2048]{1,0:T(8,128)(2,1)S(1)} %get-tuple-element.18), channel_id=1, source_target_pairs={{0,1},{1,0},{2,3},{3,2},{4,5},{5,4},{6,7},{7,6},{8,9},{9,8},{10,11... | collective-permute-start | bytes 1179656 | tf_op jit(solution)/shard_map/ppermute | solution.py:361
  92.9 53.6 %copy-start.4 = (f32[2048]{0:T(1024)S(1)}, f32[2048]{0:T(1024)}, u32[]{:S(2)}) copy-start(f32[2048]{0:T(1024)} %param.22) | copy-start | bytes 24580
  131.4 4.1 %collective-permute-start.8 = (bf16[96,2048]{1,0:T(8,128)(2,1)S(1)}, bf16[96,2048]{1,0:T(8,128)(2,1)S(1)}, u32[]{:S(2)}, u32[]{:S(2)}) collective-permute-start(bf16[96,2048]{1,0:T(8,128)(2,1)S(1)} %get-tuple-element.20), channel_id=1, source_target_pairs={{0,1},{1,0},{2,3},{3,2},{4,5},{5,4},{6,7},{7,6},{8,9},{9,8},{10,11... | collective-permute-start | bytes 1179656 | tf_op jit(solution)/shard_map/ppermute | solution.py:361
Sparse Core Ops, SparseCore 0:
  10.3 116.0 all-gather.1

commit v8 on v7

--- a/solution.py
+++ b/solution.py
@@ -52,16 +52,15 @@
     side = jnp.where(line == 15, norm, side)
     left = side[:, 0:128].astype(BF16)
     right = jnp.concatenate([side[:, 128:], jnp.zeros((16, 64), F32)], axis=1).astype(BF16)
-    for n in range(YS):
-        out[n, 0:ROWS, :] = rows
-        out[n, ROWS : ROWS + 16, :] = left
-        out[n, ROWS + 16 : KP, :] = right
+    out[0:ROWS, :] = rows
+    out[ROWS : ROWS + 16, :] = left
+    out[ROWS + 16 : KP, :] = right
 
 
 def payload(keys, values, gates):
     return pl.pallas_call(
         payload_kernel,
-        out_shape=jax.ShapeDtypeStruct((YS, KP, 128), BF16),
+        out_shape=jax.ShapeDtypeStruct((KP, 128), BF16),
         cost_estimate=pl.CostEstimate(flops=100_000, bytes_accessed=500_000, transcendentals=0),
         name="payload",
     )(keys, values, gates)
@@ -401,7 +400,7 @@
     weights = lax.all_gather(packed, SP, axis=0, tiled=True)
     scaled = queries * jnp.asarray(HD**-0.5, BF16)
     q_all = [scaled] + [lax.ppermute(scaled, "z", ask(r)) for r in range(1, QG)]
-    held = lax.all_to_all(payload(keys.T, values.T, log_gates.T), "y", 0, 0, tiled=True)
+    held = lax.all_gather(payload(keys.T, values.T, log_gates.T), "y")
     lent = lax.ppermute(held, "z", swap)
     z = lax.axis_index("z")
     zh = sum(jnp.where(z == ZGRID[a][b], a, 0) for a in range(ZH) for b in range(QG))

time: 155 us -> 153 us (0.987)
  waiting for transfers between devices: 31.2 us -> 23.1 us
  blocking collectives: 57.1 us -> 61.6 us
  Pallas kernels: 14.6 us -> 18.4 us
  starting transfers between devices: 33.2 us -> 30.9 us
    all_gather x0 -> x1, blocking collectives: none -> 21.8 us  [shards(): held = lax.all_gather(payload(keys.T, values.T, log_gates.T), 'y')]
    all_to_all x1 -> x0, blocking collectives: 20.5 us -> none  [shards(): lax.all_to_all(payload(keys.T, values.T, log_gates.T), 'y', 0, 0, tiled=T...]
    ppermute x3, starting transfers between devices: 12 us -> 3.89 us  [shards(): lax.ppermute(parts[r], 'z', answer(r))]
    ppermute x2, starting transfers between devices: 4.67 us -> 11.7 us  [sum_at_owner(): given = lax.ppermute(theirs, 'c', [(0, 1), (1, 0)])]
    pallas_call x1, Pallas kernels: 7.28 us -> 11.3 us  [attention(): pl.pallas_call(attention_kernel, out_shape=[jax.ShapeDtypeStruct((OUTR, Q...]
    all_gather x1, waiting for transfers between devices: 6.84 us -> 3.5 us  [shards(): weights = lax.all_gather(packed, SP, axis=0, tiled=True)]
    all_to_all x2, blocking collectives: 23 us -> 26.2 us  [sum_at_owner(): arrived = lax.all_to_all(blocks, 'x', 0, 0, tiled=True)]
    ppermute x3, waiting for transfers between devices: 9.02 us -> 6.24 us  [shards(): lax.ppermute(parts[r], 'z', answer(r))]
  transfers between devices with their start and end apart: 10 -> 10, of which waited for: 7 -> 8; matrix products, arithmetic and copies ran while one was open for 1% -> 1% of each run, Pallas kernels for 6% -> 9%
where the time goes in v8:
time: 153 us; the launch traced here: 152 us
  blocking collectives  61.6 us (40%)
  starting transfers between devices  30.9 us (20%)
  waiting for transfers between devices  23.1 us (15%)
  Pallas kernels  18.4 us (12%)
  between operations  13.6 us (9%)
  other arithmetic  2.65 us (2%)
  local copies, waits for them, and re-layouts  1.67 us (1%)
    all_to_all x2, blocking collectives, sum_at_owner(): arrived = lax.all_to_all(blocks, 'x', 0, 0, tiled=True)  26.2 us
    all_gather x1, blocking collectives, shards(): held = lax.all_gather(payload(keys.T, values.T, log_gates.T), 'y')  21.8 us
    ppermute x2, starting transfers between devices, sum_at_owner(): given = lax.ppermute(theirs, 'c', [(0, 1), (1, 0)])  11.7 us
    ppermute x1, starting transfers between devices, shards(): lent = lax.ppermute(held, 'z', swap)  11.5 us
    pallas_call x1, Pallas kernels, attention(): pl.pallas_call(attention_kernel, out_shape=[jax.ShapeDtypeStruct((OUTR, Q...  11.3 us
    ppermute x3, waiting for transfers between devices, shards(): q_all = [scaled] + [lax.ppermute(scaled, 'z', ask(r)) for r in range(1, QG)]  10.7 us
    all_to_all x1, blocking collectives, copies(): return lax.all_to_all(sent, axis, 0, 0, tiled=True)  8.68 us
    ppermute x3, waiting for transfers between devices, shards(): lax.ppermute(parts[r], 'z', answer(r))  6.24 us
  transfers between devices with their start and end apart: 10, of which 8 were waited for; matrix products, arithmetic and copies ran while one was open for 1% of the time, Pallas kernels for 9%

profile of v8, /device:TPU:1, one launch (start us, length us, event | category | flops | bytes accessed | tf_op | source)
XLA Modules:
  0.0 152.1 jit_solution(7903847378593553630)
XLA Ops:
  6.5 1.6 %concatenate.3 = bf16[32,2176]{1,0:T(8,128)(2,1)} concatenate(bf16[32,704]{1,0:T(8,128)(2,1)} %param.23, bf16[32,704]{1,0:T(8,128)(2,1)} %param.24, bf16[32,704]{1,0:T(8,128)(2,1)} %bitcast.17, bf16[32,64]{1,0:T(8,128)(2,1)S(1)} %broadcast_in_dim.8), dimensions={1} | concatenate | bytes 278528 | tf_op jit(solution)/shard_map/concatenate | solution.py:399
  8.2 1.5 %payload.1 = bf16[224,128]{1,0:T(8,128)(2,1)} custom-call(bf16[64,192]{1,0:T(8,128)(2,1)} %bitcast.18, bf16[64,192]{1,0:T(8,128)(2,1)} %bitcast.19, f32[4,192]{1,0:T(4,128)} %bitcast.20), custom_call_target="tpu_custom_call" | custom-call | flops 100000 | bytes 500000 | tf_op jit(solution)/shard_map/payload/pallas_call | solution.py:61
  9.7 21.8 %all-gather = bf16[1792,128]{1,0:T(8,128)(2,1)S(1)} all-gather(bf16[224,128]{1,0:T(8,128)(2,1)} %payload.1), channel_id=2, replica_groups=mesh['z'=8,'y'=8,'x'=4,'c'=2] {'y'}, dimensions={0}, use_global_device_ids=true | all-gather | bytes 516096 | tf_op jit(solution)/shard_map/all_gather | solution.py:403
  31.5 11.5 %collective-permute-start = (bf16[8,224,128]{2,1,0:T(8,128)(2,1)S(1)}, bf16[8,224,128]{2,1,0:T(8,128)(2,1)S(1)}, u32[]{:S(2)}, u32[]{:S(2)}) collective-permute-start(bf16[8,224,128]{2,1,0:T(8,128)(2,1)S(1)} %bitcast.12), channel_id=1, source_target_pairs={{64,128},{192,256},{320,384},{0,448},{128,64},{256,192},{384,320},... | collective-permute-start | bytes 1376264 | tf_op jit(solution)/shard_map/ppermute | solution.py:404
  43.0 0.9 broadcast_multiply_fusion.q0
  43.9 1.3 collective-permute-start.3
  45.2 1.3 collective-permute-start.2
  46.5 1.3 collective-permute-start.1
  47.9 4.1 %collective-permute-done.3.q3 = bf16[192,256]{1,0:T(8,128)(2,1)S(1)} collective-permute-done((bf16[192,256]{1,0:T(8,128)(2,1)S(1)}, bf16[192,256]{1,0:T(8,128)(2,1)S(1)}, u32[]{:S(2)}, u32[]{:S(2)}) %collective-permute-start.3) | collective-permute-done | bytes 98336 | tf_op jit(solution)/shard_map/ppermute | solution.py:402
  52.0 3.1 %collective-permute-done.2.q2 = bf16[192,256]{1,0:T(8,128)(2,1)S(1)} collective-permute-done((bf16[192,256]{1,0:T(8,128)(2,1)S(1)}, bf16[192,256]{1,0:T(8,128)(2,1)S(1)}, u32[]{:S(2)}, u32[]{:S(2)}) %collective-permute-start.2) | collective-permute-done | bytes 98336 | tf_op jit(solution)/shard_map/ppermute | solution.py:402
  55.1 3.6 %collective-permute-done.1.q1 = bf16[192,256]{1,0:T(8,128)(2,1)S(1)} collective-permute-done((bf16[192,256]{1,0:T(8,128)(2,1)S(1)}, bf16[192,256]{1,0:T(8,128)(2,1)S(1)}, u32[]{:S(2)}, u32[]{:S(2)}) %collective-permute-start.1) | collective-permute-done | bytes 98336 | tf_op jit(solution)/shard_map/ppermute | solution.py:402
  58.7 11.3 %attention.1 = (bf16[72,768]{1,0:T(8,128)(2,1)S(1)}, bf16[72,768]{1,0:T(8,128)(2,1)S(1)}, bf16[72,768]{1,0:T(8,128)(2,1)S(1)}, bf16[72,768]{1,0:T(8,128)(2,1)S(1)}) custom-call(s32[3]{0:T(128)S(1)} %pad_add_fusion.pos, bf16[8,224,128]{2,1,0:T(8,128)(2,1)S(1)} %bitcast.13, bf16[8,224,128]{2,1,0:T(8,128)(2,1)S(1)} %collective-permute-done.kv1, ...), custom_call_target="tpu_custom_call" | custom-call | flops 12000000000 | bytes 4000000 | tf_op jit(solution)/shard_map/attention/pallas_call | solution.py:217
  69.9 1.3 collective-permute-start.4
  71.3 1.3 collective-permute-start.5
  72.6 1.3 collective-permute-start.6
  73.9 2.0 %collective-permute-done.5.p2 = bf16[72,768]{1,0:T(8,128)(2,1)S(1)} collective-permute-done((bf16[72,768]{1,0:T(8,128)(2,1)S(1)}, bf16[72,768]{1,0:T(8,128)(2,1)S(1)}, u32[]{:S(2)}, u32[]{:S(2)}) %collective-permute-start.5) | collective-permute-done | bytes 110624 | tf_op jit(solution)/shard_map/ppermute | solution.py:410
  75.9 4.2 %collective-permute-done.6.p3 = bf16[72,768]{1,0:T(8,128)(2,1)S(1)} collective-permute-done((bf16[72,768]{1,0:T(8,128)(2,1)S(1)}, bf16[72,768]{1,0:T(8,128)(2,1)S(1)}, u32[]{:S(2)}, u32[]{:S(2)}) %collective-permute-start.6) | collective-permute-done | bytes 110624 | tf_op jit(solution)/shard_map/ppermute | solution.py:410
  80.1 0.6 merge.1
  80.8 8.9 %collective-permute-start.7 = (bf16[96,2048]{1,0:T(8,128)(2,1)S(1)}, bf16[96,2048]{1,0:T(8,128)(2,1)S(1)}, u32[]{:S(2)}, u32[]{:S(2)}) collective-permute-start(bf16[96,2048]{1,0:T(8,128)(2,1)S(1)} %get-tuple-element.18), channel_id=1, source_target_pairs={{0,1},{1,0},{2,3},{3,2},{4,5},{5,4},{6,7},{7,6},{8,9},{9,8},{10,11... | collective-permute-start | bytes 1179656 | tf_op jit(solution)/shard_map/ppermute | solution.py:360
  89.7 1.3 collective-permute-done.7
  91.1 15.2 %all_to_all.15 = bf16[4,24,2048]{2,1,0:T(8,128)(2,1)S(1)} all-to-all(bf16[4,24,2048]{2,1,0:T(8,128)(2,1)S(1)} %bitcast.14), channel_id=1, replica_groups=mesh['z'=8,'y'=8,'x'=4,'c'=2] {'x'}, dimensions={0} | all-to-all | bytes 786432 | tf_op jit(solution)/shard_map/all_to_all | solution.py:363
  106.4 0.1 multiply_reduce_fusion.2
  106.5 0.2 multiply_reduce_fusion.1
  106.9 8.7 %all_to_all.16 = bf16[4,24,2048]{2,1,0:T(8,128)(2,1)S(1)} all-to-all(bf16[4,24,2048]{2,1,0:T(8,128)(2,1)S(1)} %broadcast_in_dim.7), channel_id=1, replica_groups=mesh['z'=8,'y'=8,'x'=4,'c'=2] {'x'}, dimensions={0} | all-to-all | bytes 786432 | tf_op jit(solution)/shard_map/all_to_all | solution.py:356
  115.6 5.0 %all_gather.14.rows = bf16[192,2048]{1,0:T(8,128)(2,1)S(1)} all-gather(bf16[96,2048]{1,0:T(8,128)(2,1)S(1)} %bitcast.16), channel_id=1, replica_groups=mesh['z'=8,'y'=8,'x'=4,'c'=2] {'c'}, dimensions={0}, use_global_device_ids=true | all-gather | bytes 1179648 | tf_op jit(solution)/shard_map/all_gather | solution.py:416
  120.6 3.5 %all-gather.3.cloned.1.call-done.weights = bf16[2048,2176]{1,0:T(8,128)(2,1)} async-done(((bf16[32,2176]{1,0:T(8,128)(2,1)}), bf16[2048,2176]{1,0:T(8,128)(2,1)}) %all-gather.3.cloned.1.call-update) | async-done | bytes 8912912 | tf_op jit(solution)/shard_map/all_gather | solution.py:400
  124.1 5.0 %ffn.1 = (bf16[96,2048]{1,0:T(8,128)(2,1)S(1)}, bf16[96,2048]{1,0:T(8,128)(2,1)S(1)}) custom-call(s32[1]{0:T(128)} %bitcast.core, bf16[192,2048]{1,0:T(8,128)(2,1)S(1)} %all_gather.14.rows, bf16[2048,2176]{1,0:T(8,128)(2,1)} %all-gather.3.cloned.1.call-done.weights), custom_call_target="tpu_custom_call" | custom-call | flops 1700000000 | bytes 10000000 | tf_op jit(solution)/shard_map/ffn/pallas_call | solution.py:337
  129.1 2.7 %collective-permute-start.8 = (bf16[96,2048]{1,0:T(8,128)(2,1)S(1)}, bf16[96,2048]{1,0:T(8,128)(2,1)S(1)}, u32[]{:S(2)}, u32[]{:S(2)}) collective-permute-start(bf16[96,2048]{1,0:T(8,128)(2,1)S(1)} %get-tuple-element.20), channel_id=1, source_target_pairs={{0,1},{1,0},{2,3},{3,2},{4,5},{5,4},{6,7},{7,6},{8,9},{9,8},{10,11... | collective-permute-start | bytes 1179656 | tf_op jit(solution)/shard_map/ppermute | solution.py:360
  131.8 1.3 collective-permute-done.8
  133.3 11.0 %all_to_all.17 = bf16[4,24,2048]{2,1,0:T(8,128)(2,1)S(1)} all-to-all(bf16[4,24,2048]{2,1,0:T(8,128)(2,1)S(1)} %bitcast.15), channel_id=1, replica_groups=mesh['z'=8,'y'=8,'x'=4,'c'=2] {'x'}, dimensions={0} | all-to-all | bytes 786432 | tf_op jit(solution)/shard_map/all_to_all | solution.py:363
  144.3 0.1 multiply_reduce_fusion
  144.4 0.8 add_convert_fusion.2
  (27 shorter events, 0.6 us)
Async XLA Ops:
  6.5 117.6 %all-gather.3.cloned.1.call-start = ((), (), s32[]{:S(2)}) async-start(), calls=%async_computation.3 | async-start | bytes 9052160 | tf_op jit(solution)/shard_map/all_gather | solution.py:400
  31.5 27.2 %collective-permute-start = (bf16[8,224,128]{2,1,0:T(8,128)(2,1)S(1)}, bf16[8,224,128]{2,1,0:T(8,128)(2,1)S(1)}, u32[]{:S(2)}, u32[]{:S(2)}) collective-permute-start(bf16[8,224,128]{2,1,0:T(8,128)(2,1)S(1)} %bitcast.12), channel_id=1, source_target_pairs={{64,128},{192,256},{320,384},{0,448},{128,64},{256,192},{384,320},... | collective-permute-start | bytes 1376264 | tf_op jit(solution)/shard_map/ppermute | solution.py:404
  43.9 8.1 %collective-permute-start.3 = (bf16[192,256]{1,0:T(8,128)(2,1)S(1)}, bf16[192,256]{1,0:T(8,128)(2,1)S(1)}, u32[]{:S(2)}, u32[]{:S(2)}) collective-permute-start(bf16[192,256]{1,0:T(8,128)(2,1)S(1)} %broadcast_multiply_fusion.q0), channel_id=1, source_target_pairs={{128,0},{256,128},{384,256},{448,320},{64,448},{192,64},{320,192},... | collective-permute-start | bytes 294920 | tf_op jit(solution)/shard_map/ppermute | solution.py:402
  45.2 9.9 %collective-permute-start.2 = (bf16[192,256]{1,0:T(8,128)(2,1)S(1)}, bf16[192,256]{1,0:T(8,128)(2,1)S(1)}, u32[]{:S(2)}, u32[]{:S(2)}) collective-permute-start(bf16[192,256]{1,0:T(8,128)(2,1)S(1)} %broadcast_multiply_fusion.q0), channel_id=1, source_target_pairs={{256,0},{384,128},{448,192},{192,448},{320,64},{257,1},{385,129},{... | collective-permute-start | bytes 294920 | tf_op jit(solution)/shard_map/ppermute | solution.py:402
  46.5 12.2 %collective-permute-start.1 = (bf16[192,256]{1,0:T(8,128)(2,1)S(1)}, bf16[192,256]{1,0:T(8,128)(2,1)S(1)}, u32[]{:S(2)}, u32[]{:S(2)}) collective-permute-start(bf16[192,256]{1,0:T(8,128)(2,1)S(1)} %broadcast_multiply_fusion.q0), channel_id=1, source_target_pairs={{384,0},{448,64},{320,448},{385,1},{449,65},{321,449},{386,2},{450... | collective-permute-start | bytes 294920 | tf_op jit(solution)/shard_map/ppermute | solution.py:402
  47.9 32.2 %copy-start = (bf16[256,2048]{1,0:T(8,128)(2,1)S(1)}, bf16[256,2048]{1,0:T(8,128)(2,1)}, u32[]{:S(2)}) copy-start(bf16[256,2048]{1,0:T(8,128)(2,1)} %weight.1) | copy-start | bytes 3145732
  47.9 32.2 %copy-start.1 = (bf16[192,256]{1,0:T(8,128)(2,1)S(1)}, bf16[192,256]{1,0:T(8,128)(2,1)}, u32[]{:S(2)}) copy-start(bf16[192,256]{1,0:T(8,128)(2,1)} %gates.1) | copy-start | bytes 294916
  47.9 58.6 %copy-start.2 = (bf16[24,2048]{1,0:T(8,128)(2,1)S(1)}, bf16[24,2048]{1,0:T(8,128)(2,1)}, u32[]{:S(2)}) copy-start(bf16[24,2048]{1,0:T(8,128)(2,1)} %param.13) | copy-start | bytes 294916
  47.9 58.6 %copy-start.3 = (f32[2048]{0:T(1024)S(1)}, f32[2048]{0:T(1024)}, u32[]{:S(2)}) copy-start(f32[2048]{0:T(1024)} %param.20) | copy-start | bytes 24580
  47.9 58.8 %copy-start.5 = (f32[2048]{0:T(1024)S(1)}, f32[2048]{0:T(1024)}, u32[]{:S(2)}) copy-start(f32[2048]{0:T(1024)} %param.21) | copy-start | bytes 24580
  69.9 3.9 %collective-permute-start.4 = (bf16[72,768]{1,0:T(8,128)(2,1)S(1)}, bf16[72,768]{1,0:T(8,128)(2,1)S(1)}, u32[]{:S(2)}, u32[]{:S(2)}) collective-permute-start(bf16[72,768]{1,0:T(8,128)(2,1)S(1)} %get-tuple-element.14), channel_id=1, source_target_pairs={{0,384},{64,448},{448,320},{1,385},{65,449},{449,321},{2,386},{66,... | collective-permute-start | bytes 331784 | tf_op jit(solution)/shard_map/ppermute | solution.py:410
  71.3 4.6 %collective-permute-start.5 = (bf16[72,768]{1,0:T(8,128)(2,1)S(1)}, bf16[72,768]{1,0:T(8,128)(2,1)S(1)}, u32[]{:S(2)}, u32[]{:S(2)}) collective-permute-start(bf16[72,768]{1,0:T(8,128)(2,1)S(1)} %get-tuple-element.15), channel_id=1, source_target_pairs={{0,256},{128,384},{192,448},{448,192},{64,320},{1,257},{129,385},{... | collective-permute-start | bytes 331784 | tf_op jit(solution)/shard_map/ppermute | solution.py:410
  72.6 7.6 %collective-permute-start.6 = (bf16[72,768]{1,0:T(8,128)(2,1)S(1)}, bf16[72,768]{1,0:T(8,128)(2,1)S(1)}, u32[]{:S(2)}, u32[]{:S(2)}) collective-permute-start(bf16[72,768]{1,0:T(8,128)(2,1)S(1)} %get-tuple-element.16), channel_id=1, source_target_pairs={{0,128},{128,256},{256,384},{320,448},{448,64},{64,192},{192,320},... | collective-permute-start | bytes 331784 | tf_op jit(solution)/shard_map/ppermute | solution.py:410
  80.8 10.3 %collective-permute-start.7 = (bf16[96,2048]{1,0:T(8,128)(2,1)S(1)}, bf16[96,2048]{1,0:T(8,128)(2,1)S(1)}, u32[]{:S(2)}, u32[]{:S(2)}) collective-permute-start(bf16[96,2048]{1,0:T(8,128)(2,1)S(1)} %get-tuple-element.18), channel_id=1, source_target_pairs={{0,1},{1,0},{2,3},{3,2},{4,5},{5,4},{6,7},{7,6},{8,9},{9,8},{10,11... | collective-permute-start | bytes 1179656 | tf_op jit(solution)/shard_map/ppermute | solution.py:360
  91.0 53.4 %copy-start.4 = (f32[2048]{0:T(1024)S(1)}, f32[2048]{0:T(1024)}, u32[]{:S(2)}) copy-start(f32[2048]{0:T(1024)} %param.22) | copy-start | bytes 24580
  129.1 4.1 %collective-permute-start.8 = (bf16[96,2048]{1,0:T(8,128)(2,1)S(1)}, bf16[96,2048]{1,0:T(8,128)(2,1)S(1)}, u32[]{:S(2)}, u32[]{:S(2)}) collective-permute-start(bf16[96,2048]{1,0:T(8,128)(2,1)S(1)} %get-tuple-element.20), channel_id=1, source_target_pairs={{0,1},{1,0},{2,3},{3,2},{4,5},{5,4},{6,7},{7,6},{8,9},{9,8},{10,11... | collective-permute-start | bytes 1179656 | tf_op jit(solution)/shard_map/ppermute | solution.py:360
Sparse Core Ops, SparseCore 0:
  10.3 113.7 all-gather.2

commit v9 on v8

--- a/solution.py
+++ b/solution.py
@@ -11,7 +11,7 @@
 ROWS = 192
 QG = 4
 ZH = 8 // QG
-ZGRID = ((0, 2, 4, 6), (7, 1, 3, 5))
+ZGRID = ((0, 2, 5, 7), (1, 3, 4, 6))
 YS = 8
 NB = ZH * YS
 TILE = 1536

time: 153 us -> 151 us (0.987)
  waiting for transfers between devices: 23.1 us -> 18.5 us
  blocking collectives: 61.6 us -> 65.7 us
    ppermute x1, starting transfers between devices: 11.5 us -> 4.38 us  [shards(): lent = lax.ppermute(held, 'z', swap)]
    ppermute x2, starting transfers between devices: 11.7 us -> 16.5 us  [sum_at_owner(): given = lax.ppermute(theirs, 'c', [(0, 1), (1, 0)])]
    ppermute x3, waiting for transfers between devices: 6.24 us -> 1.71 us  [shards(): lax.ppermute(parts[r], 'z', answer(r))]
    all_to_all x2, blocking collectives: 26.2 us -> 30.2 us  [sum_at_owner(): arrived = lax.all_to_all(blocks, 'x', 0, 0, tiled=True)]
    ppermute x3, starting transfers between devices: 3.89 us -> 6.11 us  [shards(): lax.ppermute(parts[r], 'z', answer(r))]
    all_gather x1, waiting for transfers between devices: 3.5 us -> 1.72 us  [shards(): weights = lax.all_gather(packed, SP, axis=0, tiled=True)]
    ppermute x3, waiting for transfers between devices: 10.7 us -> 12.4 us  [shards(): q_all = [scaled] + [lax.ppermute(scaled, 'z', ask(r)) for r in range(1, QG)]]
  transfers between devices with their start and end apart: 10 -> 10, of which waited for: 8 -> 7; matrix products, arithmetic and copies ran while one was open for 1% -> 1% of each run, Pallas kernels for 9% -> 9%
where the time goes in v9:
time: 151 us
  blocking collectives  65.7 us (44%)
  starting transfers between devices  30.9 us (20%)
  waiting for transfers between devices  18.5 us (12%)
  Pallas kernels  17.9 us (12%)
  between operations  13.6 us (9%)
  other arithmetic  2.65 us (2%)
  local copies, waits for them, and re-layouts  1.67 us (1%)
    all_to_all x2, blocking collectives, sum_at_owner(): arrived = lax.all_to_all(blocks, 'x', 0, 0, tiled=True)  30.2 us
    all_gather x1, blocking collectives, shards(): held = lax.all_gather(payload(keys.T, values.T, log_gates.T), 'y')  21.8 us
    ppermute x2, starting transfers between devices, sum_at_owner(): given = lax.ppermute(theirs, 'c', [(0, 1), (1, 0)])  16.5 us
    ppermute x3, waiting for transfers between devices, shards(): q_all = [scaled] + [lax.ppermute(scaled, 'z', ask(r)) for r in range(1, QG)]  12.4 us
    pallas_call x1, Pallas kernels, attention(): pl.pallas_call(attention_kernel, out_shape=[jax.ShapeDtypeStruct((OUTR, Q...  10.7 us
    all_to_all x1, blocking collectives, copies(): return lax.all_to_all(sent, axis, 0, 0, tiled=True)  8.68 us
    ppermute x3, starting transfers between devices, shards(): lax.ppermute(parts[r], 'z', answer(r))  6.11 us
    all_gather x1, blocking collectives, shards(): normed_all = lax.all_gather(along, 'c', axis=0, tiled=True)  5.01 us
  transfers between devices with their start and end apart: 10, of which 7 were waited for; matrix products, arithmetic and copies ran while one was open for 1% of the time, Pallas kernels for 9%

profile of v9, /device:TPU:1, one launch (start us, length us, event | category | flops | bytes accessed | tf_op | source)
XLA Modules:
  0.0 150.9 jit_solution(12973881447306152948)
XLA Ops:
  6.5 1.6 %concatenate.3 = bf16[32,2176]{1,0:T(8,128)(2,1)} concatenate(bf16[32,704]{1,0:T(8,128)(2,1)} %param.23, bf16[32,704]{1,0:T(8,128)(2,1)} %param.24, bf16[32,704]{1,0:T(8,128)(2,1)} %bitcast.17, bf16[32,64]{1,0:T(8,128)(2,1)S(1)} %broadcast_in_dim.8), dimensions={1} | concatenate | bytes 278528 | tf_op jit(solution)/shard_map/concatenate | solution.py:399
  8.2 1.5 %payload.1 = bf16[224,128]{1,0:T(8,128)(2,1)} custom-call(bf16[64,192]{1,0:T(8,128)(2,1)} %bitcast.18, bf16[64,192]{1,0:T(8,128)(2,1)} %bitcast.19, f32[4,192]{1,0:T(4,128)} %bitcast.20), custom_call_target="tpu_custom_call" | custom-call | flops 100000 | bytes 500000 | tf_op jit(solution)/shard_map/payload/pallas_call | solution.py:61
  9.7 21.8 %all-gather = bf16[1792,128]{1,0:T(8,128)(2,1)S(1)} all-gather(bf16[224,128]{1,0:T(8,128)(2,1)} %payload.1), channel_id=2, replica_groups=mesh['z'=8,'y'=8,'x'=4,'c'=2] {'y'}, dimensions={0}, use_global_device_ids=true | all-gather | bytes 516096 | tf_op jit(solution)/shard_map/all_gather | solution.py:403
  31.5 4.4 %collective-permute-start = (bf16[8,224,128]{2,1,0:T(8,128)(2,1)S(1)}, bf16[8,224,128]{2,1,0:T(8,128)(2,1)S(1)}, u32[]{:S(2)}, u32[]{:S(2)}) collective-permute-start(bf16[8,224,128]{2,1,0:T(8,128)(2,1)S(1)} %bitcast.12), channel_id=1, source_target_pairs={{64,0},{192,128},{256,320},{384,448},{0,64},{128,192},{320,256},{6... | collective-permute-start | bytes 1376264 | tf_op jit(solution)/shard_map/ppermute | solution.py:404
  35.9 0.9 broadcast_multiply_fusion.q0
  36.8 1.3 collective-permute-start.3
  38.1 1.3 collective-permute-start.2
  39.4 1.3 collective-permute-start.1
  40.8 4.5 %collective-permute-done.3.q3 = bf16[192,256]{1,0:T(8,128)(2,1)S(1)} collective-permute-done((bf16[192,256]{1,0:T(8,128)(2,1)S(1)}, bf16[192,256]{1,0:T(8,128)(2,1)S(1)}, u32[]{:S(2)}, u32[]{:S(2)}) %collective-permute-start.3) | collective-permute-done | bytes 98336 | tf_op jit(solution)/shard_map/ppermute | solution.py:402
  45.4 4.0 %collective-permute-done.2.q2 = bf16[192,256]{1,0:T(8,128)(2,1)S(1)} collective-permute-done((bf16[192,256]{1,0:T(8,128)(2,1)S(1)}, bf16[192,256]{1,0:T(8,128)(2,1)S(1)}, u32[]{:S(2)}, u32[]{:S(2)}) %collective-permute-start.2) | collective-permute-done | bytes 98336 | tf_op jit(solution)/shard_map/ppermute | solution.py:402
  49.4 3.8 %collective-permute-done.1.q1 = bf16[192,256]{1,0:T(8,128)(2,1)S(1)} collective-permute-done((bf16[192,256]{1,0:T(8,128)(2,1)S(1)}, bf16[192,256]{1,0:T(8,128)(2,1)S(1)}, u32[]{:S(2)}, u32[]{:S(2)}) %collective-permute-start.1) | collective-permute-done | bytes 98336 | tf_op jit(solution)/shard_map/ppermute | solution.py:402
  53.2 10.7 %attention.1 = (bf16[72,768]{1,0:T(8,128)(2,1)S(1)}, bf16[72,768]{1,0:T(8,128)(2,1)S(1)}, bf16[72,768]{1,0:T(8,128)(2,1)S(1)}, bf16[72,768]{1,0:T(8,128)(2,1)S(1)}) custom-call(s32[3]{0:T(128)S(1)} %pad_add_fusion.pos, bf16[8,224,128]{2,1,0:T(8,128)(2,1)S(1)} %bitcast.13, bf16[8,224,128]{2,1,0:T(8,128)(2,1)S(1)} %collective-permute-done.kv1, ...), custom_call_target="tpu_custom_call" | custom-call | flops 12000000000 | bytes 4000000 | tf_op jit(solution)/shard_map/attention/pallas_call | solution.py:217
  64.0 1.3 collective-permute-start.4
  65.3 1.3 collective-permute-start.5
  66.6 3.5 %collective-permute-start.6 = (bf16[72,768]{1,0:T(8,128)(2,1)S(1)}, bf16[72,768]{1,0:T(8,128)(2,1)S(1)}, u32[]{:S(2)}, u32[]{:S(2)}) collective-permute-start(bf16[72,768]{1,0:T(8,128)(2,1)S(1)} %get-tuple-element.16), channel_id=1, source_target_pairs={{0,128},{128,320},{320,448},{64,192},{192,256},{256,384},{1,129},{... | collective-permute-start | bytes 331784 | tf_op jit(solution)/shard_map/ppermute | solution.py:410
  70.1 1.7 %collective-permute-done.6.p3 = bf16[72,768]{1,0:T(8,128)(2,1)S(1)} collective-permute-done((bf16[72,768]{1,0:T(8,128)(2,1)S(1)}, bf16[72,768]{1,0:T(8,128)(2,1)S(1)}, u32[]{:S(2)}, u32[]{:S(2)}) %collective-permute-start.6) | collective-permute-done | bytes 110624 | tf_op jit(solution)/shard_map/ppermute | solution.py:410
  71.8 0.6 merge.1
  72.5 13.5 %collective-permute-start.7 = (bf16[96,2048]{1,0:T(8,128)(2,1)S(1)}, bf16[96,2048]{1,0:T(8,128)(2,1)S(1)}, u32[]{:S(2)}, u32[]{:S(2)}) collective-permute-start(bf16[96,2048]{1,0:T(8,128)(2,1)S(1)} %get-tuple-element.18), channel_id=1, source_target_pairs={{0,1},{1,0},{2,3},{3,2},{4,5},{5,4},{6,7},{7,6},{8,9},{9,8},{10,11... | collective-permute-start | bytes 1179656 | tf_op jit(solution)/shard_map/ppermute | solution.py:360
  86.0 1.3 collective-permute-done.7
  87.4 15.9 %all_to_all.15 = bf16[4,24,2048]{2,1,0:T(8,128)(2,1)S(1)} all-to-all(bf16[4,24,2048]{2,1,0:T(8,128)(2,1)S(1)} %bitcast.14), channel_id=1, replica_groups=mesh['z'=8,'y'=8,'x'=4,'c'=2] {'x'}, dimensions={0} | all-to-all | bytes 786432 | tf_op jit(solution)/shard_map/all_to_all | solution.py:363
  103.4 0.1 multiply_reduce_fusion.2
  103.6 0.2 multiply_reduce_fusion.1
  103.8 0.1 multiply_convert_fusion
  104.0 8.7 %all_to_all.16 = bf16[4,24,2048]{2,1,0:T(8,128)(2,1)S(1)} all-to-all(bf16[4,24,2048]{2,1,0:T(8,128)(2,1)S(1)} %broadcast_in_dim.7), channel_id=1, replica_groups=mesh['z'=8,'y'=8,'x'=4,'c'=2] {'x'}, dimensions={0} | all-to-all | bytes 786432 | tf_op jit(solution)/shard_map/all_to_all | solution.py:356
  112.6 5.0 %all_gather.14.rows = bf16[192,2048]{1,0:T(8,128)(2,1)S(1)} all-gather(bf16[96,2048]{1,0:T(8,128)(2,1)S(1)} %bitcast.16), channel_id=1, replica_groups=mesh['z'=8,'y'=8,'x'=4,'c'=2] {'c'}, dimensions={0}, use_global_device_ids=true | all-gather | bytes 1179648 | tf_op jit(solution)/shard_map/all_gather | solution.py:416
  117.6 1.7 %all-gather.3.cloned.1.call-done.weights = bf16[2048,2176]{1,0:T(8,128)(2,1)} async-done(((bf16[32,2176]{1,0:T(8,128)(2,1)}), bf16[2048,2176]{1,0:T(8,128)(2,1)}) %all-gather.3.cloned.1.call-update) | async-done | bytes 8912912 | tf_op jit(solution)/shard_map/all_gather | solution.py:400
  119.4 5.0 %ffn.1 = (bf16[96,2048]{1,0:T(8,128)(2,1)S(1)}, bf16[96,2048]{1,0:T(8,128)(2,1)S(1)}) custom-call(s32[1]{0:T(128)} %bitcast.core, bf16[192,2048]{1,0:T(8,128)(2,1)S(1)} %all_gather.14.rows, bf16[2048,2176]{1,0:T(8,128)(2,1)} %all-gather.3.cloned.1.call-done.weights), custom_call_target="tpu_custom_call" | custom-call | flops 1700000000 | bytes 10000000 | tf_op jit(solution)/shard_map/ffn/pallas_call | solution.py:337
  124.3 3.0 %collective-permute-start.8 = (bf16[96,2048]{1,0:T(8,128)(2,1)S(1)}, bf16[96,2048]{1,0:T(8,128)(2,1)S(1)}, u32[]{:S(2)}, u32[]{:S(2)}) collective-permute-start(bf16[96,2048]{1,0:T(8,128)(2,1)S(1)} %get-tuple-element.20), channel_id=1, source_target_pairs={{0,1},{1,0},{2,3},{3,2},{4,5},{5,4},{6,7},{7,6},{8,9},{9,8},{10,11... | collective-permute-start | bytes 1179656 | tf_op jit(solution)/shard_map/ppermute | solution.py:360
  127.4 1.3 collective-permute-done.8
  128.8 14.3 %all_to_all.17 = bf16[4,24,2048]{2,1,0:T(8,128)(2,1)S(1)} all-to-all(bf16[4,24,2048]{2,1,0:T(8,128)(2,1)S(1)} %bitcast.15), channel_id=1, replica_groups=mesh['z'=8,'y'=8,'x'=4,'c'=2] {'x'}, dimensions={0} | all-to-all | bytes 786432 | tf_op jit(solution)/shard_map/all_to_all | solution.py:363
  143.1 0.1 multiply_reduce_fusion
  143.3 0.8 add_convert_fusion.2
  (27 shorter events, 0.5 us)
Async XLA Ops:
  6.5 112.8 %all-gather.3.cloned.1.call-start = ((), (), s32[]{:S(2)}) async-start(), calls=%async_computation.3 | async-start | bytes 9052160 | tf_op jit(solution)/shard_map/all_gather | solution.py:400
  31.5 21.7 %collective-permute-start = (bf16[8,224,128]{2,1,0:T(8,128)(2,1)S(1)}, bf16[8,224,128]{2,1,0:T(8,128)(2,1)S(1)}, u32[]{:S(2)}, u32[]{:S(2)}) collective-permute-start(bf16[8,224,128]{2,1,0:T(8,128)(2,1)S(1)} %bitcast.12), channel_id=1, source_target_pairs={{64,0},{192,128},{256,320},{384,448},{0,64},{128,192},{320,256},{6... | collective-permute-start | bytes 1376264 | tf_op jit(solution)/shard_map/ppermute | solution.py:404
  36.8 8.6 %collective-permute-start.3 = (bf16[192,256]{1,0:T(8,128)(2,1)S(1)}, bf16[192,256]{1,0:T(8,128)(2,1)S(1)}, u32[]{:S(2)}, u32[]{:S(2)}) collective-permute-start(bf16[192,256]{1,0:T(8,128)(2,1)S(1)} %broadcast_multiply_fusion.q0), channel_id=1, source_target_pairs={{128,0},{320,128},{448,320},{192,64},{256,192},{384,256},{129,1},{... | collective-permute-start | bytes 294920 | tf_op jit(solution)/shard_map/ppermute | solution.py:402
  38.1 11.3 %collective-permute-start.2 = (bf16[192,256]{1,0:T(8,128)(2,1)S(1)}, bf16[192,256]{1,0:T(8,128)(2,1)S(1)}, u32[]{:S(2)}, u32[]{:S(2)}) collective-permute-start(bf16[192,256]{1,0:T(8,128)(2,1)S(1)} %broadcast_multiply_fusion.q0), channel_id=1, source_target_pairs={{320,0},{448,128},{256,64},{384,192},{321,1},{449,129},{257,65},{3... | collective-permute-start | bytes 294920 | tf_op jit(solution)/shard_map/ppermute | solution.py:402
  39.4 13.8 %collective-permute-start.1 = (bf16[192,256]{1,0:T(8,128)(2,1)S(1)}, bf16[192,256]{1,0:T(8,128)(2,1)S(1)}, u32[]{:S(2)}, u32[]{:S(2)}) collective-permute-start(bf16[192,256]{1,0:T(8,128)(2,1)S(1)} %broadcast_multiply_fusion.q0), channel_id=1, source_target_pairs={{448,0},{384,64},{449,1},{385,65},{450,2},{386,66},{451,3},{387,67... | collective-permute-start | bytes 294920 | tf_op jit(solution)/shard_map/ppermute | solution.py:402
  40.8 31.0 %copy-start = (bf16[256,2048]{1,0:T(8,128)(2,1)S(1)}, bf16[256,2048]{1,0:T(8,128)(2,1)}, u32[]{:S(2)}) copy-start(bf16[256,2048]{1,0:T(8,128)(2,1)} %weight.1) | copy-start | bytes 3145732
  40.8 31.0 %copy-start.1 = (bf16[192,256]{1,0:T(8,128)(2,1)S(1)}, bf16[192,256]{1,0:T(8,128)(2,1)}, u32[]{:S(2)}) copy-start(bf16[192,256]{1,0:T(8,128)(2,1)} %gates.1) | copy-start | bytes 294916
  40.8 62.7 %copy-start.2 = (bf16[24,2048]{1,0:T(8,128)(2,1)S(1)}, bf16[24,2048]{1,0:T(8,128)(2,1)}, u32[]{:S(2)}) copy-start(bf16[24,2048]{1,0:T(8,128)(2,1)} %param.13) | copy-start | bytes 294916
  40.8 62.7 %copy-start.3 = (f32[2048]{0:T(1024)S(1)}, f32[2048]{0:T(1024)}, u32[]{:S(2)}) copy-start(f32[2048]{0:T(1024)} %param.20) | copy-start | bytes 24580
  40.8 63.0 %copy-start.5 = (f32[2048]{0:T(1024)S(1)}, f32[2048]{0:T(1024)}, u32[]{:S(2)}) copy-start(f32[2048]{0:T(1024)} %param.21) | copy-start | bytes 24580
  64.0 6.1 %collective-permute-start.4 = (bf16[72,768]{1,0:T(8,128)(2,1)S(1)}, bf16[72,768]{1,0:T(8,128)(2,1)S(1)}, u32[]{:S(2)}, u32[]{:S(2)}) collective-permute-start(bf16[72,768]{1,0:T(8,128)(2,1)S(1)} %get-tuple-element.14), channel_id=1, source_target_pairs={{0,448},{64,384},{1,449},{65,385},{2,450},{66,386},{3,451},{67,387... | collective-permute-start | bytes 331784 | tf_op jit(solution)/shard_map/ppermute | solution.py:410
  65.3 4.8 %collective-permute-start.5 = (bf16[72,768]{1,0:T(8,128)(2,1)S(1)}, bf16[72,768]{1,0:T(8,128)(2,1)S(1)}, u32[]{:S(2)}, u32[]{:S(2)}) collective-permute-start(bf16[72,768]{1,0:T(8,128)(2,1)S(1)} %get-tuple-element.15), channel_id=1, source_target_pairs={{0,320},{128,448},{64,256},{192,384},{1,321},{129,449},{65,257},{1... | collective-permute-start | bytes 331784 | tf_op jit(solution)/shard_map/ppermute | solution.py:410
  66.6 5.3 %collective-permute-start.6 = (bf16[72,768]{1,0:T(8,128)(2,1)S(1)}, bf16[72,768]{1,0:T(8,128)(2,1)S(1)}, u32[]{:S(2)}, u32[]{:S(2)}) collective-permute-start(bf16[72,768]{1,0:T(8,128)(2,1)S(1)} %get-tuple-element.16), channel_id=1, source_target_pairs={{0,128},{128,320},{320,448},{64,192},{192,256},{256,384},{1,129},{... | collective-permute-start | bytes 331784 | tf_op jit(solution)/shard_map/ppermute | solution.py:410
  72.5 14.9 %collective-permute-start.7 = (bf16[96,2048]{1,0:T(8,128)(2,1)S(1)}, bf16[96,2048]{1,0:T(8,128)(2,1)S(1)}, u32[]{:S(2)}, u32[]{:S(2)}) collective-permute-start(bf16[96,2048]{1,0:T(8,128)(2,1)S(1)} %get-tuple-element.18), channel_id=1, source_target_pairs={{0,1},{1,0},{2,3},{3,2},{4,5},{5,4},{6,7},{7,6},{8,9},{9,8},{10,11... | collective-permute-start | bytes 1179656 | tf_op jit(solution)/shard_map/ppermute | solution.py:360
  87.3 56.0 %copy-start.4 = (f32[2048]{0:T(1024)S(1)}, f32[2048]{0:T(1024)}, u32[]{:S(2)}) copy-start(f32[2048]{0:T(1024)} %param.22) | copy-start | bytes 24580
  124.3 4.4 %collective-permute-start.8 = (bf16[96,2048]{1,0:T(8,128)(2,1)S(1)}, bf16[96,2048]{1,0:T(8,128)(2,1)S(1)}, u32[]{:S(2)}, u32[]{:S(2)}) collective-permute-start(bf16[96,2048]{1,0:T(8,128)(2,1)S(1)} %get-tuple-element.20), channel_id=1, source_target_pairs={{0,1},{1,0},{2,3},{3,2},{4,5},{5,4},{6,7},{7,6},{8,9},{9,8},{10,11... | collective-permute-start | bytes 1179656 | tf_op jit(solution)/shard_map/ppermute | solution.py:360
Sparse Core Ops, SparseCore 0:
  10.3 108.9 all-gather.2
